TPU v7x, 512 devices: a whole 4x8x8 slice. The times are simulated.
512 devices in a mesh: sp: 32 (over z, x), tp: 16 (over y, core).
Axes of the slice: x: 4, y: 8, z: 8, core: 2. Of those that a mesh axis runs over, the one named last changes fastest.
Arguments:
- pool_input: bfloat16 [8192, 1024], P('sp', 'tp'), may hold values from -6 to 6
- pool_weight: bfloat16 [16, 64, 64], P('tp'), may hold values from -0.75 to 0.75
- pool_gain: bfloat16 [1024], P('tp'), may hold values from 0.099609375 to 1.8984375
- out_weight: bfloat16 [1024, 2048], P(None, 'tp'), may hold values from -0.1875 to 0.1875
- resid: bfloat16 [8192, 2048], P('sp', 'tp'), may hold values from -90 to 90
- norm_gain: bfloat16 [2048], P('tp'), may hold values from 0.099609375 to 1.8984375
- routes: int32 [8192, 2], P('sp'), may hold values from 0 to 31, all different within a row; in each aligned block of 256 rows (0 to 255, 256 to 511, ...) at most 32 rows name the same one
- route_weight: float32 [8192, 2], P('sp'), may hold values from 0.2 to 1
- expert_gate: bfloat16 [32, 2048, 4096], P('sp', None, 'tp'), may hold values from -0.375 to 0.375
- expert_up: bfloat16 [32, 2048, 4096], P('sp', None, 'tp'), may hold values from -0.375 to 0.375
- expert_down: bfloat16 [32, 4096, 2048], P('sp', 'tp'), may hold values from -0.0234375 to 0.0234375
Outputs:
- layer_out: bfloat16 [8192, 2048], P('sp', 'tp')
Inputs may be any that keep to these rules, and one draw needn't show every extreme that they name: `routes`: the 2 experts of a position differ. In each aligned block of 256 positions no expert is named by more than 32 assignments; some block reaches that bound.
All inputs are finite; a program needn't handle non-finite values.
Results may differ from a plain program's by a relative error of at most 0.0085.
Values may be sent and summed in bfloat16 or wider, within the bound.
No kernel may reach another device: no remote copies, remote signals or barrier semaphores. Data moves between devices by JAX's collectives and lax.ppermute only.
A program may use at most 64 MiB of HBM per device.

v0:
```python
import functools

import jax
import jax.numpy as jnp
from jax import lax
from jax.experimental import pallas as pl
from jax.experimental.pallas import tpu as pltpu
from jax.sharding import PartitionSpec as P


GSIZE = 64
REACH = 16
TOPK = 2
CORES = 2

GATE_LIMIT = 7.0
GATE_ALPHA = 1.702
NORM_EPS = 1e-05

F32 = jnp.float32
BF16 = jnp.bfloat16
MIB = 1024 * 1024


def iota(shape, dim):
    return lax.broadcasted_iota(jnp.int32, shape, dim)


def mm(a, b, ca=1, cb=0):
    return lax.dot_general(a, b, (((ca,), (cb,)), ((), ())), preferred_element_type=F32)


def call(kernel, out_shape, args, flops, mib, aliases=None, space=pltpu.VMEM, scratch=()):
    return pl.pallas_call(
        kernel,
        out_shape=out_shape,
        in_specs=[pl.BlockSpec(memory_space=space)] * len(args),
        scratch_shapes=scratch,
        out_specs=jax.tree.map(lambda _: pl.BlockSpec(memory_space=pltpu.VMEM), out_shape),
        compiler_params=pltpu.CompilerParams(vmem_limit_bytes=mib * MIB),
        cost_estimate=pl.CostEstimate(flops=flops, bytes_accessed=flops // 512, transcendentals=0),
        input_output_aliases=aliases or {},
    )(*args)


def pool_kernel(before_ref, x_ref, w_ref, gain_ref, norm_ref, out_ref):
    rows, width = x_ref.shape
    window = lax.shift_left(jnp.int32(2), lax.rem(lax.axis_index("tp"), 4))
    place = iota((rows, rows), 0) - iota((rows, rows), 1)
    inside = jnp.where((place >= 0) & (place < window), 1.0, 0.0).astype(BF16)
    gap = iota((rows, REACH), 0) + REACH - iota((rows, REACH), 1)
    behind = jnp.where(gap < window, 1.0, 0.0).astype(BF16)
    x = x_ref[...]
    total = mm(inside, x) + mm(behind, before_ref[...])
    spot = lax.axis_index("sp") * rows + iota((rows, 1), 0)
    count = jnp.minimum(spot + 1, window).astype(F32)
    pooled = (total / count - x.astype(F32)).astype(BF16)
    mixed = (mm(pooled, w_ref[...]) * gain_ref[...].astype(F32)).astype(BF16)
    eye = jnp.where(iota((width, width), 0) == iota((width, width), 1), 1.0, 0.0).astype(BF16)
    out_ref[:width, :] = mm(eye, mixed, 1, 1).astype(BF16)
    features = norm_ref.shape[1]
    tail = out_ref.shape[0] - width
    out_ref[width:, :features] = jnp.broadcast_to(norm_ref[...].astype(F32), (tail, features)).astype(BF16)
    out_ref[width:, features:] = jnp.zeros((tail, out_ref.shape[1] - features), BF16)


def row_slots(routes_ref, experts, capacity):
    rows = routes_ref.shape[1]
    named = [iota((experts, rows), 0) == routes_ref[k : k + 1, :] for k in range(TOPK)]
    ones = sum(jnp.where(n, 1.0, 0.0) for n in named)
    upper = jnp.where(iota((rows, rows), 0) < iota((rows, rows), 1), 1.0, 0.0).astype(BF16)
    earlier = mm(ones.astype(BF16), upper)
    slots = []
    for k in range(TOPK):
        rank = jnp.sum(jnp.where(named[k], earlier, 0.0), axis=0, keepdims=True).astype(jnp.int32)
        slots.append(routes_ref[k : k + 1, :] * capacity + rank)
    return slots


def column_slots(routes_ref, experts, capacity):
    rows = routes_ref.shape[0]
    named = [iota((rows, experts), 1) == routes_ref[:, k : k + 1] for k in range(TOPK)]
    ones = sum(jnp.where(n, 1.0, 0.0) for n in named)
    lower = jnp.where(iota((rows, rows), 0) > iota((rows, rows), 1), 1.0, 0.0).astype(BF16)
    earlier = mm(lower, ones.astype(BF16))
    slots = []
    for k in range(TOPK):
        rank = jnp.sum(jnp.where(named[k], earlier, 0.0), axis=1, keepdims=True).astype(jnp.int32)
        slots.append(routes_ref[:, k : k + 1] * capacity + rank)
    return slots


def slot_ids(shape, dim, capacity, core):
    half = capacity // CORES
    place = iota(shape, dim)
    return lax.div(place, half) * capacity + core * half + lax.rem(place, half)


def column_slots(routes_ref, experts, capacity):
    rows = routes_ref.shape[0]
    named = [iota((rows, experts), 1) == routes_ref[:, k : k + 1] for k in range(TOPK)]
    ones = sum(jnp.where(n, 1.0, 0.0) for n in named)
    lower = jnp.where(iota((rows, rows), 0) > iota((rows, rows), 1), 1.0, 0.0).astype(BF16)
    earlier = mm(lower, ones.astype(BF16))
    slots = []
    for k in range(TOPK):
        rank = jnp.sum(jnp.where(named[k], earlier, 0.0), axis=1, keepdims=True).astype(jnp.int32)
        slots.append(routes_ref[:, k : k + 1] * capacity + rank)
    return slots


class Pack:
    def __init__(self, deep, width, channels, rows):
        self.gate, self.up, self.down = 0, deep, 2 * deep
        self.project = 3 * deep
        self.resid = self.project + channels // 2
        self.rows = self.resid + rows // 2
        self.width = width


def prep_kernel(pack, gate, up, down, project, resid, x, w, gain, norm, out, x_out, w_out, gain_out, norm_out, sems):
    width, features = pack.width, project.shape[1]
    units = down.shape[0]
    pairs = [(x, x_out), (w, w_out), (gain, gain_out), (norm, norm_out)]
    for base, source in ((pack.project, project), (pack.resid, resid)):
        half = source.shape[0] // 2
        for i in range(2):
            pairs.append(
                (source.at[i * half : (i + 1) * half, :],
                 out.at[base : base + half, i * features : (i + 1) * features])
            )
    pairs.append((gate, out.at[pack.gate : pack.up, :]))
    pairs.append((up, out.at[pack.up : pack.down, :]))
    for i in range(down.shape[1] // width):
        pairs.append(
            (down.at[:, i * width : (i + 1) * width], out.at[pack.down + i * units : pack.down + (i + 1) * units, :])
        )
    copies = [pltpu.make_async_copy(a, b, sems.at[i]) for i, (a, b) in enumerate(pairs)]
    for copy in copies:
        copy.start()
    for copy in copies:
        copy.wait()


def dispatch_kernel(pack, experts, capacity, mixed_ref, own_ref, other_ref, routes_ref, stream_ref, gain_ref, out_ref):
    core = lax.rem(lax.axis_index("tp"), CORES)
    members, _, rows = mixed_ref.shape
    features = stream_ref.shape[1]
    mixed = mixed_ref[:, :GSIZE, :].reshape(members * GSIZE, rows)
    deep = members * GSIZE // 2
    streams = []
    for ref in (own_ref, other_ref):
        halves = [ref[pack.project : pack.resid, i * features : (i + 1) * features] for i in range(2)]
        projected = mm(mixed[:deep], halves[0], 0, 0) + mm(mixed[deep:], halves[1], 0, 0)
        resid = jnp.concatenate(
            [ref[pack.resid : pack.rows, i * features : (i + 1) * features] for i in range(2)], axis=0
        )
        streams.append((resid.astype(F32) + projected).astype(BF16))
    own, other = streams
    stream_ref[...] = own
    for t in range(members):
        y, c = divmod(t, CORES)
        gain_ref[y, :, c * features : (c + 1) * features] = mixed_ref[t, GSIZE : GSIZE + 8, :features].astype(F32)
    slots = row_slots(routes_ref, experts, capacity)
    ids = slot_ids((out_ref.shape[0], rows), 0, capacity, core)
    hit = (slots[0] == ids) | (slots[1] == ids)
    chosen = jnp.where(hit, 1.0, 0.0).astype(BF16)
    out_ref[:, :features] = mm(chosen, jnp.where(core == 0, own, other)).astype(BF16)
    out_ref[:, features:] = mm(chosen, jnp.where(core == 0, other, own)).astype(BF16)


def add_chunk(pack, x, chip, gain_ref, packs, acc_ref, square_ref, first=False):
    width = x.shape[1]
    value = x.astype(F32)
    square = value * value
    lanes = square_ref.shape[1]
    square = sum(square[:, i : i + lanes] for i in range(0, width, lanes))
    scaled = (value * gain_ref[chip, 0:1, :]).astype(BF16)
    for i, base in enumerate((pack.gate, pack.up)):
        for j, ref in enumerate(packs):
            rows = pl.ds(pl.multiple_of(base + chip * width, width), width)
            part = mm(scaled, ref[rows, :])
            columns = part.shape[1]
            span = slice((2 * i + j) * columns, (2 * i + j + 1) * columns)
            acc_ref[:, span] = part if first else acc_ref[:, span] + part
    square_ref[...] = square if first else square_ref[...] + square


def chip_at(chips, step):
    here = lax.div(lax.axis_index("tp"), CORES)
    return lax.rem(here + step + chips, chips)


def first_kernel(pack, chips, x_ref, gain_ref, own_ref, other_ref, acc_ref, square_ref):
    add_chunk(pack, x_ref[...], chip_at(chips, 0), gain_ref, (own_ref, other_ref), acc_ref, square_ref, True)


def both_kernel(pack, chips, step, p_ref, m_ref, gain_ref, own_ref, other_ref, acc_in, square_in, acc_ref, square_ref):
    packs = (own_ref, other_ref)
    add_chunk(pack, p_ref[...], chip_at(chips, -step), gain_ref, packs, acc_ref, square_ref)
    add_chunk(pack, m_ref[...], chip_at(chips, step), gain_ref, packs, acc_ref, square_ref)


def partial(pack, hidden_ref, packs, chip):
    units = hidden_ref.shape[1] // CORES
    rows = pl.ds(pl.multiple_of(pack.down + chip * units, units), units)
    return sum(mm(hidden_ref[:, i * units : (i + 1) * units], ref[rows, :]) for i, ref in enumerate(packs))


def last_kernel(
    pack, chips, total, p_ref, m_ref, gain_ref, own_ref, other_ref, acc_in, square_in,
    acc_ref, square_ref, hidden_ref, up_ref, low_ref,
):
    x = jnp.concatenate([p_ref[...], m_ref[...]], axis=0)
    packs = (own_ref, other_ref)
    far = chip_at(chips, chips // 2)
    add_chunk(pack, x, far, gain_ref, packs, acc_ref, square_ref)
    mean = jnp.sum(square_ref[...], axis=1, keepdims=True) / total
    scale = lax.rsqrt(mean + NORM_EPS)
    units = hidden_ref.shape[1]
    gate = jnp.minimum(acc_ref[:, :units] * scale, GATE_LIMIT)
    up = jnp.clip(acc_ref[:, units:] * scale, -GATE_LIMIT, GATE_LIMIT)
    hidden_ref[...] = ((up + 1.0) * gate * jax.nn.sigmoid(GATE_ALPHA * gate)).astype(BF16)
    out = partial(pack, hidden_ref, packs, far).astype(BF16)
    half = up_ref.shape[0]
    up_ref[...] = out[:half]
    low_ref[...] = out[half:]


def down_kernel(pack, chips, steps, hidden_ref, own_ref, other_ref, *outs):
    for step, out_ref in zip(steps, outs):
        out_ref[...] = partial(pack, hidden_ref, (own_ref, other_ref), chip_at(chips, step))


def add_kernel(low, part_ref, came_ref, out_ref):
    rows, held = part_ref.shape[0], came_ref.shape[0]
    if held == rows:
        out_ref[...] = (part_ref[...] + came_ref[...].astype(F32)).astype(BF16)
        return
    near = slice(rows - held, rows) if low else slice(0, held)
    rest = slice(0, rows - held) if low else slice(held, rows)
    out_ref[near, :] = (part_ref[near, :] + came_ref[...].astype(F32)).astype(BF16)
    out_ref[rest, :] = part_ref[rest, :].astype(BF16)


def own_kernel(part_ref, p_ref, m_ref, out_ref):
    out_ref[...] = (part_ref[...] + p_ref[...].astype(F32) + m_ref[...].astype(F32)).astype(BF16)


def pick_kernel(experts, capacity, back_ref, routes_ref, weight_ref, mine_ref, other_ref):
    core = lax.rem(lax.axis_index("tp"), CORES)
    slots = column_slots(routes_ref, experts, capacity)
    shape = (routes_ref.shape[0], back_ref.shape[0])
    ids = slot_ids(shape, 1, capacity, core)
    rows = back_ref[...]
    total = 0.0
    for k in range(TOPK):
        chosen = jnp.where(slots[k] == ids, 1.0, 0.0).astype(BF16)
        total = total + mm(chosen, rows) * weight_ref[:, k : k + 1]
    features = mine_ref.shape[1]
    left, right = total[:, :features], total[:, features:]
    mine_ref[...] = jnp.where(core == 0, left, right)
    other_ref[...] = jnp.where(core == 0, right, left)


def join_kernel(stream_ref, mine_ref, other_ref, out_ref):
    out_ref[...] = (stream_ref[...].astype(F32) + mine_ref[...] + other_ref[...]).astype(BF16)


def on_device(
    pool_input,
    pool_weight,
    pool_gain,
    out_weight,
    resid,
    norm_gain,
    routes,
    route_weight,
    expert_gate,
    expert_up,
    expert_down,
):
    tok_rows, channels = pool_input.shape
    features = out_weight.shape[1]
    blocks, members = lax.axis_size("sp"), lax.axis_size("tp")
    chips = members // CORES
    experts = blocks * expert_gate.shape[0]
    capacity = 2 * tok_rows * TOPK // experts
    half = capacity // CORES
    width = features * CORES
    total = features * members
    held = blocks * half

    def along(value, step):
        pairs = [
            (y * CORES + c, (y + step) % chips * CORES + c) for y in range(chips) for c in range(CORES)
        ]
        return lax.ppermute(value, "tp", pairs)

    def across(value):
        return lax.ppermute(value, "tp", [(t, t ^ 1) for t in range(members)])

    shape = jax.ShapeDtypeStruct
    deep, units = expert_gate.shape[1:]
    pack = Pack(deep, width, out_weight.shape[0], tok_rows)
    before = lax.ppermute(
        pool_input[tok_rows - REACH :], "sp", [(s, s + 1) for s in range(blocks - 1)]
    )
    small = (pool_input, pool_weight[0], pool_gain.reshape(1, channels), norm_gain.reshape(1, features))
    own, *small = call(
        functools.partial(prep_kernel, pack),
        (shape((pack.rows, width), BF16), *(shape(v.shape, v.dtype) for v in small)),
        (expert_gate[0], expert_up[0], expert_down[0], out_weight, resid, *small),
        pack.rows * width * 512,
        58,
        space=pltpu.HBM,
        scratch=[pltpu.SemaphoreType.DMA((10 + chips,))],
    )
    other = across(own)
    packs = (own, other)
    pooled = call(
        pool_kernel,
        shape((GSIZE + 16, tok_rows), BF16),
        (before, *small),
        tok_rows * tok_rows * channels * 2,
        8,
    )
    mixed = lax.all_gather(pooled, "tp", axis=0, tiled=False)
    stored, gains, sent = call(
        functools.partial(dispatch_kernel, pack, experts, capacity),
        (
            shape((tok_rows, features), BF16),
            shape((chips, 8, width), F32),
            shape((experts * half, width), BF16),
        ),
        (mixed, *packs, routes.T),
        2 * experts * half * width * tok_rows,
        16,
    )
    x = lax.all_to_all(
        sent.reshape(experts, half, width), "sp", split_axis=0, concat_axis=0, tiled=True
    ).reshape(held, width)

    acc_shape = (shape((held, 4 * units), F32), shape((held, 128), F32))
    chunk_flops = 2 * held * width * 4 * units
    acc, square = call(
        functools.partial(first_kernel, pack, chips), acc_shape, (x, gains, *packs), chunk_flops, 16
    )
    ahead, back = x, x
    middle = held // 2
    last = chips // 2
    for step in range(1, last):
        ahead = along(ahead, 1)
        back = along(back, -1)
        acc, square = call(
            functools.partial(both_kernel, pack, chips, step),
            acc_shape,
            (ahead, back, gains, *packs, acc, square),
            2 * chunk_flops,
            16,
            {5: 0, 6: 1},
        )
    ahead = along(ahead[:middle], 1)
    back = along(back[middle:], -1)
    _, _, hidden, ahead, back = call(
        functools.partial(last_kernel, pack, chips, float(total)),
        (
            *acc_shape,
            shape((held, CORES * units), BF16),
            shape((middle, width), BF16),
            shape((middle, width), BF16),
        ),
        (ahead, back, gains, *packs, acc, square),
        2 * chunk_flops,
        24,
        {5: 0, 6: 1},
    )
    for step in range(last - 1, -1, -1):
        steps = (step, -step) if step else (0,)
        parts = call(
            functools.partial(down_kernel, pack, chips, steps),
            (shape((held, width), F32),) * len(steps),
            (hidden, *packs),
            chunk_flops // 2 * len(steps),
            16,
        )
        ahead = along(ahead, 1)
        back = along(back, -1)
        if step:
            ahead, back = (
                call(
                    functools.partial(add_kernel, low),
                    shape((held, width), BF16),
                    (part, came),
                    held * width,
                    8,
                )
                for low, (part, came) in enumerate(zip(parts, (ahead, back)))
            )
    result = call(own_kernel, shape((held, width), BF16), (*parts, ahead, back), held * width, 8)
    returned = lax.all_to_all(
        result.reshape(blocks, half, width), "sp", split_axis=0, concat_axis=0, tiled=True
    ).reshape(experts * half, width)
    mine, theirs = call(
        functools.partial(pick_kernel, experts, capacity),
        (shape((tok_rows, features), F32),) * 2,
        (returned, routes, route_weight),
        4 * experts * half * width * tok_rows,
        12,
    )
    return call(
        join_kernel,
        shape((tok_rows, features), BF16),
        (stored, mine, across(theirs)),
        tok_rows * features,
        8,
    )


def solution(mesh):
    in_specs = (
        P("sp", "tp"),
        P("tp", None, None),
        P("tp"),
        P(None, "tp"),
        P("sp", "tp"),
        P("tp"),
        P("sp", None),
        P("sp", None),
        P("sp", None, "tp"),
        P("sp", None, "tp"),
        P("sp", "tp", None),
    )
    out_specs = P("sp", "tp")

    return jax.shard_map(on_device, mesh=mesh, in_specs=in_specs, out_specs=out_specs, check_vma=False)
```

profile of v0, /device:TPU:1, one launch (start us, length us, event | category | flops | bytes accessed | tf_op | source)
XLA Modules:
  0.0 176.0 jit_solution(2287065524064744812)
XLA Ops:
  1.5 4.0 %shard_map.109 = (bf16[6784,256]{1,0:T(8,128)(2,1)}, bf16[256,64]{1,0:T(8,128)(2,1)}, bf16[64,64]{1,0:T(8,128)(2,1)}, bf16[1,64]{1,0:T(2,128)(2,1)}, bf16[1,128]{1,0:T(2,128)(2,1)}) custom-call(bf16[2048,256]{1,0:T(8,128)(2,1)} %bitcast.19, bf16[2048,256]{1,0:T(8,128)(2,1)} %bitcast.20, bf16[256,2048]{1,0:T(8,128)(2,1)} %bitcast.21, ...), custom_call_target="tpu_custom_call" | custom-call | flops 889192448 | bytes 1736704 | tf_op jit(solution)/shard_map/pallas_call | solution.py:34
  5.5 8.7 %collective-permute-start.1 = (bf16[6784,256]{1,0:T(8,128)(2,1)}, bf16[6784,256]{1,0:T(8,128)(2,1)S(1)}, u32[]{:S(2)}, u32[]{:S(2)}) collective-permute-start(bf16[6784,256]{1,0:T(8,128)(2,1)} %get-tuple-element.36.own_ref), channel_id=1, source_target_pairs={{0,1},{1,0},{2,3},{3,2},{4,5},{5,4},{6,7},{7,6},{8,9},{9,8},{10,11... | collective-permute-start | bytes 10420232 | tf_op jit(solution)/shard_map/ppermute | solution.py:301
  20.3 16.6 %all-gather = bf16[1280,256]{1,0:T(8,128)(2,1)S(1)} all-gather(bf16[80,256]{1,0:T(8,128)(2,1)S(1)} %shard_map.110), channel_id=2, replica_groups=mesh['sp'=32,'tp'=16] {'tp'}, dimensions={0}, use_global_device_ids=true | all-gather | bytes 696320 | tf_op jit(solution)/shard_map/all_gather | solution.py:328
  36.9 2.0 %copy-done = bf16[6784,256]{1,0:T(8,128)(2,1)S(1)} copy-done((bf16[6784,256]{1,0:T(8,128)(2,1)S(1)}, bf16[6784,256]{1,0:T(8,128)(2,1)}, u32[]{:S(2)}) %copy-start) | copy-done | bytes 3473432
  39.7 25.9 %all_to_all.10 = bf16[32,16,256]{2,1,0:T(8,128)(2,1)S(1)} all-to-all(bf16[32,16,256]{2,1,0:T(8,128)(2,1)S(1)} %bitcast.17), channel_id=1, replica_groups=mesh['sp'=32,'tp'=16] {'sp'}, dimensions={0} | all-to-all | bytes 524288 | tf_op jit(solution)/shard_map/all_to_all | solution.py:340
  67.5 4.6 %collective-permute-start.6 = (bf16[512,256]{1,0:T(8,128)(2,1)S(1)}, bf16[512,256]{1,0:T(8,128)(2,1)S(1)}, u32[]{:S(2)}, u32[]{:S(2)}) collective-permute-start(bf16[512,256]{1,0:T(8,128)(2,1)S(1)} %bitcast.14), channel_id=1, source_target_pairs={{0,14},{1,15},{2,0},{3,1},{4,2},{5,3},{6,4},{7,5},{8,6},{9,7},{10,... | collective-permute-start | bytes 786440 | tf_op jit(solution)/shard_map/ppermute | solution.py:298
  75.9 4.6 %collective-permute-start.7 = (bf16[512,256]{1,0:T(8,128)(2,1)S(1)}, bf16[512,256]{1,0:T(8,128)(2,1)S(1)}, u32[]{:S(2)}, u32[]{:S(2)}) collective-permute-start(bf16[512,256]{1,0:T(8,128)(2,1)S(1)} %collective-permute-done.6.m_ref), channel_id=1, source_target_pairs={{0,14},{1,15},{2,0},{3,1},{4,2},{5,3},{6,4},{7,5},{8,6},{9,7},{10,... | collective-permute-start | bytes 786440 | tf_op jit(solution)/shard_map/ppermute | solution.py:298
  84.2 4.6 %collective-permute-start.8 = (bf16[512,256]{1,0:T(8,128)(2,1)S(1)}, bf16[512,256]{1,0:T(8,128)(2,1)S(1)}, u32[]{:S(2)}, u32[]{:S(2)}) collective-permute-start(bf16[512,256]{1,0:T(8,128)(2,1)S(1)} %collective-permute-done.7.m_ref), channel_id=1, source_target_pairs={{0,14},{1,15},{2,0},{3,1},{4,2},{5,3},{6,4},{7,5},{8,6},{9,7},{10,... | collective-permute-start | bytes 786440 | tf_op jit(solution)/shard_map/ppermute | solution.py:298
  90.6 1.9 %collective-permute-start.5 = (bf16[256,256]{1,0:T(8,128)(2,1)S(1)}, bf16[256,256]{1,0:T(8,128)(2,1)S(1)}, u32[]{:S(2)}, u32[]{:S(2)}) collective-permute-start(bf16[256,256]{1,0:T(8,128)(2,1)S(1)} %slice.13), channel_id=1, source_target_pairs={{0,2},{1,3},{2,4},{3,5},{4,6},{5,7},{6,8},{7,9},{8,10},{9,11},{10,... | collective-permute-start | bytes 393224 | tf_op jit(solution)/shard_map/ppermute | solution.py:298
  92.5 4.6 %collective-permute-start.9 = (bf16[256,256]{1,0:T(8,128)(2,1)S(1)}, bf16[256,256]{1,0:T(8,128)(2,1)S(1)}, u32[]{:S(2)}, u32[]{:S(2)}) collective-permute-start(bf16[256,256]{1,0:T(8,128)(2,1)S(1)} %slice.14), channel_id=1, source_target_pairs={{0,14},{1,15},{2,0},{3,1},{4,2},{5,3},{6,4},{7,5},{8,6},{9,7},{10,... | collective-permute-start | bytes 393224 | tf_op jit(solution)/shard_map/ppermute | solution.py:298
  101.5 3.5 %collective-permute-start.14 = (bf16[256,256]{1,0:T(8,128)(2,1)S(1)}, bf16[256,256]{1,0:T(8,128)(2,1)S(1)}, u32[]{:S(2)}, u32[]{:S(2)}) collective-permute-start(bf16[256,256]{1,0:T(8,128)(2,1)S(1)} %get-tuple-element.56), channel_id=1, source_target_pairs={{0,14},{1,15},{2,0},{3,1},{4,2},{5,3},{6,4},{7,5},{8,6},{9,7},{10,... | collective-permute-start | bytes 393224 | tf_op jit(solution)/shard_map/ppermute | solution.py:298
  105.0 1.9 %collective-permute-start.10 = (bf16[256,256]{1,0:T(8,128)(2,1)S(1)}, bf16[256,256]{1,0:T(8,128)(2,1)S(1)}, u32[]{:S(2)}, u32[]{:S(2)}) collective-permute-start(bf16[256,256]{1,0:T(8,128)(2,1)S(1)} %get-tuple-element.52), channel_id=1, source_target_pairs={{0,2},{1,3},{2,4},{3,5},{4,6},{5,7},{6,8},{7,9},{8,10},{9,11},{10,... | collective-permute-start | bytes 393224 | tf_op jit(solution)/shard_map/ppermute | solution.py:298
  107.4 4.6 %collective-permute-start.15 = (bf16[512,256]{1,0:T(8,128)(2,1)S(1)}, bf16[512,256]{1,0:T(8,128)(2,1)S(1)}, u32[]{:S(2)}, u32[]{:S(2)}) collective-permute-start(bf16[512,256]{1,0:T(8,128)(2,1)S(1)} %shard_map.124), channel_id=1, source_target_pairs={{0,14},{1,15},{2,0},{3,1},{4,2},{5,3},{6,4},{7,5},{8,6},{9,7},{10,... | collective-permute-start | bytes 786440 | tf_op jit(solution)/shard_map/ppermute | solution.py:298
  112.1 1.9 %collective-permute-start.11 = (bf16[512,256]{1,0:T(8,128)(2,1)S(1)}, bf16[512,256]{1,0:T(8,128)(2,1)S(1)}, u32[]{:S(2)}, u32[]{:S(2)}) collective-permute-start(bf16[512,256]{1,0:T(8,128)(2,1)S(1)} %shard_map.121), channel_id=1, source_target_pairs={{0,2},{1,3},{2,4},{3,5},{4,6},{5,7},{6,8},{7,9},{8,10},{9,11},{10,... | collective-permute-start | bytes 786440 | tf_op jit(solution)/shard_map/ppermute | solution.py:298
  114.5 2.3 %collective-permute-done.15.came_ref = bf16[512,256]{1,0:T(8,128)(2,1)S(1)} collective-permute-done((bf16[512,256]{1,0:T(8,128)(2,1)S(1)}, bf16[512,256]{1,0:T(8,128)(2,1)S(1)}, u32[]{:S(2)}, u32[]{:S(2)}) %collective-permute-start.15) | collective-permute-done | bytes 262176 | tf_op jit(solution)/shard_map/ppermute | solution.py:298
  116.8 5.0 %collective-permute-start.16 = (bf16[512,256]{1,0:T(8,128)(2,1)S(1)}, bf16[512,256]{1,0:T(8,128)(2,1)S(1)}, u32[]{:S(2)}, u32[]{:S(2)}) collective-permute-start(bf16[512,256]{1,0:T(8,128)(2,1)S(1)} %shard_map.125), channel_id=1, source_target_pairs={{0,14},{1,15},{2,0},{3,1},{4,2},{5,3},{6,4},{7,5},{8,6},{9,7},{10,... | collective-permute-start | bytes 786440 | tf_op jit(solution)/shard_map/ppermute | solution.py:298
  124.3 3.2 %collective-permute-done.16.came_ref = bf16[512,256]{1,0:T(8,128)(2,1)S(1)} collective-permute-done((bf16[512,256]{1,0:T(8,128)(2,1)S(1)}, bf16[512,256]{1,0:T(8,128)(2,1)S(1)}, u32[]{:S(2)}, u32[]{:S(2)}) %collective-permute-start.16) | collective-permute-done | bytes 262176 | tf_op jit(solution)/shard_map/ppermute | solution.py:298
  127.5 5.3 %collective-permute-start.17 = (bf16[512,256]{1,0:T(8,128)(2,1)S(1)}, bf16[512,256]{1,0:T(8,128)(2,1)S(1)}, u32[]{:S(2)}, u32[]{:S(2)}) collective-permute-start(bf16[512,256]{1,0:T(8,128)(2,1)S(1)} %shard_map.126), channel_id=1, source_target_pairs={{0,14},{1,15},{2,0},{3,1},{4,2},{5,3},{6,4},{7,5},{8,6},{9,7},{10,... | collective-permute-start | bytes 786440 | tf_op jit(solution)/shard_map/ppermute | solution.py:298
  132.9 1.9 %collective-permute-start.13 = (bf16[512,256]{1,0:T(8,128)(2,1)S(1)}, bf16[512,256]{1,0:T(8,128)(2,1)S(1)}, u32[]{:S(2)}, u32[]{:S(2)}) collective-permute-start(bf16[512,256]{1,0:T(8,128)(2,1)S(1)} %shard_map.123), channel_id=1, source_target_pairs={{0,2},{1,3},{2,4},{3,5},{4,6},{5,7},{6,8},{7,9},{8,10},{9,11},{10,... | collective-permute-start | bytes 786440 | tf_op jit(solution)/shard_map/ppermute | solution.py:298
  135.2 2.5 %collective-permute-done.17.m_ref = bf16[512,256]{1,0:T(8,128)(2,1)S(1)} collective-permute-done((bf16[512,256]{1,0:T(8,128)(2,1)S(1)}, bf16[512,256]{1,0:T(8,128)(2,1)S(1)}, u32[]{:S(2)}, u32[]{:S(2)}) %collective-permute-start.17) | collective-permute-done | bytes 262176 | tf_op jit(solution)/shard_map/ppermute | solution.py:298
  137.6 5.1 %collective-permute-done.13.p_ref = bf16[512,256]{1,0:T(8,128)(2,1)S(1)} collective-permute-done((bf16[512,256]{1,0:T(8,128)(2,1)S(1)}, bf16[512,256]{1,0:T(8,128)(2,1)S(1)}, u32[]{:S(2)}, u32[]{:S(2)}) %collective-permute-start.13) | collective-permute-done | bytes 262176 | tf_op jit(solution)/shard_map/ppermute | solution.py:298
  143.5 6.0 %all-to-all-start.1 = ((bf16[32,16,256]{2,1,0:T(8,128)(2,1)}), bf16[32,16,256]{2,1,0:T(8,128)(2,1)S(1)}, u32[]{:S(2)}, u32[]{:S(2)}) async-start(bf16[32,16,256]{2,1,0:T(8,128)(2,1)} %bitcast.10), calls=%async_computation.1 | async-start | bytes 524288 | tf_op jit(solution)/shard_map/all_to_all | solution.py:401
  149.8 10.1 %all-to-all-done.1 = bf16[32,16,256]{2,1,0:T(8,128)(2,1)S(1)} async-done(((bf16[32,16,256]{2,1,0:T(8,128)(2,1)}), bf16[32,16,256]{2,1,0:T(8,128)(2,1)S(1)}, u32[]{:S(2)}, u32[]{:S(2)}) %all-to-all-start.1) | async-done | bytes 262176 | tf_op jit(solution)/shard_map/all_to_all | solution.py:401
  160.7 13.7 %collective-permute-start.18 = (f32[256,128]{1,0:T(8,128)S(1)}, f32[256,128]{1,0:T(8,128)S(1)}, u32[]{:S(2)}, u32[]{:S(2)}) collective-permute-start(f32[256,128]{1,0:T(8,128)S(1)} %get-tuple-element.58), channel_id=1, source_target_pairs={{0,1},{1,0},{2,3},{3,2},{4,5},{5,4},{6,7},{7,6},{8,9},{9,8},{10,11... | collective-permute-start | bytes 393224 | tf_op jit(solution)/shard_map/ppermute | solution.py:301
  (61 shorter events, 31.1 us)
Async XLA Ops:
  1.5 35.4 %copy-start.4 = (s32[256,2]{0,1:T(2,128)S(1)}, s32[256,2]{0,1:T(2,128)}, u32[]{:S(2)}) copy-start(s32[256,2]{0,1:T(2,128)} %param.17) | copy-start | bytes 6148
  5.5 31.4 %collective-permute-start.1 = (bf16[6784,256]{1,0:T(8,128)(2,1)}, bf16[6784,256]{1,0:T(8,128)(2,1)S(1)}, u32[]{:S(2)}, u32[]{:S(2)}) collective-permute-start(bf16[6784,256]{1,0:T(8,128)(2,1)} %get-tuple-element.36.own_ref), channel_id=1, source_target_pairs={{0,1},{1,0},{2,3},{3,2},{4,5},{5,4},{6,7},{7,6},{8,9},{9,8},{10,11... | collective-permute-start | bytes 10420232 | tf_op jit(solution)/shard_map/ppermute | solution.py:301
  15.0 2.0 %collective-permute-start = (bf16[16,64]{1,0:T(8,128)(2,1)S(1)}, bf16[16,64]{1,0:T(8,128)(2,1)S(1)}, u32[]{:S(2)}, u32[]{:S(2)}) collective-permute-start(bf16[16,64]{1,0:T(8,128)(2,1)S(1)} %slice.12), channel_id=1, source_target_pairs={{0,16},{16,32},{32,48},{48,64},{64,80},{80,96},{96,112},{112,128},... | collective-permute-start | bytes 6152 | tf_op jit(solution)/shard_map/ppermute | solution.py:306
  36.9 2.0 %copy-start = (bf16[6784,256]{1,0:T(8,128)(2,1)S(1)}, bf16[6784,256]{1,0:T(8,128)(2,1)}, u32[]{:S(2)}) copy-start(bf16[6784,256]{1,0:T(8,128)(2,1)} %get-tuple-element.36.own_ref) | copy-start | bytes 10420228
  65.6 8.3 %collective-permute-start.2 = (bf16[512,256]{1,0:T(8,128)(2,1)S(1)}, bf16[512,256]{1,0:T(8,128)(2,1)S(1)}, u32[]{:S(2)}, u32[]{:S(2)}) collective-permute-start(bf16[512,256]{1,0:T(8,128)(2,1)S(1)} %bitcast.13), channel_id=1, source_target_pairs={{0,2},{1,3},{2,4},{3,5},{4,6},{5,7},{6,8},{7,9},{8,10},{9,11},{10,... | collective-permute-start | bytes 786440 | tf_op jit(solution)/shard_map/ppermute | solution.py:298
  67.5 8.3 %collective-permute-start.6 = (bf16[512,256]{1,0:T(8,128)(2,1)S(1)}, bf16[512,256]{1,0:T(8,128)(2,1)S(1)}, u32[]{:S(2)}, u32[]{:S(2)}) collective-permute-start(bf16[512,256]{1,0:T(8,128)(2,1)S(1)} %bitcast.14), channel_id=1, source_target_pairs={{0,14},{1,15},{2,0},{3,1},{4,2},{5,3},{6,4},{7,5},{8,6},{9,7},{10,... | collective-permute-start | bytes 786440 | tf_op jit(solution)/shard_map/ppermute | solution.py:298
  73.9 8.3 %collective-permute-start.3 = (bf16[512,256]{1,0:T(8,128)(2,1)S(1)}, bf16[512,256]{1,0:T(8,128)(2,1)S(1)}, u32[]{:S(2)}, u32[]{:S(2)}) collective-permute-start(bf16[512,256]{1,0:T(8,128)(2,1)S(1)} %collective-permute-done.2.p_ref), channel_id=1, source_target_pairs={{0,2},{1,3},{2,4},{3,5},{4,6},{5,7},{6,8},{7,9},{8,10},{9,11},{10,... | collective-permute-start | bytes 786440 | tf_op jit(solution)/shard_map/ppermute | solution.py:298
  75.9 8.3 %collective-permute-start.7 = (bf16[512,256]{1,0:T(8,128)(2,1)S(1)}, bf16[512,256]{1,0:T(8,128)(2,1)S(1)}, u32[]{:S(2)}, u32[]{:S(2)}) collective-permute-start(bf16[512,256]{1,0:T(8,128)(2,1)S(1)} %collective-permute-done.6.m_ref), channel_id=1, source_target_pairs={{0,14},{1,15},{2,0},{3,1},{4,2},{5,3},{6,4},{7,5},{8,6},{9,7},{10,... | collective-permute-start | bytes 786440 | tf_op jit(solution)/shard_map/ppermute | solution.py:298
  82.3 8.3 %collective-permute-start.4 = (bf16[512,256]{1,0:T(8,128)(2,1)S(1)}, bf16[512,256]{1,0:T(8,128)(2,1)S(1)}, u32[]{:S(2)}, u32[]{:S(2)}) collective-permute-start(bf16[512,256]{1,0:T(8,128)(2,1)S(1)} %collective-permute-done.3.p_ref), channel_id=1, source_target_pairs={{0,2},{1,3},{2,4},{3,5},{4,6},{5,7},{6,8},{7,9},{8,10},{9,11},{10,... | collective-permute-start | bytes 786440 | tf_op jit(solution)/shard_map/ppermute | solution.py:298
  84.2 8.3 %collective-permute-start.8 = (bf16[512,256]{1,0:T(8,128)(2,1)S(1)}, bf16[512,256]{1,0:T(8,128)(2,1)S(1)}, u32[]{:S(2)}, u32[]{:S(2)}) collective-permute-start(bf16[512,256]{1,0:T(8,128)(2,1)S(1)} %collective-permute-done.7.m_ref), channel_id=1, source_target_pairs={{0,14},{1,15},{2,0},{3,1},{4,2},{5,3},{6,4},{7,5},{8,6},{9,7},{10,... | collective-permute-start | bytes 786440 | tf_op jit(solution)/shard_map/ppermute | solution.py:298
  90.6 8.8 %collective-permute-start.5 = (bf16[256,256]{1,0:T(8,128)(2,1)S(1)}, bf16[256,256]{1,0:T(8,128)(2,1)S(1)}, u32[]{:S(2)}, u32[]{:S(2)}) collective-permute-start(bf16[256,256]{1,0:T(8,128)(2,1)S(1)} %slice.13), channel_id=1, source_target_pairs={{0,2},{1,3},{2,4},{3,5},{4,6},{5,7},{6,8},{7,9},{8,10},{9,11},{10,... | collective-permute-start | bytes 393224 | tf_op jit(solution)/shard_map/ppermute | solution.py:298
  92.5 6.8 %collective-permute-start.9 = (bf16[256,256]{1,0:T(8,128)(2,1)S(1)}, bf16[256,256]{1,0:T(8,128)(2,1)S(1)}, u32[]{:S(2)}, u32[]{:S(2)}) collective-permute-start(bf16[256,256]{1,0:T(8,128)(2,1)S(1)} %slice.14), channel_id=1, source_target_pairs={{0,14},{1,15},{2,0},{3,1},{4,2},{5,3},{6,4},{7,5},{8,6},{9,7},{10,... | collective-permute-start | bytes 393224 | tf_op jit(solution)/shard_map/ppermute | solution.py:298
  98.6 2.0 %copy-start.1 = (bf16[6784,256]{1,0:T(8,128)(2,1)S(1)}, bf16[6784,256]{1,0:T(8,128)(2,1)}, u32[]{:S(2)}) copy-start(bf16[6784,256]{1,0:T(8,128)(2,1)} %get-tuple-element.36.own_ref) | copy-start | bytes 10420228
  101.5 5.8 %collective-permute-start.14 = (bf16[256,256]{1,0:T(8,128)(2,1)S(1)}, bf16[256,256]{1,0:T(8,128)(2,1)S(1)}, u32[]{:S(2)}, u32[]{:S(2)}) collective-permute-start(bf16[256,256]{1,0:T(8,128)(2,1)S(1)} %get-tuple-element.56), channel_id=1, source_target_pairs={{0,14},{1,15},{2,0},{3,1},{4,2},{5,3},{6,4},{7,5},{8,6},{9,7},{10,... | collective-permute-start | bytes 393224 | tf_op jit(solution)/shard_map/ppermute | solution.py:298
  105.0 7.0 %collective-permute-start.10 = (bf16[256,256]{1,0:T(8,128)(2,1)S(1)}, bf16[256,256]{1,0:T(8,128)(2,1)S(1)}, u32[]{:S(2)}, u32[]{:S(2)}) collective-permute-start(bf16[256,256]{1,0:T(8,128)(2,1)S(1)} %get-tuple-element.52), channel_id=1, source_target_pairs={{0,2},{1,3},{2,4},{3,5},{4,6},{5,7},{6,8},{7,9},{8,10},{9,11},{10,... | collective-permute-start | bytes 393224 | tf_op jit(solution)/shard_map/ppermute | solution.py:298
  107.4 9.3 %collective-permute-start.15 = (bf16[512,256]{1,0:T(8,128)(2,1)S(1)}, bf16[512,256]{1,0:T(8,128)(2,1)S(1)}, u32[]{:S(2)}, u32[]{:S(2)}) collective-permute-start(bf16[512,256]{1,0:T(8,128)(2,1)S(1)} %shard_map.124), channel_id=1, source_target_pairs={{0,14},{1,15},{2,0},{3,1},{4,2},{5,3},{6,4},{7,5},{8,6},{9,7},{10,... | collective-permute-start | bytes 786440 | tf_op jit(solution)/shard_map/ppermute | solution.py:298
  112.1 9.7 %collective-permute-start.11 = (bf16[512,256]{1,0:T(8,128)(2,1)S(1)}, bf16[512,256]{1,0:T(8,128)(2,1)S(1)}, u32[]{:S(2)}, u32[]{:S(2)}) collective-permute-start(bf16[512,256]{1,0:T(8,128)(2,1)S(1)} %shard_map.121), channel_id=1, source_target_pairs={{0,2},{1,3},{2,4},{3,5},{4,6},{5,7},{6,8},{7,9},{8,10},{9,11},{10,... | collective-permute-start | bytes 786440 | tf_op jit(solution)/shard_map/ppermute | solution.py:298
  116.8 10.7 %collective-permute-start.16 = (bf16[512,256]{1,0:T(8,128)(2,1)S(1)}, bf16[512,256]{1,0:T(8,128)(2,1)S(1)}, u32[]{:S(2)}, u32[]{:S(2)}) collective-permute-start(bf16[512,256]{1,0:T(8,128)(2,1)S(1)} %shard_map.125), channel_id=1, source_target_pairs={{0,14},{1,15},{2,0},{3,1},{4,2},{5,3},{6,4},{7,5},{8,6},{9,7},{10,... | collective-permute-start | bytes 786440 | tf_op jit(solution)/shard_map/ppermute | solution.py:298
  121.9 11.0 %collective-permute-start.12 = (bf16[512,256]{1,0:T(8,128)(2,1)S(1)}, bf16[512,256]{1,0:T(8,128)(2,1)S(1)}, u32[]{:S(2)}, u32[]{:S(2)}) collective-permute-start(bf16[512,256]{1,0:T(8,128)(2,1)S(1)} %shard_map.122), channel_id=1, source_target_pairs={{0,2},{1,3},{2,4},{3,5},{4,6},{5,7},{6,8},{7,9},{8,10},{9,11},{10,... | collective-permute-start | bytes 786440 | tf_op jit(solution)/shard_map/ppermute | solution.py:298
  127.5 10.1 %collective-permute-start.17 = (bf16[512,256]{1,0:T(8,128)(2,1)S(1)}, bf16[512,256]{1,0:T(8,128)(2,1)S(1)}, u32[]{:S(2)}, u32[]{:S(2)}) collective-permute-start(bf16[512,256]{1,0:T(8,128)(2,1)S(1)} %shard_map.126), channel_id=1, source_target_pairs={{0,14},{1,15},{2,0},{3,1},{4,2},{5,3},{6,4},{7,5},{8,6},{9,7},{10,... | collective-permute-start | bytes 786440 | tf_op jit(solution)/shard_map/ppermute | solution.py:298
  132.9 16.8 %copy-start.7 = (f32[256,2]{0,1:T(2,128)S(1)}, f32[256,2]{0,1:T(2,128)}, u32[]{:S(2)}) copy-start(f32[256,2]{0,1:T(2,128)} %param.18) | copy-start | bytes 6148
  132.9 9.8 %collective-permute-start.13 = (bf16[512,256]{1,0:T(8,128)(2,1)S(1)}, bf16[512,256]{1,0:T(8,128)(2,1)S(1)}, u32[]{:S(2)}, u32[]{:S(2)}) collective-permute-start(bf16[512,256]{1,0:T(8,128)(2,1)S(1)} %shard_map.123), channel_id=1, source_target_pairs={{0,2},{1,3},{2,4},{3,5},{4,6},{5,7},{6,8},{7,9},{8,10},{9,11},{10,... | collective-permute-start | bytes 786440 | tf_op jit(solution)/shard_map/ppermute | solution.py:298
  143.5 16.4 %all-to-all-start.1 = ((bf16[32,16,256]{2,1,0:T(8,128)(2,1)}), bf16[32,16,256]{2,1,0:T(8,128)(2,1)S(1)}, u32[]{:S(2)}, u32[]{:S(2)}) async-start(bf16[32,16,256]{2,1,0:T(8,128)(2,1)} %bitcast.10), calls=%async_computation.1 | async-start | bytes 524288 | tf_op jit(solution)/shard_map/all_to_all | solution.py:401
  160.7 14.6 %collective-permute-start.18 = (f32[256,128]{1,0:T(8,128)S(1)}, f32[256,128]{1,0:T(8,128)S(1)}, u32[]{:S(2)}, u32[]{:S(2)}) collective-permute-start(f32[256,128]{1,0:T(8,128)S(1)} %get-tuple-element.58), channel_id=1, source_target_pairs={{0,1},{1,0},{2,3},{3,2},{4,5},{5,4},{6,7},{7,6},{8,9},{9,8},{10,11... | collective-permute-start | bytes 393224 | tf_op jit(solution)/shard_map/ppermute | solution.py:301
  (4 other events, 2.9 us)
where the time goes:
time: 177 us; the launch traced here: 176 us
  starting transfers between devices  81.7 us (46%)
  blocking collectives  42.5 us (24%)
  waiting for transfers between devices  29.9 us (17%)
  Pallas kernels  12.9 us (7%)
  local copies, waits for them, and re-layouts  8.54 us (5%)
    ppermute x16, starting transfers between devices, along(): return lax.ppermute(value, 'tp', pairs)  52 us
    all_to_all x1, blocking collectives, on_device(): lax.all_to_all(sent.reshape(experts, half, width), 'sp', split_axis=0, co...  25.9 us
    ppermute x2, starting transfers between devices, across(): return lax.ppermute(value, 'tp', [(t, t ^ 1) for t in range(members)])  22.4 us
    ppermute x16, waiting for transfers between devices, along(): return lax.ppermute(value, 'tp', pairs)  18.1 us
    all_gather x1, blocking collectives, on_device(): mixed = lax.all_gather(pooled, 'tp', axis=0, tiled=False)  16.6 us
    pallas_call x21, Pallas kernels, call(): pl.pallas_call(kernel, out_shape=out_shape, in_specs=[pl.BlockSpec(memory...  12.9 us
    all_to_all x1, waiting for transfers between devices, on_device(): lax.all_to_all(result.reshape(blocks, half, width), 'sp', split_axis=0, c...  10.1 us
    unnamed x19, local copies, waits for them, and re-layouts  7.83 us
  transfers between devices with their start and end apart: 20, of which 10 were waited for; matrix products, arithmetic and copies ran while one was open for 1% of the time, Pallas kernels for 3%

commit v1 on v0

--- a/solution.py
+++ b/solution.py
@@ -44,20 +44,21 @@
 
 
 def pool_kernel(before_ref, x_ref, w_ref, gain_ref, norm_ref, out_ref):
-    rows, width = x_ref.shape
+    width, rows = x_ref.shape
     window = lax.shift_left(jnp.int32(2), lax.rem(lax.axis_index("tp"), 4))
-    place = iota((rows, rows), 0) - iota((rows, rows), 1)
+    place = iota((rows, rows), 1) - iota((rows, rows), 0)
     inside = jnp.where((place >= 0) & (place < window), 1.0, 0.0).astype(BF16)
-    gap = iota((rows, REACH), 0) + REACH - iota((rows, REACH), 1)
+    reach = before_ref.shape[1]
+    gap = iota((reach, rows), 1) + reach - iota((reach, rows), 0)
     behind = jnp.where(gap < window, 1.0, 0.0).astype(BF16)
     x = x_ref[...]
-    total = mm(inside, x) + mm(behind, before_ref[...])
-    spot = lax.axis_index("sp") * rows + iota((rows, 1), 0)
+    total = mm(x, inside) + mm(before_ref[...], behind)
+    spot = lax.axis_index("sp") * rows + iota((1, rows), 1)
     count = jnp.minimum(spot + 1, window).astype(F32)
     pooled = (total / count - x.astype(F32)).astype(BF16)
-    mixed = (mm(pooled, w_ref[...]) * gain_ref[...].astype(F32)).astype(BF16)
-    eye = jnp.where(iota((width, width), 0) == iota((width, width), 1), 1.0, 0.0).astype(BF16)
-    out_ref[:width, :] = mm(eye, mixed, 1, 1).astype(BF16)
+    eye = iota((width, width), 0) == iota((width, width), 1)
+    gain = jnp.sum(jnp.where(eye, gain_ref[...].astype(F32), 0.0), axis=1, keepdims=True)
+    out_ref[:width, :] = (mm(w_ref[...], pooled, 0, 0) * gain).astype(BF16)
     features = norm_ref.shape[1]
     tail = out_ref.shape[0] - width
     out_ref[width:, :features] = jnp.broadcast_to(norm_ref[...].astype(F32), (tail, features)).astype(BF16)
@@ -208,39 +209,28 @@
 
 
 def last_kernel(
-    pack, chips, total, p_ref, m_ref, gain_ref, own_ref, other_ref, acc_in, square_in,
-    acc_ref, square_ref, hidden_ref, up_ref, low_ref,
+    pack, chips, total, p_ref, gain_ref, own_ref, other_ref, acc_in, square_in, acc_ref, square_ref, hidden_ref, out_ref
 ):
-    x = jnp.concatenate([p_ref[...], m_ref[...]], axis=0)
     packs = (own_ref, other_ref)
     far = chip_at(chips, chips // 2)
-    add_chunk(pack, x, far, gain_ref, packs, acc_ref, square_ref)
+    add_chunk(pack, p_ref[...], far, gain_ref, packs, acc_ref, square_ref)
     mean = jnp.sum(square_ref[...], axis=1, keepdims=True) / total
     scale = lax.rsqrt(mean + NORM_EPS)
     units = hidden_ref.shape[1]
     gate = jnp.minimum(acc_ref[:, :units] * scale, GATE_LIMIT)
     up = jnp.clip(acc_ref[:, units:] * scale, -GATE_LIMIT, GATE_LIMIT)
     hidden_ref[...] = ((up + 1.0) * gate * jax.nn.sigmoid(GATE_ALPHA * gate)).astype(BF16)
-    out = partial(pack, hidden_ref, packs, far).astype(BF16)
-    half = up_ref.shape[0]
-    up_ref[...] = out[:half]
-    low_ref[...] = out[half:]
+    out_ref[...] = partial(pack, hidden_ref, packs, far).astype(BF16)
 
 
 def down_kernel(pack, chips, steps, hidden_ref, own_ref, other_ref, *outs):
     for step, out_ref in zip(steps, outs):
-        out_ref[...] = partial(pack, hidden_ref, (own_ref, other_ref), chip_at(chips, step))
-
-
-def add_kernel(low, part_ref, came_ref, out_ref):
-    rows, held = part_ref.shape[0], came_ref.shape[0]
-    if held == rows:
-        out_ref[...] = (part_ref[...] + came_ref[...].astype(F32)).astype(BF16)
-        return
-    near = slice(rows - held, rows) if low else slice(0, held)
-    rest = slice(0, rows - held) if low else slice(held, rows)
-    out_ref[near, :] = (part_ref[near, :] + came_ref[...].astype(F32)).astype(BF16)
-    out_ref[rest, :] = part_ref[rest, :].astype(BF16)
+        value = partial(pack, hidden_ref, (own_ref, other_ref), chip_at(chips, step))
+        out_ref[...] = value.astype(out_ref.dtype)
+
+
+def add_kernel(part_ref, came_ref, out_ref):
+    out_ref[...] = (part_ref[...] + came_ref[...].astype(F32)).astype(BF16)
 
 
 def own_kernel(part_ref, p_ref, m_ref, out_ref):
@@ -304,15 +294,18 @@
     deep, units = expert_gate.shape[1:]
     pack = Pack(deep, width, out_weight.shape[0], tok_rows)
     before = lax.ppermute(
-        pool_input[tok_rows - REACH :], "sp", [(s, s + 1) for s in range(blocks - 1)]
-    )
-    small = (pool_input, pool_weight[0], pool_gain.reshape(1, channels), norm_gain.reshape(1, features))
+        pool_input.T[:, tok_rows - REACH * 8 :], "sp", [(s, s + 1) for s in range(blocks - 1)]
+    )
+    small = (pool_input.T, pool_weight[0], pool_gain.reshape(1, channels), norm_gain.reshape(1, features))
     own, *small = call(
         functools.partial(prep_kernel, pack),
-        (shape((pack.rows, width), BF16), *(shape(v.shape, v.dtype) for v in small)),
-        (expert_gate[0], expert_up[0], expert_down[0], out_weight, resid, *small),
+        (pltpu.VMEM((pack.rows, width), BF16), *(pltpu.VMEM(v.shape, v.dtype) for v in small)),
+        tuple(
+            pltpu.with_memory_space_constraint(v, pltpu.HBM)
+            for v in (expert_gate[0], expert_up[0], expert_down[0], out_weight, resid, *small)
+        ),
         pack.rows * width * 512,
-        58,
+        8,
         space=pltpu.HBM,
         scratch=[pltpu.SemaphoreType.DMA((10 + chips,))],
     )
@@ -347,7 +340,6 @@
         functools.partial(first_kernel, pack, chips), acc_shape, (x, gains, *packs), chunk_flops, 16
     )
     ahead, back = x, x
-    middle = held // 2
     last = chips // 2
     for step in range(1, last):
         ahead = along(ahead, 1)
@@ -360,43 +352,36 @@
             16,
             {5: 0, 6: 1},
         )
-    ahead = along(ahead[:middle], 1)
-    back = along(back[middle:], -1)
-    _, _, hidden, ahead, back = call(
+    ahead = along(ahead, 1)
+    _, _, hidden, ahead = call(
         functools.partial(last_kernel, pack, chips, float(total)),
-        (
-            *acc_shape,
-            shape((held, CORES * units), BF16),
-            shape((middle, width), BF16),
-            shape((middle, width), BF16),
-        ),
-        (ahead, back, gains, *packs, acc, square),
+        (*acc_shape, shape((held, CORES * units), BF16), shape((held, width), BF16)),
+        (ahead, gains, *packs, acc, square),
         2 * chunk_flops,
         24,
-        {5: 0, 6: 1},
-    )
+        {4: 0, 5: 1},
+    )
+
+    def joined(part, came):
+        return call(add_kernel, shape((held, width), BF16), (part, came), held * width, 8)
+
     for step in range(last - 1, -1, -1):
+        ahead = along(ahead, 1)
         steps = (step, -step) if step else (0,)
+        kinds = (F32, BF16 if step == last - 1 else F32)[: len(steps)]
         parts = call(
             functools.partial(down_kernel, pack, chips, steps),
-            (shape((held, width), F32),) * len(steps),
+            tuple(shape((held, width), kind) for kind in kinds),
             (hidden, *packs),
             chunk_flops // 2 * len(steps),
             16,
         )
-        ahead = along(ahead, 1)
-        back = along(back, -1)
-        if step:
-            ahead, back = (
-                call(
-                    functools.partial(add_kernel, low),
-                    shape((held, width), BF16),
-                    (part, came),
-                    held * width,
-                    8,
-                )
-                for low, (part, came) in enumerate(zip(parts, (ahead, back)))
-            )
+        if step == last - 1:
+            back = parts[1]
+        else:
+            back = along(back, -1)
+            back = joined(parts[1], back) if step else back
+        ahead = joined(parts[0], ahead) if step else ahead
     result = call(own_kernel, shape((held, width), BF16), (*parts, ahead, back), held * width, 8)
     returned = lax.all_to_all(
         result.reshape(blocks, half, width), "sp", split_axis=0, concat_axis=0, tiled=True

time: 177 us -> 164 us (0.927)
  starting transfers between devices: 81.7 us -> 71.1 us
  local copies, waits for them, and re-layouts: 8.54 us -> 0.28 us
  waiting for transfers between devices: 29.9 us -> 37.7 us
  Pallas kernels: 12.9 us -> 11 us
    ppermute x16 -> x14, starting transfers between devices: 52 us -> 43 us  [along(): return lax.ppermute(value, 'tp', pairs)]
    ppermute x16 -> x14, waiting for transfers between devices: 18.1 us -> 25.8 us  [along(): return lax.ppermute(value, 'tp', pairs)]
    unnamed x19 -> x8, local copies, waits for them, and re-layouts: 7.83 us -> 0.28 us
    all_to_all x1, starting transfers between devices: 6.01 us -> 3.97 us  [on_device(): lax.all_to_all(result.reshape(blocks, half, width), 'sp', split_axis=0, c...]
    pallas_call x21 -> x20, Pallas kernels: 12.9 us -> 11 us  [call(): pl.pallas_call(kernel, out_shape=out_shape, in_specs=[pl.BlockSpec(memory...]
  transfers between devices with their start and end apart: 20 -> 18, of which waited for: 10 -> 11; matrix products, arithmetic and copies ran while one was open for 1% -> 0% of each run, Pallas kernels for 3% -> 3%
where the time goes in v1:
time: 164 us; the launch traced here: 163 us
  starting transfers between devices  71.1 us (43%)
  blocking collectives  42.5 us (26%)
  waiting for transfers between devices  37.7 us (23%)
  Pallas kernels  11 us (7%)
    ppermute x14, starting transfers between devices, along(): return lax.ppermute(value, 'tp', pairs)  43 us
    all_to_all x1, blocking collectives, on_device(): lax.all_to_all(sent.reshape(experts, half, width), 'sp', split_axis=0, co...  25.9 us
    ppermute x14, waiting for transfers between devices, along(): return lax.ppermute(value, 'tp', pairs)  25.8 us
    ppermute x2, starting transfers between devices, across(): return lax.ppermute(value, 'tp', [(t, t ^ 1) for t in range(members)])  22.8 us
    all_gather x1, blocking collectives, on_device(): mixed = lax.all_gather(pooled, 'tp', axis=0, tiled=False)  16.6 us
    pallas_call x20, Pallas kernels, call(): pl.pallas_call(kernel, out_shape=out_shape, in_specs=[pl.BlockSpec(memory...  11 us
    all_to_all x1, waiting for transfers between devices, on_device(): lax.all_to_all(result.reshape(blocks, half, width), 'sp', split_axis=0, c...  10.1 us
    all_to_all x1, starting transfers between devices, on_device(): lax.all_to_all(result.reshape(blocks, half, width), 'sp', split_axis=0, c...  3.97 us
  transfers between devices with their start and end apart: 18, of which 11 were waited for; matrix products, arithmetic and copies ran while one was open for 0% of the time, Pallas kernels for 3%

profile of v1, /device:TPU:1, one launch (start us, length us, event | category | flops | bytes accessed | tf_op | source)
XLA Modules:
  0.0 162.9 jit_solution(4978881675633786249)
XLA Ops:
  0.0 2.2 %shard_map.109 = (bf16[6784,256]{1,0:T(8,128)(2,1)S(1)}, bf16[64,256]{1,0:T(8,128)(2,1)S(1)}, bf16[64,64]{1,0:T(8,128)(2,1)S(1)}, bf16[1,64]{1,0:T(2,128)(2,1)S(1)}, bf16[1,128]{1,0:T(2,128)(2,1)S(1)}) custom-call(bf16[2048,256]{1,0:T(8,128)(2,1)} %bitcast.20, bf16[2048,256]{1,0:T(8,128)(2,1)} %bitcast.21, bf16[256,2048]{1,0:T(8,128)(2,1)} %bitcast.22, ...), custom_call_target="tpu_custom_call" | custom-call | flops 889192448 | bytes 1736704 | tf_op jit(solution)/shard_map/pallas_call | solution.py:34
  2.2 8.7 %collective-permute-start.1 = (bf16[6784,256]{1,0:T(8,128)(2,1)S(1)}, bf16[6784,256]{1,0:T(8,128)(2,1)S(1)}, u32[]{:S(2)}, u32[]{:S(2)}) collective-permute-start(bf16[6784,256]{1,0:T(8,128)(2,1)S(1)} %get-tuple-element.35.own_ref), channel_id=1, source_target_pairs={{0,1},{1,0},{2,3},{3,2},{4,5},{5,4},{6,7},{7,6},{8,9},{9,8},{10,11... | collective-permute-start | bytes 10420232 | tf_op jit(solution)/shard_map/ppermute | solution.py:291
  13.5 16.6 %all-gather = bf16[1280,256]{1,0:T(8,128)(2,1)S(1)} all-gather(bf16[80,256]{1,0:T(8,128)(2,1)S(1)} %shard_map.110), channel_id=2, replica_groups=mesh['sp'=32,'tp'=16] {'tp'}, dimensions={0}, use_global_device_ids=true | all-gather | bytes 696320 | tf_op jit(solution)/shard_map/all_gather | solution.py:321
  30.9 25.9 %all_to_all.10 = bf16[32,16,256]{2,1,0:T(8,128)(2,1)S(1)} all-to-all(bf16[32,16,256]{2,1,0:T(8,128)(2,1)S(1)} %bitcast.18), channel_id=1, replica_groups=mesh['sp'=32,'tp'=16] {'sp'}, dimensions={0} | all-to-all | bytes 524288 | tf_op jit(solution)/shard_map/all_to_all | solution.py:333
  56.8 1.9 %collective-permute-start.2 = (bf16[512,256]{1,0:T(8,128)(2,1)S(1)}, bf16[512,256]{1,0:T(8,128)(2,1)S(1)}, u32[]{:S(2)}, u32[]{:S(2)}) collective-permute-start(bf16[512,256]{1,0:T(8,128)(2,1)S(1)} %bitcast.14), channel_id=1, source_target_pairs={{0,2},{1,3},{2,4},{3,5},{4,6},{5,7},{6,8},{7,9},{8,10},{9,11},{10,... | collective-permute-start | bytes 786440 | tf_op jit(solution)/shard_map/ppermute | solution.py:288
  58.7 4.6 %collective-permute-start.6 = (bf16[512,256]{1,0:T(8,128)(2,1)S(1)}, bf16[512,256]{1,0:T(8,128)(2,1)S(1)}, u32[]{:S(2)}, u32[]{:S(2)}) collective-permute-start(bf16[512,256]{1,0:T(8,128)(2,1)S(1)} %bitcast.15), channel_id=1, source_target_pairs={{0,14},{1,15},{2,0},{3,1},{4,2},{5,3},{6,4},{7,5},{8,6},{9,7},{10,... | collective-permute-start | bytes 786440 | tf_op jit(solution)/shard_map/ppermute | solution.py:288
  65.1 1.9 %collective-permute-start.3 = (bf16[512,256]{1,0:T(8,128)(2,1)S(1)}, bf16[512,256]{1,0:T(8,128)(2,1)S(1)}, u32[]{:S(2)}, u32[]{:S(2)}) collective-permute-start(bf16[512,256]{1,0:T(8,128)(2,1)S(1)} %collective-permute-done.2.p_ref), channel_id=1, source_target_pairs={{0,2},{1,3},{2,4},{3,5},{4,6},{5,7},{6,8},{7,9},{8,10},{9,11},{10,... | collective-permute-start | bytes 786440 | tf_op jit(solution)/shard_map/ppermute | solution.py:288
  67.0 4.6 %collective-permute-start.7 = (bf16[512,256]{1,0:T(8,128)(2,1)S(1)}, bf16[512,256]{1,0:T(8,128)(2,1)S(1)}, u32[]{:S(2)}, u32[]{:S(2)}) collective-permute-start(bf16[512,256]{1,0:T(8,128)(2,1)S(1)} %collective-permute-done.6.m_ref), channel_id=1, source_target_pairs={{0,14},{1,15},{2,0},{3,1},{4,2},{5,3},{6,4},{7,5},{8,6},{9,7},{10,... | collective-permute-start | bytes 786440 | tf_op jit(solution)/shard_map/ppermute | solution.py:288
  73.4 1.9 %collective-permute-start.4 = (bf16[512,256]{1,0:T(8,128)(2,1)S(1)}, bf16[512,256]{1,0:T(8,128)(2,1)S(1)}, u32[]{:S(2)}, u32[]{:S(2)}) collective-permute-start(bf16[512,256]{1,0:T(8,128)(2,1)S(1)} %collective-permute-done.3.p_ref), channel_id=1, source_target_pairs={{0,2},{1,3},{2,4},{3,5},{4,6},{5,7},{6,8},{7,9},{8,10},{9,11},{10,... | collective-permute-start | bytes 786440 | tf_op jit(solution)/shard_map/ppermute | solution.py:288
  75.4 4.6 %collective-permute-start.8 = (bf16[512,256]{1,0:T(8,128)(2,1)S(1)}, bf16[512,256]{1,0:T(8,128)(2,1)S(1)}, u32[]{:S(2)}, u32[]{:S(2)}) collective-permute-start(bf16[512,256]{1,0:T(8,128)(2,1)S(1)} %collective-permute-done.7.m_ref), channel_id=1, source_target_pairs={{0,14},{1,15},{2,0},{3,1},{4,2},{5,3},{6,4},{7,5},{8,6},{9,7},{10,... | collective-permute-start | bytes 786440 | tf_op jit(solution)/shard_map/ppermute | solution.py:288
  86.4 3.7 %collective-permute-done.5.p_ref = bf16[512,256]{1,0:T(8,128)(2,1)S(1)} collective-permute-done((bf16[512,256]{1,0:T(8,128)(2,1)S(1)}, bf16[512,256]{1,0:T(8,128)(2,1)S(1)}, u32[]{:S(2)}, u32[]{:S(2)}) %collective-permute-start.5) | collective-permute-done | bytes 262176 | tf_op jit(solution)/shard_map/ppermute | solution.py:288
  91.0 1.9 %collective-permute-start.9 = (bf16[512,256]{1,0:T(8,128)(2,1)S(1)}, bf16[512,256]{1,0:T(8,128)(2,1)S(1)}, u32[]{:S(2)}, u32[]{:S(2)}) collective-permute-start(bf16[512,256]{1,0:T(8,128)(2,1)S(1)} %get-tuple-element.51), channel_id=1, source_target_pairs={{0,2},{1,3},{2,4},{3,5},{4,6},{5,7},{6,8},{7,9},{8,10},{9,11},{10,... | collective-permute-start | bytes 786440 | tf_op jit(solution)/shard_map/ppermute | solution.py:288
  93.4 4.6 %collective-permute-start.13 = (bf16[512,256]{1,0:T(8,128)(2,1)S(1)}, bf16[512,256]{1,0:T(8,128)(2,1)S(1)}, u32[]{:S(2)}, u32[]{:S(2)}) collective-permute-start(bf16[512,256]{1,0:T(8,128)(2,1)S(1)} %get-tuple-element.54), channel_id=1, source_target_pairs={{0,14},{1,15},{2,0},{3,1},{4,2},{5,3},{6,4},{7,5},{8,6},{9,7},{10,... | collective-permute-start | bytes 786440 | tf_op jit(solution)/shard_map/ppermute | solution.py:288
  99.4 1.9 %collective-permute-start.10 = (bf16[512,256]{1,0:T(8,128)(2,1)S(1)}, bf16[512,256]{1,0:T(8,128)(2,1)S(1)}, u32[]{:S(2)}, u32[]{:S(2)}) collective-permute-start(bf16[512,256]{1,0:T(8,128)(2,1)S(1)} %shard_map.121), channel_id=1, source_target_pairs={{0,2},{1,3},{2,4},{3,5},{4,6},{5,7},{6,8},{7,9},{8,10},{9,11},{10,... | collective-permute-start | bytes 786440 | tf_op jit(solution)/shard_map/ppermute | solution.py:288
  101.8 4.6 %collective-permute-start.14 = (bf16[512,256]{1,0:T(8,128)(2,1)S(1)}, bf16[512,256]{1,0:T(8,128)(2,1)S(1)}, u32[]{:S(2)}, u32[]{:S(2)}) collective-permute-start(bf16[512,256]{1,0:T(8,128)(2,1)S(1)} %shard_map.124), channel_id=1, source_target_pairs={{0,14},{1,15},{2,0},{3,1},{4,2},{5,3},{6,4},{7,5},{8,6},{9,7},{10,... | collective-permute-start | bytes 786440 | tf_op jit(solution)/shard_map/ppermute | solution.py:288
  106.4 3.1 %collective-permute-done.10.came_ref = bf16[512,256]{1,0:T(8,128)(2,1)S(1)} collective-permute-done((bf16[512,256]{1,0:T(8,128)(2,1)S(1)}, bf16[512,256]{1,0:T(8,128)(2,1)S(1)}, u32[]{:S(2)}, u32[]{:S(2)}) %collective-permute-start.10) | collective-permute-done | bytes 262176 | tf_op jit(solution)/shard_map/ppermute | solution.py:288
  109.6 1.9 %collective-permute-start.11 = (bf16[512,256]{1,0:T(8,128)(2,1)S(1)}, bf16[512,256]{1,0:T(8,128)(2,1)S(1)}, u32[]{:S(2)}, u32[]{:S(2)}) collective-permute-start(bf16[512,256]{1,0:T(8,128)(2,1)S(1)} %shard_map.122), channel_id=1, source_target_pairs={{0,2},{1,3},{2,4},{3,5},{4,6},{5,7},{6,8},{7,9},{8,10},{9,11},{10,... | collective-permute-start | bytes 786440 | tf_op jit(solution)/shard_map/ppermute | solution.py:288
  112.1 4.8 %collective-permute-start.15 = (bf16[512,256]{1,0:T(8,128)(2,1)S(1)}, bf16[512,256]{1,0:T(8,128)(2,1)S(1)}, u32[]{:S(2)}, u32[]{:S(2)}) collective-permute-start(bf16[512,256]{1,0:T(8,128)(2,1)S(1)} %shard_map.125), channel_id=1, source_target_pairs={{0,14},{1,15},{2,0},{3,1},{4,2},{5,3},{6,4},{7,5},{8,6},{9,7},{10,... | collective-permute-start | bytes 786440 | tf_op jit(solution)/shard_map/ppermute | solution.py:288
  116.9 4.0 %collective-permute-done.11.came_ref = bf16[512,256]{1,0:T(8,128)(2,1)S(1)} collective-permute-done((bf16[512,256]{1,0:T(8,128)(2,1)S(1)}, bf16[512,256]{1,0:T(8,128)(2,1)S(1)}, u32[]{:S(2)}, u32[]{:S(2)}) %collective-permute-start.11) | collective-permute-done | bytes 262176 | tf_op jit(solution)/shard_map/ppermute | solution.py:288
  120.9 1.9 %collective-permute-start.12 = (bf16[512,256]{1,0:T(8,128)(2,1)S(1)}, bf16[512,256]{1,0:T(8,128)(2,1)S(1)}, u32[]{:S(2)}, u32[]{:S(2)}) collective-permute-start(bf16[512,256]{1,0:T(8,128)(2,1)S(1)} %shard_map.123), channel_id=1, source_target_pairs={{0,2},{1,3},{2,4},{3,5},{4,6},{5,7},{6,8},{7,9},{8,10},{9,11},{10,... | collective-permute-start | bytes 786440 | tf_op jit(solution)/shard_map/ppermute | solution.py:288
  123.2 8.2 %collective-permute-done.12.p_ref = bf16[512,256]{1,0:T(8,128)(2,1)S(1)} collective-permute-done((bf16[512,256]{1,0:T(8,128)(2,1)S(1)}, bf16[512,256]{1,0:T(8,128)(2,1)S(1)}, u32[]{:S(2)}, u32[]{:S(2)}) %collective-permute-start.12) | collective-permute-done | bytes 262176 | tf_op jit(solution)/shard_map/ppermute | solution.py:288
  132.1 4.0 %all-to-all-start.1 = ((bf16[32,16,256]{2,1,0:T(8,128)(2,1)}), bf16[32,16,256]{2,1,0:T(8,128)(2,1)S(1)}, u32[]{:S(2)}, u32[]{:S(2)}) async-start(bf16[32,16,256]{2,1,0:T(8,128)(2,1)} %bitcast.11), calls=%async_computation.1 | async-start | bytes 524288 | tf_op jit(solution)/shard_map/all_to_all | solution.py:386
  136.4 10.1 %all-to-all-done.1 = bf16[32,16,256]{2,1,0:T(8,128)(2,1)S(1)} async-done(((bf16[32,16,256]{2,1,0:T(8,128)(2,1)}), bf16[32,16,256]{2,1,0:T(8,128)(2,1)S(1)}, u32[]{:S(2)}, u32[]{:S(2)}) %all-to-all-start.1) | async-done | bytes 262176 | tf_op jit(solution)/shard_map/all_to_all | solution.py:386
  147.2 14.1 %collective-permute-start.16 = (f32[256,128]{1,0:T(8,128)S(1)}, f32[256,128]{1,0:T(8,128)S(1)}, u32[]{:S(2)}, u32[]{:S(2)}) collective-permute-start(f32[256,128]{1,0:T(8,128)S(1)} %get-tuple-element.56), channel_id=1, source_target_pairs={{0,1},{1,0},{2,3},{3,2},{4,5},{5,4},{6,7},{7,6},{8,9},{9,8},{10,11... | collective-permute-start | bytes 393224 | tf_op jit(solution)/shard_map/ppermute | solution.py:291
  (43 shorter events, 20.9 us)
Async XLA Ops:
  0.0 11.0 %copy-start.1 = (bf16[256,64]{0,1:T(8,128)(2,1)S(1)}, bf16[256,64]{0,1:T(8,128)(2,1)}, u32[]{:S(2)}) copy-start(bf16[256,64]{0,1:T(8,128)(2,1)} %param.11) | copy-start | bytes 98308
  0.0 30.1 %copy-start = (s32[256,2]{0,1:T(2,128)S(1)}, s32[256,2]{0,1:T(2,128)}, u32[]{:S(2)}) copy-start(s32[256,2]{0,1:T(2,128)} %param.17) | copy-start | bytes 6148
  2.2 27.8 %collective-permute-start.1 = (bf16[6784,256]{1,0:T(8,128)(2,1)S(1)}, bf16[6784,256]{1,0:T(8,128)(2,1)S(1)}, u32[]{:S(2)}, u32[]{:S(2)}) collective-permute-start(bf16[6784,256]{1,0:T(8,128)(2,1)S(1)} %get-tuple-element.35.own_ref), channel_id=1, source_target_pairs={{0,1},{1,0},{2,3},{3,2},{4,5},{5,4},{6,7},{7,6},{8,9},{9,8},{10,11... | collective-permute-start | bytes 10420232 | tf_op jit(solution)/shard_map/ppermute | solution.py:291
  11.0 2.1 %collective-permute-start = (bf16[64,128]{1,0:T(8,128)(2,1)S(1)}, bf16[64,128]{1,0:T(8,128)(2,1)S(1)}, u32[]{:S(2)}, u32[]{:S(2)}) collective-permute-start(bf16[64,128]{1,0:T(8,128)(2,1)S(1)} %slice.4), channel_id=1, source_target_pairs={{0,16},{16,32},{32,48},{48,64},{64,80},{80,96},{96,112},{112,128},... | collective-permute-start | bytes 49160 | tf_op jit(solution)/shard_map/ppermute | solution.py:296
  56.8 8.3 %collective-permute-start.2 = (bf16[512,256]{1,0:T(8,128)(2,1)S(1)}, bf16[512,256]{1,0:T(8,128)(2,1)S(1)}, u32[]{:S(2)}, u32[]{:S(2)}) collective-permute-start(bf16[512,256]{1,0:T(8,128)(2,1)S(1)} %bitcast.14), channel_id=1, source_target_pairs={{0,2},{1,3},{2,4},{3,5},{4,6},{5,7},{6,8},{7,9},{8,10},{9,11},{10,... | collective-permute-start | bytes 786440 | tf_op jit(solution)/shard_map/ppermute | solution.py:288
  58.7 8.3 %collective-permute-start.6 = (bf16[512,256]{1,0:T(8,128)(2,1)S(1)}, bf16[512,256]{1,0:T(8,128)(2,1)S(1)}, u32[]{:S(2)}, u32[]{:S(2)}) collective-permute-start(bf16[512,256]{1,0:T(8,128)(2,1)S(1)} %bitcast.15), channel_id=1, source_target_pairs={{0,14},{1,15},{2,0},{3,1},{4,2},{5,3},{6,4},{7,5},{8,6},{9,7},{10,... | collective-permute-start | bytes 786440 | tf_op jit(solution)/shard_map/ppermute | solution.py:288
  65.1 8.3 %collective-permute-start.3 = (bf16[512,256]{1,0:T(8,128)(2,1)S(1)}, bf16[512,256]{1,0:T(8,128)(2,1)S(1)}, u32[]{:S(2)}, u32[]{:S(2)}) collective-permute-start(bf16[512,256]{1,0:T(8,128)(2,1)S(1)} %collective-permute-done.2.p_ref), channel_id=1, source_target_pairs={{0,2},{1,3},{2,4},{3,5},{4,6},{5,7},{6,8},{7,9},{8,10},{9,11},{10,... | collective-permute-start | bytes 786440 | tf_op jit(solution)/shard_map/ppermute | solution.py:288
  67.0 8.3 %collective-permute-start.7 = (bf16[512,256]{1,0:T(8,128)(2,1)S(1)}, bf16[512,256]{1,0:T(8,128)(2,1)S(1)}, u32[]{:S(2)}, u32[]{:S(2)}) collective-permute-start(bf16[512,256]{1,0:T(8,128)(2,1)S(1)} %collective-permute-done.6.m_ref), channel_id=1, source_target_pairs={{0,14},{1,15},{2,0},{3,1},{4,2},{5,3},{6,4},{7,5},{8,6},{9,7},{10,... | collective-permute-start | bytes 786440 | tf_op jit(solution)/shard_map/ppermute | solution.py:288
  73.4 8.3 %collective-permute-start.4 = (bf16[512,256]{1,0:T(8,128)(2,1)S(1)}, bf16[512,256]{1,0:T(8,128)(2,1)S(1)}, u32[]{:S(2)}, u32[]{:S(2)}) collective-permute-start(bf16[512,256]{1,0:T(8,128)(2,1)S(1)} %collective-permute-done.3.p_ref), channel_id=1, source_target_pairs={{0,2},{1,3},{2,4},{3,5},{4,6},{5,7},{6,8},{7,9},{8,10},{9,11},{10,... | collective-permute-start | bytes 786440 | tf_op jit(solution)/shard_map/ppermute | solution.py:288
  75.4 10.2 %collective-permute-start.8 = (bf16[512,256]{1,0:T(8,128)(2,1)S(1)}, bf16[512,256]{1,0:T(8,128)(2,1)S(1)}, u32[]{:S(2)}, u32[]{:S(2)}) collective-permute-start(bf16[512,256]{1,0:T(8,128)(2,1)S(1)} %collective-permute-done.7.m_ref), channel_id=1, source_target_pairs={{0,14},{1,15},{2,0},{3,1},{4,2},{5,3},{6,4},{7,5},{8,6},{9,7},{10,... | collective-permute-start | bytes 786440 | tf_op jit(solution)/shard_map/ppermute | solution.py:288
  81.8 8.3 %collective-permute-start.5 = (bf16[512,256]{1,0:T(8,128)(2,1)S(1)}, bf16[512,256]{1,0:T(8,128)(2,1)S(1)}, u32[]{:S(2)}, u32[]{:S(2)}) collective-permute-start(bf16[512,256]{1,0:T(8,128)(2,1)S(1)} %collective-permute-done.4.p_ref), channel_id=1, source_target_pairs={{0,2},{1,3},{2,4},{3,5},{4,6},{5,7},{6,8},{7,9},{8,10},{9,11},{10,... | collective-permute-start | bytes 786440 | tf_op jit(solution)/shard_map/ppermute | solution.py:288
  91.0 8.3 %collective-permute-start.9 = (bf16[512,256]{1,0:T(8,128)(2,1)S(1)}, bf16[512,256]{1,0:T(8,128)(2,1)S(1)}, u32[]{:S(2)}, u32[]{:S(2)}) collective-permute-start(bf16[512,256]{1,0:T(8,128)(2,1)S(1)} %get-tuple-element.51), channel_id=1, source_target_pairs={{0,2},{1,3},{2,4},{3,5},{4,6},{5,7},{6,8},{7,9},{8,10},{9,11},{10,... | collective-permute-start | bytes 786440 | tf_op jit(solution)/shard_map/ppermute | solution.py:288
  93.4 8.4 %collective-permute-start.13 = (bf16[512,256]{1,0:T(8,128)(2,1)S(1)}, bf16[512,256]{1,0:T(8,128)(2,1)S(1)}, u32[]{:S(2)}, u32[]{:S(2)}) collective-permute-start(bf16[512,256]{1,0:T(8,128)(2,1)S(1)} %get-tuple-element.54), channel_id=1, source_target_pairs={{0,14},{1,15},{2,0},{3,1},{4,2},{5,3},{6,4},{7,5},{8,6},{9,7},{10,... | collective-permute-start | bytes 786440 | tf_op jit(solution)/shard_map/ppermute | solution.py:288
  99.4 10.2 %collective-permute-start.10 = (bf16[512,256]{1,0:T(8,128)(2,1)S(1)}, bf16[512,256]{1,0:T(8,128)(2,1)S(1)}, u32[]{:S(2)}, u32[]{:S(2)}) collective-permute-start(bf16[512,256]{1,0:T(8,128)(2,1)S(1)} %shard_map.121), channel_id=1, source_target_pairs={{0,2},{1,3},{2,4},{3,5},{4,6},{5,7},{6,8},{7,9},{8,10},{9,11},{10,... | collective-permute-start | bytes 786440 | tf_op jit(solution)/shard_map/ppermute | solution.py:288
  101.8 10.2 %collective-permute-start.14 = (bf16[512,256]{1,0:T(8,128)(2,1)S(1)}, bf16[512,256]{1,0:T(8,128)(2,1)S(1)}, u32[]{:S(2)}, u32[]{:S(2)}) collective-permute-start(bf16[512,256]{1,0:T(8,128)(2,1)S(1)} %shard_map.124), channel_id=1, source_target_pairs={{0,14},{1,15},{2,0},{3,1},{4,2},{5,3},{6,4},{7,5},{8,6},{9,7},{10,... | collective-permute-start | bytes 786440 | tf_op jit(solution)/shard_map/ppermute | solution.py:288
  109.6 11.2 %collective-permute-start.11 = (bf16[512,256]{1,0:T(8,128)(2,1)S(1)}, bf16[512,256]{1,0:T(8,128)(2,1)S(1)}, u32[]{:S(2)}, u32[]{:S(2)}) collective-permute-start(bf16[512,256]{1,0:T(8,128)(2,1)S(1)} %shard_map.122), channel_id=1, source_target_pairs={{0,2},{1,3},{2,4},{3,5},{4,6},{5,7},{6,8},{7,9},{8,10},{9,11},{10,... | collective-permute-start | bytes 786440 | tf_op jit(solution)/shard_map/ppermute | solution.py:288
  112.1 11.1 %collective-permute-start.15 = (bf16[512,256]{1,0:T(8,128)(2,1)S(1)}, bf16[512,256]{1,0:T(8,128)(2,1)S(1)}, u32[]{:S(2)}, u32[]{:S(2)}) collective-permute-start(bf16[512,256]{1,0:T(8,128)(2,1)S(1)} %shard_map.125), channel_id=1, source_target_pairs={{0,14},{1,15},{2,0},{3,1},{4,2},{5,3},{6,4},{7,5},{8,6},{9,7},{10,... | collective-permute-start | bytes 786440 | tf_op jit(solution)/shard_map/ppermute | solution.py:288
  120.9 15.3 %copy-start.2 = (f32[256,2]{0,1:T(2,128)S(1)}, f32[256,2]{0,1:T(2,128)}, u32[]{:S(2)}) copy-start(f32[256,2]{0,1:T(2,128)} %param.18) | copy-start | bytes 6148
  120.9 10.4 %collective-permute-start.12 = (bf16[512,256]{1,0:T(8,128)(2,1)S(1)}, bf16[512,256]{1,0:T(8,128)(2,1)S(1)}, u32[]{:S(2)}, u32[]{:S(2)}) collective-permute-start(bf16[512,256]{1,0:T(8,128)(2,1)S(1)} %shard_map.123), channel_id=1, source_target_pairs={{0,2},{1,3},{2,4},{3,5},{4,6},{5,7},{6,8},{7,9},{8,10},{9,11},{10,... | collective-permute-start | bytes 786440 | tf_op jit(solution)/shard_map/ppermute | solution.py:288
  132.1 14.4 %all-to-all-start.1 = ((bf16[32,16,256]{2,1,0:T(8,128)(2,1)}), bf16[32,16,256]{2,1,0:T(8,128)(2,1)S(1)}, u32[]{:S(2)}, u32[]{:S(2)}) async-start(bf16[32,16,256]{2,1,0:T(8,128)(2,1)} %bitcast.11), calls=%async_computation.1 | async-start | bytes 524288 | tf_op jit(solution)/shard_map/all_to_all | solution.py:386
  147.2 15.1 %collective-permute-start.16 = (f32[256,128]{1,0:T(8,128)S(1)}, f32[256,128]{1,0:T(8,128)S(1)}, u32[]{:S(2)}, u32[]{:S(2)}) collective-permute-start(f32[256,128]{1,0:T(8,128)S(1)} %get-tuple-element.56), channel_id=1, source_target_pairs={{0,1},{1,0},{2,3},{3,2},{4,5},{5,4},{6,7},{7,6},{8,9},{9,8},{10,11... | collective-permute-start | bytes 393224 | tf_op jit(solution)/shard_map/ppermute | solution.py:291

commit v2 on v1

--- a/solution.py
+++ b/solution.py
@@ -9,7 +9,6 @@
 
 
 GSIZE = 64
-REACH = 16
 TOPK = 2
 CORES = 2
 
@@ -209,7 +208,7 @@
 
 
 def last_kernel(
-    pack, chips, total, p_ref, gain_ref, own_ref, other_ref, acc_in, square_in, acc_ref, square_ref, hidden_ref, out_ref
+    pack, chips, total, p_ref, gain_ref, own_ref, other_ref, acc_in, square_in, acc_ref, square_ref, hidden_ref, up_ref, low_ref
 ):
     packs = (own_ref, other_ref)
     far = chip_at(chips, chips // 2)
@@ -220,13 +219,13 @@
     gate = jnp.minimum(acc_ref[:, :units] * scale, GATE_LIMIT)
     up = jnp.clip(acc_ref[:, units:] * scale, -GATE_LIMIT, GATE_LIMIT)
     hidden_ref[...] = ((up + 1.0) * gate * jax.nn.sigmoid(GATE_ALPHA * gate)).astype(BF16)
-    out_ref[...] = partial(pack, hidden_ref, packs, far).astype(BF16)
+    up_ref[...] = partial(pack, hidden_ref, packs, far).astype(BF16)
+    low_ref[...] = partial(pack, hidden_ref, packs, chip_at(chips, 1 - chips // 2)).astype(BF16)
 
 
 def down_kernel(pack, chips, steps, hidden_ref, own_ref, other_ref, *outs):
     for step, out_ref in zip(steps, outs):
-        value = partial(pack, hidden_ref, (own_ref, other_ref), chip_at(chips, step))
-        out_ref[...] = value.astype(out_ref.dtype)
+        out_ref[...] = partial(pack, hidden_ref, (own_ref, other_ref), chip_at(chips, step))
 
 
 def add_kernel(part_ref, came_ref, out_ref):
@@ -294,7 +293,7 @@
     deep, units = expert_gate.shape[1:]
     pack = Pack(deep, width, out_weight.shape[0], tok_rows)
     before = lax.ppermute(
-        pool_input.T[:, tok_rows - REACH * 8 :], "sp", [(s, s + 1) for s in range(blocks - 1)]
+        pool_input.T, "sp", [(s, s + 1) for s in range(blocks - 1)]
     )
     small = (pool_input.T, pool_weight[0], pool_gain.reshape(1, channels), norm_gain.reshape(1, features))
     own, *small = call(
@@ -353,9 +352,9 @@
             {5: 0, 6: 1},
         )
     ahead = along(ahead, 1)
-    _, _, hidden, ahead = call(
+    _, _, hidden, ahead, back = call(
         functools.partial(last_kernel, pack, chips, float(total)),
-        (*acc_shape, shape((held, CORES * units), BF16), shape((held, width), BF16)),
+        (*acc_shape, shape((held, CORES * units), BF16), *(shape((held, width), BF16),) * 2),
         (ahead, gains, *packs, acc, square),
         2 * chunk_flops,
         24,
@@ -365,24 +364,22 @@
     def joined(part, came):
         return call(add_kernel, shape((held, width), BF16), (part, came), held * width, 8)
 
+    steps = [*range(last - 1, -1, -1), *range(2 - last, 0)]
+    parts = call(
+        functools.partial(down_kernel, pack, chips, steps),
+        (shape((held, width), F32),) * len(steps),
+        (hidden, *packs),
+        chunk_flops // 2 * len(steps),
+        24,
+    )
+    part = dict(zip(steps, parts))
     for step in range(last - 1, -1, -1):
         ahead = along(ahead, 1)
-        steps = (step, -step) if step else (0,)
-        kinds = (F32, BF16 if step == last - 1 else F32)[: len(steps)]
-        parts = call(
-            functools.partial(down_kernel, pack, chips, steps),
-            tuple(shape((held, width), kind) for kind in kinds),
-            (hidden, *packs),
-            chunk_flops // 2 * len(steps),
-            16,
-        )
-        if step == last - 1:
-            back = parts[1]
-        else:
+        if step:
             back = along(back, -1)
-            back = joined(parts[1], back) if step else back
-        ahead = joined(parts[0], ahead) if step else ahead
-    result = call(own_kernel, shape((held, width), BF16), (*parts, ahead, back), held * width, 8)
+            ahead = joined(part[step], ahead)
+            back = joined(part[1 - step], back) if step > 1 else back
+    result = call(own_kernel, pltpu.VMEM((held, width), BF16), (part[0], ahead, back), held * width, 8)
     returned = lax.all_to_all(
         result.reshape(blocks, half, width), "sp", split_axis=0, concat_axis=0, tiled=True
     ).reshape(experts * half, width)

time: 164 us -> 164 us (level)
    pallas_call x20 -> x17, Pallas kernels: 11 us -> 10.4 us  [call(): pl.pallas_call(kernel, out_shape=out_shape, in_specs=[pl.BlockSpec(memory...]
where the time goes in v2:
time: 164 us; the launch traced here: 163 us
  starting transfers between devices  71.1 us (43%)
  blocking collectives  42.5 us (26%)
  waiting for transfers between devices  38.6 us (24%)
  Pallas kernels  10.4 us (6%)
    ppermute x14, starting transfers between devices, along(): return lax.ppermute(value, 'tp', pairs)  43 us
    ppermute x14, waiting for transfers between devices, along(): return lax.ppermute(value, 'tp', pairs)  26.5 us
    all_to_all x1, blocking collectives, on_device(): lax.all_to_all(sent.reshape(experts, half, width), 'sp', split_axis=0, co...  25.9 us
    ppermute x2, starting transfers between devices, across(): return lax.ppermute(value, 'tp', [(t, t ^ 1) for t in range(members)])  22.9 us
    all_gather x1, blocking collectives, on_device(): mixed = lax.all_gather(pooled, 'tp', axis=0, tiled=False)  16.6 us
    pallas_call x17, Pallas kernels, call(): pl.pallas_call(kernel, out_shape=out_shape, in_specs=[pl.BlockSpec(memory...  10.4 us
    all_to_all x1, waiting for transfers between devices, on_device(): lax.all_to_all(result.reshape(blocks, half, width), 'sp', split_axis=0, c...  10.1 us
    all_to_all x1, starting transfers between devices, on_device(): lax.all_to_all(result.reshape(blocks, half, width), 'sp', split_axis=0, c...  3.94 us
  transfers between devices with their start and end apart: 18, of which 11 were waited for; matrix products, arithmetic and copies ran while one was open for 0% of the time, Pallas kernels for 3%

profile of v2, /device:TPU:1, one launch (start us, length us, event | category | flops | bytes accessed | tf_op | source)
XLA Modules:
  0.0 163.1 jit_solution(15634892192183356543)
XLA Ops:
  0.0 2.2 %shard_map.109 = (bf16[6784,256]{1,0:T(8,128)(2,1)S(1)}, bf16[64,256]{1,0:T(8,128)(2,1)S(1)}, bf16[64,64]{1,0:T(8,128)(2,1)S(1)}, bf16[1,64]{1,0:T(2,128)(2,1)S(1)}, bf16[1,128]{1,0:T(2,128)(2,1)S(1)}) custom-call(bf16[2048,256]{1,0:T(8,128)(2,1)} %bitcast.20, bf16[2048,256]{1,0:T(8,128)(2,1)} %bitcast.21, bf16[256,2048]{1,0:T(8,128)(2,1)} %bitcast.22, ...), custom_call_target="tpu_custom_call" | custom-call | flops 889192448 | bytes 1736704 | tf_op jit(solution)/shard_map/pallas_call | solution.py:33
  2.2 8.7 %collective-permute-start.1 = (bf16[6784,256]{1,0:T(8,128)(2,1)S(1)}, bf16[6784,256]{1,0:T(8,128)(2,1)S(1)}, u32[]{:S(2)}, u32[]{:S(2)}) collective-permute-start(bf16[6784,256]{1,0:T(8,128)(2,1)S(1)} %get-tuple-element.36.own_ref), channel_id=1, source_target_pairs={{0,1},{1,0},{2,3},{3,2},{4,5},{5,4},{6,7},{7,6},{8,9},{9,8},{10,11... | collective-permute-start | bytes 10420232 | tf_op jit(solution)/shard_map/ppermute | solution.py:290
  13.6 16.6 %all-gather = bf16[1280,256]{1,0:T(8,128)(2,1)S(1)} all-gather(bf16[80,256]{1,0:T(8,128)(2,1)S(1)} %shard_map.110), channel_id=2, replica_groups=mesh['sp'=32,'tp'=16] {'tp'}, dimensions={0}, use_global_device_ids=true | all-gather | bytes 696320 | tf_op jit(solution)/shard_map/all_gather | solution.py:320
  31.0 25.9 %all_to_all.10 = bf16[32,16,256]{2,1,0:T(8,128)(2,1)S(1)} all-to-all(bf16[32,16,256]{2,1,0:T(8,128)(2,1)S(1)} %bitcast.18), channel_id=1, replica_groups=mesh['sp'=32,'tp'=16] {'sp'}, dimensions={0} | all-to-all | bytes 524288 | tf_op jit(solution)/shard_map/all_to_all | solution.py:332
  57.0 1.9 %collective-permute-start.2 = (bf16[512,256]{1,0:T(8,128)(2,1)S(1)}, bf16[512,256]{1,0:T(8,128)(2,1)S(1)}, u32[]{:S(2)}, u32[]{:S(2)}) collective-permute-start(bf16[512,256]{1,0:T(8,128)(2,1)S(1)} %bitcast.14), channel_id=1, source_target_pairs={{0,2},{1,3},{2,4},{3,5},{4,6},{5,7},{6,8},{7,9},{8,10},{9,11},{10,... | collective-permute-start | bytes 786440 | tf_op jit(solution)/shard_map/ppermute | solution.py:287
  58.9 4.6 %collective-permute-start.6 = (bf16[512,256]{1,0:T(8,128)(2,1)S(1)}, bf16[512,256]{1,0:T(8,128)(2,1)S(1)}, u32[]{:S(2)}, u32[]{:S(2)}) collective-permute-start(bf16[512,256]{1,0:T(8,128)(2,1)S(1)} %bitcast.15), channel_id=1, source_target_pairs={{0,14},{1,15},{2,0},{3,1},{4,2},{5,3},{6,4},{7,5},{8,6},{9,7},{10,... | collective-permute-start | bytes 786440 | tf_op jit(solution)/shard_map/ppermute | solution.py:287
  65.3 1.9 %collective-permute-start.3 = (bf16[512,256]{1,0:T(8,128)(2,1)S(1)}, bf16[512,256]{1,0:T(8,128)(2,1)S(1)}, u32[]{:S(2)}, u32[]{:S(2)}) collective-permute-start(bf16[512,256]{1,0:T(8,128)(2,1)S(1)} %collective-permute-done.2.p_ref), channel_id=1, source_target_pairs={{0,2},{1,3},{2,4},{3,5},{4,6},{5,7},{6,8},{7,9},{8,10},{9,11},{10,... | collective-permute-start | bytes 786440 | tf_op jit(solution)/shard_map/ppermute | solution.py:287
  67.2 4.6 %collective-permute-start.7 = (bf16[512,256]{1,0:T(8,128)(2,1)S(1)}, bf16[512,256]{1,0:T(8,128)(2,1)S(1)}, u32[]{:S(2)}, u32[]{:S(2)}) collective-permute-start(bf16[512,256]{1,0:T(8,128)(2,1)S(1)} %collective-permute-done.6.m_ref), channel_id=1, source_target_pairs={{0,14},{1,15},{2,0},{3,1},{4,2},{5,3},{6,4},{7,5},{8,6},{9,7},{10,... | collective-permute-start | bytes 786440 | tf_op jit(solution)/shard_map/ppermute | solution.py:287
  73.6 1.9 %collective-permute-start.4 = (bf16[512,256]{1,0:T(8,128)(2,1)S(1)}, bf16[512,256]{1,0:T(8,128)(2,1)S(1)}, u32[]{:S(2)}, u32[]{:S(2)}) collective-permute-start(bf16[512,256]{1,0:T(8,128)(2,1)S(1)} %collective-permute-done.3.p_ref), channel_id=1, source_target_pairs={{0,2},{1,3},{2,4},{3,5},{4,6},{5,7},{6,8},{7,9},{8,10},{9,11},{10,... | collective-permute-start | bytes 786440 | tf_op jit(solution)/shard_map/ppermute | solution.py:287
  75.5 4.6 %collective-permute-start.8 = (bf16[512,256]{1,0:T(8,128)(2,1)S(1)}, bf16[512,256]{1,0:T(8,128)(2,1)S(1)}, u32[]{:S(2)}, u32[]{:S(2)}) collective-permute-start(bf16[512,256]{1,0:T(8,128)(2,1)S(1)} %collective-permute-done.7.m_ref), channel_id=1, source_target_pairs={{0,14},{1,15},{2,0},{3,1},{4,2},{5,3},{6,4},{7,5},{8,6},{9,7},{10,... | collective-permute-start | bytes 786440 | tf_op jit(solution)/shard_map/ppermute | solution.py:287
  86.5 3.7 %collective-permute-done.5.p_ref = bf16[512,256]{1,0:T(8,128)(2,1)S(1)} collective-permute-done((bf16[512,256]{1,0:T(8,128)(2,1)S(1)}, bf16[512,256]{1,0:T(8,128)(2,1)S(1)}, u32[]{:S(2)}, u32[]{:S(2)}) %collective-permute-start.5) | collective-permute-done | bytes 262176 | tf_op jit(solution)/shard_map/ppermute | solution.py:287
  91.2 1.9 %collective-permute-start.9 = (bf16[512,256]{1,0:T(8,128)(2,1)S(1)}, bf16[512,256]{1,0:T(8,128)(2,1)S(1)}, u32[]{:S(2)}, u32[]{:S(2)}) collective-permute-start(bf16[512,256]{1,0:T(8,128)(2,1)S(1)} %get-tuple-element.53), channel_id=1, source_target_pairs={{0,2},{1,3},{2,4},{3,5},{4,6},{5,7},{6,8},{7,9},{8,10},{9,11},{10,... | collective-permute-start | bytes 786440 | tf_op jit(solution)/shard_map/ppermute | solution.py:287
  93.1 4.6 %collective-permute-start.13 = (bf16[512,256]{1,0:T(8,128)(2,1)S(1)}, bf16[512,256]{1,0:T(8,128)(2,1)S(1)}, u32[]{:S(2)}, u32[]{:S(2)}) collective-permute-start(bf16[512,256]{1,0:T(8,128)(2,1)S(1)} %get-tuple-element.56), channel_id=1, source_target_pairs={{0,14},{1,15},{2,0},{3,1},{4,2},{5,3},{6,4},{7,5},{8,6},{9,7},{10,... | collective-permute-start | bytes 786440 | tf_op jit(solution)/shard_map/ppermute | solution.py:287
  99.6 1.9 %collective-permute-start.10 = (bf16[512,256]{1,0:T(8,128)(2,1)S(1)}, bf16[512,256]{1,0:T(8,128)(2,1)S(1)}, u32[]{:S(2)}, u32[]{:S(2)}) collective-permute-start(bf16[512,256]{1,0:T(8,128)(2,1)S(1)} %shard_map.118), channel_id=1, source_target_pairs={{0,2},{1,3},{2,4},{3,5},{4,6},{5,7},{6,8},{7,9},{8,10},{9,11},{10,... | collective-permute-start | bytes 786440 | tf_op jit(solution)/shard_map/ppermute | solution.py:287
  101.6 4.6 %collective-permute-start.14 = (bf16[512,256]{1,0:T(8,128)(2,1)S(1)}, bf16[512,256]{1,0:T(8,128)(2,1)S(1)}, u32[]{:S(2)}, u32[]{:S(2)}) collective-permute-start(bf16[512,256]{1,0:T(8,128)(2,1)S(1)} %shard_map.121), channel_id=1, source_target_pairs={{0,14},{1,15},{2,0},{3,1},{4,2},{5,3},{6,4},{7,5},{8,6},{9,7},{10,... | collective-permute-start | bytes 786440 | tf_op jit(solution)/shard_map/ppermute | solution.py:287
  106.1 3.6 %collective-permute-done.10.came_ref = bf16[512,256]{1,0:T(8,128)(2,1)S(1)} collective-permute-done((bf16[512,256]{1,0:T(8,128)(2,1)S(1)}, bf16[512,256]{1,0:T(8,128)(2,1)S(1)}, u32[]{:S(2)}, u32[]{:S(2)}) %collective-permute-start.10) | collective-permute-done | bytes 262176 | tf_op jit(solution)/shard_map/ppermute | solution.py:287
  109.8 1.9 %collective-permute-start.11 = (bf16[512,256]{1,0:T(8,128)(2,1)S(1)}, bf16[512,256]{1,0:T(8,128)(2,1)S(1)}, u32[]{:S(2)}, u32[]{:S(2)}) collective-permute-start(bf16[512,256]{1,0:T(8,128)(2,1)S(1)} %shard_map.119), channel_id=1, source_target_pairs={{0,2},{1,3},{2,4},{3,5},{4,6},{5,7},{6,8},{7,9},{8,10},{9,11},{10,... | collective-permute-start | bytes 786440 | tf_op jit(solution)/shard_map/ppermute | solution.py:287
  111.8 4.8 %collective-permute-start.15 = (bf16[512,256]{1,0:T(8,128)(2,1)S(1)}, bf16[512,256]{1,0:T(8,128)(2,1)S(1)}, u32[]{:S(2)}, u32[]{:S(2)}) collective-permute-start(bf16[512,256]{1,0:T(8,128)(2,1)S(1)} %shard_map.122), channel_id=1, source_target_pairs={{0,14},{1,15},{2,0},{3,1},{4,2},{5,3},{6,4},{7,5},{8,6},{9,7},{10,... | collective-permute-start | bytes 786440 | tf_op jit(solution)/shard_map/ppermute | solution.py:287
  116.6 4.5 %collective-permute-done.11.came_ref = bf16[512,256]{1,0:T(8,128)(2,1)S(1)} collective-permute-done((bf16[512,256]{1,0:T(8,128)(2,1)S(1)}, bf16[512,256]{1,0:T(8,128)(2,1)S(1)}, u32[]{:S(2)}, u32[]{:S(2)}) %collective-permute-start.11) | collective-permute-done | bytes 262176 | tf_op jit(solution)/shard_map/ppermute | solution.py:287
  121.1 1.9 %collective-permute-start.12 = (bf16[512,256]{1,0:T(8,128)(2,1)S(1)}, bf16[512,256]{1,0:T(8,128)(2,1)S(1)}, u32[]{:S(2)}, u32[]{:S(2)}) collective-permute-start(bf16[512,256]{1,0:T(8,128)(2,1)S(1)} %shard_map.120), channel_id=1, source_target_pairs={{0,2},{1,3},{2,4},{3,5},{4,6},{5,7},{6,8},{7,9},{8,10},{9,11},{10,... | collective-permute-start | bytes 786440 | tf_op jit(solution)/shard_map/ppermute | solution.py:287
  123.0 8.5 %collective-permute-done.12.p_ref = bf16[512,256]{1,0:T(8,128)(2,1)S(1)} collective-permute-done((bf16[512,256]{1,0:T(8,128)(2,1)S(1)}, bf16[512,256]{1,0:T(8,128)(2,1)S(1)}, u32[]{:S(2)}, u32[]{:S(2)}) %collective-permute-start.12) | collective-permute-done | bytes 262176 | tf_op jit(solution)/shard_map/ppermute | solution.py:287
  132.3 3.9 %all-to-all-start.1 = ((bf16[32,16,256]{2,1,0:T(8,128)(2,1)}), bf16[32,16,256]{2,1,0:T(8,128)(2,1)S(1)}, u32[]{:S(2)}, u32[]{:S(2)}) async-start(bf16[32,16,256]{2,1,0:T(8,128)(2,1)} %bitcast.11), calls=%async_computation.1 | async-start | bytes 524288 | tf_op jit(solution)/shard_map/all_to_all | solution.py:383
  136.5 10.1 %all-to-all-done.1 = bf16[32,16,256]{2,1,0:T(8,128)(2,1)S(1)} async-done(((bf16[32,16,256]{2,1,0:T(8,128)(2,1)}), bf16[32,16,256]{2,1,0:T(8,128)(2,1)S(1)}, u32[]{:S(2)}, u32[]{:S(2)}) %all-to-all-start.1) | async-done | bytes 262176 | tf_op jit(solution)/shard_map/all_to_all | solution.py:383
  147.4 14.1 %collective-permute-start.16 = (f32[256,128]{1,0:T(8,128)S(1)}, f32[256,128]{1,0:T(8,128)S(1)}, u32[]{:S(2)}, u32[]{:S(2)}) collective-permute-start(f32[256,128]{1,0:T(8,128)S(1)} %get-tuple-element.58), channel_id=1, source_target_pairs={{0,1},{1,0},{2,3},{3,2},{4,5},{5,4},{6,7},{7,6},{8,9},{9,8},{10,11... | collective-permute-start | bytes 393224 | tf_op jit(solution)/shard_map/ppermute | solution.py:290
  (39 shorter events, 19.9 us)
Async XLA Ops:
  0.0 11.0 %copy-start.1 = (bf16[256,64]{0,1:T(8,128)(2,1)S(1)}, bf16[256,64]{0,1:T(8,128)(2,1)}, u32[]{:S(2)}) copy-start(bf16[256,64]{0,1:T(8,128)(2,1)} %param.11) | copy-start | bytes 98308
  0.0 30.2 %copy-start = (s32[256,2]{0,1:T(2,128)S(1)}, s32[256,2]{0,1:T(2,128)}, u32[]{:S(2)}) copy-start(s32[256,2]{0,1:T(2,128)} %param.17) | copy-start | bytes 6148
  2.2 28.0 %collective-permute-start.1 = (bf16[6784,256]{1,0:T(8,128)(2,1)S(1)}, bf16[6784,256]{1,0:T(8,128)(2,1)S(1)}, u32[]{:S(2)}, u32[]{:S(2)}) collective-permute-start(bf16[6784,256]{1,0:T(8,128)(2,1)S(1)} %get-tuple-element.36.own_ref), channel_id=1, source_target_pairs={{0,1},{1,0},{2,3},{3,2},{4,5},{5,4},{6,7},{7,6},{8,9},{9,8},{10,11... | collective-permute-start | bytes 10420232 | tf_op jit(solution)/shard_map/ppermute | solution.py:290
  11.0 2.3 %collective-permute-start = (bf16[64,256]{1,0:T(8,128)(2,1)S(1)}, bf16[64,256]{1,0:T(8,128)(2,1)S(1)}, u32[]{:S(2)}, u32[]{:S(2)}) collective-permute-start(bf16[64,256]{1,0:T(8,128)(2,1)S(1)} %bitcast.24), channel_id=1, source_target_pairs={{0,16},{16,32},{32,48},{48,64},{64,80},{80,96},{96,112},{112,128},... | collective-permute-start | bytes 98312 | tf_op jit(solution)/shard_map/ppermute | solution.py:295
  57.0 8.3 %collective-permute-start.2 = (bf16[512,256]{1,0:T(8,128)(2,1)S(1)}, bf16[512,256]{1,0:T(8,128)(2,1)S(1)}, u32[]{:S(2)}, u32[]{:S(2)}) collective-permute-start(bf16[512,256]{1,0:T(8,128)(2,1)S(1)} %bitcast.14), channel_id=1, source_target_pairs={{0,2},{1,3},{2,4},{3,5},{4,6},{5,7},{6,8},{7,9},{8,10},{9,11},{10,... | collective-permute-start | bytes 786440 | tf_op jit(solution)/shard_map/ppermute | solution.py:287
  58.9 8.3 %collective-permute-start.6 = (bf16[512,256]{1,0:T(8,128)(2,1)S(1)}, bf16[512,256]{1,0:T(8,128)(2,1)S(1)}, u32[]{:S(2)}, u32[]{:S(2)}) collective-permute-start(bf16[512,256]{1,0:T(8,128)(2,1)S(1)} %bitcast.15), channel_id=1, source_target_pairs={{0,14},{1,15},{2,0},{3,1},{4,2},{5,3},{6,4},{7,5},{8,6},{9,7},{10,... | collective-permute-start | bytes 786440 | tf_op jit(solution)/shard_map/ppermute | solution.py:287
  65.3 8.3 %collective-permute-start.3 = (bf16[512,256]{1,0:T(8,128)(2,1)S(1)}, bf16[512,256]{1,0:T(8,128)(2,1)S(1)}, u32[]{:S(2)}, u32[]{:S(2)}) collective-permute-start(bf16[512,256]{1,0:T(8,128)(2,1)S(1)} %collective-permute-done.2.p_ref), channel_id=1, source_target_pairs={{0,2},{1,3},{2,4},{3,5},{4,6},{5,7},{6,8},{7,9},{8,10},{9,11},{10,... | collective-permute-start | bytes 786440 | tf_op jit(solution)/shard_map/ppermute | solution.py:287
  67.2 8.3 %collective-permute-start.7 = (bf16[512,256]{1,0:T(8,128)(2,1)S(1)}, bf16[512,256]{1,0:T(8,128)(2,1)S(1)}, u32[]{:S(2)}, u32[]{:S(2)}) collective-permute-start(bf16[512,256]{1,0:T(8,128)(2,1)S(1)} %collective-permute-done.6.m_ref), channel_id=1, source_target_pairs={{0,14},{1,15},{2,0},{3,1},{4,2},{5,3},{6,4},{7,5},{8,6},{9,7},{10,... | collective-permute-start | bytes 786440 | tf_op jit(solution)/shard_map/ppermute | solution.py:287
  73.6 8.3 %collective-permute-start.4 = (bf16[512,256]{1,0:T(8,128)(2,1)S(1)}, bf16[512,256]{1,0:T(8,128)(2,1)S(1)}, u32[]{:S(2)}, u32[]{:S(2)}) collective-permute-start(bf16[512,256]{1,0:T(8,128)(2,1)S(1)} %collective-permute-done.3.p_ref), channel_id=1, source_target_pairs={{0,2},{1,3},{2,4},{3,5},{4,6},{5,7},{6,8},{7,9},{8,10},{9,11},{10,... | collective-permute-start | bytes 786440 | tf_op jit(solution)/shard_map/ppermute | solution.py:287
  75.5 10.2 %collective-permute-start.8 = (bf16[512,256]{1,0:T(8,128)(2,1)S(1)}, bf16[512,256]{1,0:T(8,128)(2,1)S(1)}, u32[]{:S(2)}, u32[]{:S(2)}) collective-permute-start(bf16[512,256]{1,0:T(8,128)(2,1)S(1)} %collective-permute-done.7.m_ref), channel_id=1, source_target_pairs={{0,14},{1,15},{2,0},{3,1},{4,2},{5,3},{6,4},{7,5},{8,6},{9,7},{10,... | collective-permute-start | bytes 786440 | tf_op jit(solution)/shard_map/ppermute | solution.py:287
  81.9 8.3 %collective-permute-start.5 = (bf16[512,256]{1,0:T(8,128)(2,1)S(1)}, bf16[512,256]{1,0:T(8,128)(2,1)S(1)}, u32[]{:S(2)}, u32[]{:S(2)}) collective-permute-start(bf16[512,256]{1,0:T(8,128)(2,1)S(1)} %collective-permute-done.4.p_ref), channel_id=1, source_target_pairs={{0,2},{1,3},{2,4},{3,5},{4,6},{5,7},{6,8},{7,9},{8,10},{9,11},{10,... | collective-permute-start | bytes 786440 | tf_op jit(solution)/shard_map/ppermute | solution.py:287
  91.2 8.3 %collective-permute-start.9 = (bf16[512,256]{1,0:T(8,128)(2,1)S(1)}, bf16[512,256]{1,0:T(8,128)(2,1)S(1)}, u32[]{:S(2)}, u32[]{:S(2)}) collective-permute-start(bf16[512,256]{1,0:T(8,128)(2,1)S(1)} %get-tuple-element.53), channel_id=1, source_target_pairs={{0,2},{1,3},{2,4},{3,5},{4,6},{5,7},{6,8},{7,9},{8,10},{9,11},{10,... | collective-permute-start | bytes 786440 | tf_op jit(solution)/shard_map/ppermute | solution.py:287
  93.1 8.4 %collective-permute-start.13 = (bf16[512,256]{1,0:T(8,128)(2,1)S(1)}, bf16[512,256]{1,0:T(8,128)(2,1)S(1)}, u32[]{:S(2)}, u32[]{:S(2)}) collective-permute-start(bf16[512,256]{1,0:T(8,128)(2,1)S(1)} %get-tuple-element.56), channel_id=1, source_target_pairs={{0,14},{1,15},{2,0},{3,1},{4,2},{5,3},{6,4},{7,5},{8,6},{9,7},{10,... | collective-permute-start | bytes 786440 | tf_op jit(solution)/shard_map/ppermute | solution.py:287
  99.6 10.2 %collective-permute-start.10 = (bf16[512,256]{1,0:T(8,128)(2,1)S(1)}, bf16[512,256]{1,0:T(8,128)(2,1)S(1)}, u32[]{:S(2)}, u32[]{:S(2)}) collective-permute-start(bf16[512,256]{1,0:T(8,128)(2,1)S(1)} %shard_map.118), channel_id=1, source_target_pairs={{0,2},{1,3},{2,4},{3,5},{4,6},{5,7},{6,8},{7,9},{8,10},{9,11},{10,... | collective-permute-start | bytes 786440 | tf_op jit(solution)/shard_map/ppermute | solution.py:287
  101.6 10.2 %collective-permute-start.14 = (bf16[512,256]{1,0:T(8,128)(2,1)S(1)}, bf16[512,256]{1,0:T(8,128)(2,1)S(1)}, u32[]{:S(2)}, u32[]{:S(2)}) collective-permute-start(bf16[512,256]{1,0:T(8,128)(2,1)S(1)} %shard_map.121), channel_id=1, source_target_pairs={{0,14},{1,15},{2,0},{3,1},{4,2},{5,3},{6,4},{7,5},{8,6},{9,7},{10,... | collective-permute-start | bytes 786440 | tf_op jit(solution)/shard_map/ppermute | solution.py:287
  109.8 26.6 %copy-start.2 = (f32[256,2]{0,1:T(2,128)S(1)}, f32[256,2]{0,1:T(2,128)}, u32[]{:S(2)}) copy-start(f32[256,2]{0,1:T(2,128)} %param.18) | copy-start | bytes 6148
  109.8 11.3 %collective-permute-start.11 = (bf16[512,256]{1,0:T(8,128)(2,1)S(1)}, bf16[512,256]{1,0:T(8,128)(2,1)S(1)}, u32[]{:S(2)}, u32[]{:S(2)}) collective-permute-start(bf16[512,256]{1,0:T(8,128)(2,1)S(1)} %shard_map.119), channel_id=1, source_target_pairs={{0,2},{1,3},{2,4},{3,5},{4,6},{5,7},{6,8},{7,9},{8,10},{9,11},{10,... | collective-permute-start | bytes 786440 | tf_op jit(solution)/shard_map/ppermute | solution.py:287
  111.8 11.2 %collective-permute-start.15 = (bf16[512,256]{1,0:T(8,128)(2,1)S(1)}, bf16[512,256]{1,0:T(8,128)(2,1)S(1)}, u32[]{:S(2)}, u32[]{:S(2)}) collective-permute-start(bf16[512,256]{1,0:T(8,128)(2,1)S(1)} %shard_map.122), channel_id=1, source_target_pairs={{0,14},{1,15},{2,0},{3,1},{4,2},{5,3},{6,4},{7,5},{8,6},{9,7},{10,... | collective-permute-start | bytes 786440 | tf_op jit(solution)/shard_map/ppermute | solution.py:287
  121.1 10.4 %collective-permute-start.12 = (bf16[512,256]{1,0:T(8,128)(2,1)S(1)}, bf16[512,256]{1,0:T(8,128)(2,1)S(1)}, u32[]{:S(2)}, u32[]{:S(2)}) collective-permute-start(bf16[512,256]{1,0:T(8,128)(2,1)S(1)} %shard_map.120), channel_id=1, source_target_pairs={{0,2},{1,3},{2,4},{3,5},{4,6},{5,7},{6,8},{7,9},{8,10},{9,11},{10,... | collective-permute-start | bytes 786440 | tf_op jit(solution)/shard_map/ppermute | solution.py:287
  132.3 14.3 %all-to-all-start.1 = ((bf16[32,16,256]{2,1,0:T(8,128)(2,1)}), bf16[32,16,256]{2,1,0:T(8,128)(2,1)S(1)}, u32[]{:S(2)}, u32[]{:S(2)}) async-start(bf16[32,16,256]{2,1,0:T(8,128)(2,1)} %bitcast.11), calls=%async_computation.1 | async-start | bytes 524288 | tf_op jit(solution)/shard_map/all_to_all | solution.py:383
  147.4 15.1 %collective-permute-start.16 = (f32[256,128]{1,0:T(8,128)S(1)}, f32[256,128]{1,0:T(8,128)S(1)}, u32[]{:S(2)}, u32[]{:S(2)}) collective-permute-start(f32[256,128]{1,0:T(8,128)S(1)} %get-tuple-element.58), channel_id=1, source_target_pairs={{0,1},{1,0},{2,3},{3,2},{4,5},{5,4},{6,7},{7,6},{8,9},{9,8},{10,11... | collective-permute-start | bytes 393224 | tf_op jit(solution)/shard_map/ppermute | solution.py:290

commit v3 on v2

--- a/solution.py
+++ b/solution.py
@@ -77,36 +77,10 @@
     return slots
 
 
-def column_slots(routes_ref, experts, capacity):
-    rows = routes_ref.shape[0]
-    named = [iota((rows, experts), 1) == routes_ref[:, k : k + 1] for k in range(TOPK)]
-    ones = sum(jnp.where(n, 1.0, 0.0) for n in named)
-    lower = jnp.where(iota((rows, rows), 0) > iota((rows, rows), 1), 1.0, 0.0).astype(BF16)
-    earlier = mm(lower, ones.astype(BF16))
-    slots = []
-    for k in range(TOPK):
-        rank = jnp.sum(jnp.where(named[k], earlier, 0.0), axis=1, keepdims=True).astype(jnp.int32)
-        slots.append(routes_ref[:, k : k + 1] * capacity + rank)
-    return slots
-
-
 def slot_ids(shape, dim, capacity, core):
     half = capacity // CORES
     place = iota(shape, dim)
     return lax.div(place, half) * capacity + core * half + lax.rem(place, half)
-
-
-def column_slots(routes_ref, experts, capacity):
-    rows = routes_ref.shape[0]
-    named = [iota((rows, experts), 1) == routes_ref[:, k : k + 1] for k in range(TOPK)]
-    ones = sum(jnp.where(n, 1.0, 0.0) for n in named)
-    lower = jnp.where(iota((rows, rows), 0) > iota((rows, rows), 1), 1.0, 0.0).astype(BF16)
-    earlier = mm(lower, ones.astype(BF16))
-    slots = []
-    for k in range(TOPK):
-        rank = jnp.sum(jnp.where(named[k], earlier, 0.0), axis=1, keepdims=True).astype(jnp.int32)
-        slots.append(routes_ref[:, k : k + 1] * capacity + rank)
-    return slots
 
 
 class Pack:
@@ -187,8 +161,8 @@
 
 
 def chip_at(chips, step):
-    here = lax.div(lax.axis_index("tp"), CORES)
-    return lax.rem(here + step + chips, chips)
+    here, core = lax.div(lax.axis_index("tp"), CORES), lax.rem(lax.axis_index("tp"), CORES)
+    return lax.rem(here + step * (1 - 2 * core) + chips, chips)
 
 
 def first_kernel(pack, chips, x_ref, gain_ref, own_ref, other_ref, acc_ref, square_ref):
@@ -238,14 +212,16 @@
 
 def pick_kernel(experts, capacity, back_ref, routes_ref, weight_ref, mine_ref, other_ref):
     core = lax.rem(lax.axis_index("tp"), CORES)
-    slots = column_slots(routes_ref, experts, capacity)
-    shape = (routes_ref.shape[0], back_ref.shape[0])
-    ids = slot_ids(shape, 1, capacity, core)
+    slots = row_slots(routes_ref, experts, capacity)
+    tokens = routes_ref.shape[1]
+    ids = slot_ids((back_ref.shape[0], tokens), 0, capacity, core)
+    eye = iota((tokens, tokens), 0) == iota((tokens, tokens), 1)
     rows = back_ref[...]
     total = 0.0
     for k in range(TOPK):
         chosen = jnp.where(slots[k] == ids, 1.0, 0.0).astype(BF16)
-        total = total + mm(chosen, rows) * weight_ref[:, k : k + 1]
+        weight = jnp.sum(jnp.where(eye, weight_ref[k : k + 1, :], 0.0), axis=1, keepdims=True)
+        total = total + mm(chosen, rows, 0, 0) * weight
     features = mine_ref.shape[1]
     left, right = total[:, :features], total[:, features:]
     mine_ref[...] = jnp.where(core == 0, left, right)
@@ -282,7 +258,7 @@
 
     def along(value, step):
         pairs = [
-            (y * CORES + c, (y + step) % chips * CORES + c) for y in range(chips) for c in range(CORES)
+            (y * CORES + c, (y + step * (1 - 2 * c)) % chips * CORES + c) for y in range(chips) for c in range(CORES)
         ]
         return lax.ppermute(value, "tp", pairs)
 
@@ -386,7 +362,7 @@
     mine, theirs = call(
         functools.partial(pick_kernel, experts, capacity),
         (shape((tok_rows, features), F32),) * 2,
-        (returned, routes, route_weight),
+        (returned, routes.T, route_weight.T),
         4 * experts * half * width * tok_rows,
         12,
     )

time: 164 us -> 163 us (level)
  waiting for transfers between devices: 38.6 us -> 18.2 us
  blocking collectives: 42.5 us -> 58.4 us
  starting transfers between devices: 71.1 us -> 75.8 us
    all_to_all x0 -> x1, blocking collectives: none -> 15.9 us  [on_device(): lax.all_to_all(result.reshape(blocks, half, width), 'sp', split_axis=0, c...]
    ppermute x14, waiting for transfers between devices: 26.5 us -> 16.2 us  [along(): return lax.ppermute(value, 'tp', pairs)]
    all_to_all x1 -> x0, waiting for transfers between devices: 10.1 us -> none  [on_device(): lax.all_to_all(result.reshape(blocks, half, width), 'sp', split_axis=0, c...]
    ppermute x14, starting transfers between devices: 43 us -> 49.5 us  [along(): return lax.ppermute(value, 'tp', pairs)]
    all_to_all x1 -> x0, starting transfers between devices: 3.94 us -> none  [on_device(): lax.all_to_all(result.reshape(blocks, half, width), 'sp', split_axis=0, c...]
    ppermute x2, starting transfers between devices: 22.9 us -> 25 us  [across(): return lax.ppermute(value, 'tp', [(t, t ^ 1) for t in range(members)])]
  transfers between devices with their start and end apart: 18 -> 17, of which waited for: 11 -> 12; matrix products, arithmetic and copies ran while one was open for 0% -> 0% of each run, Pallas kernels for 3% -> 3%
where the time goes in v3:
time: 163 us; the launch traced here: 162 us
  starting transfers between devices  75.8 us (47%)
  blocking collectives  58.4 us (36%)
  waiting for transfers between devices  18.2 us (11%)
  Pallas kernels  9.44 us (6%)
    ppermute x14, starting transfers between devices, along(): return lax.ppermute(value, 'tp', pairs)  49.5 us
    all_to_all x1, blocking collectives, on_device(): lax.all_to_all(sent.reshape(experts, half, width), 'sp', split_axis=0, co...  25.9 us
    ppermute x2, starting transfers between devices, across(): return lax.ppermute(value, 'tp', [(t, t ^ 1) for t in range(members)])  25 us
    all_gather x1, blocking collectives, on_device(): mixed = lax.all_gather(pooled, 'tp', axis=0, tiled=False)  16.6 us
    ppermute x14, waiting for transfers between devices, along(): return lax.ppermute(value, 'tp', pairs)  16.2 us
    all_to_all x1, blocking collectives, on_device(): lax.all_to_all(result.reshape(blocks, half, width), 'sp', split_axis=0, c...  15.9 us
    pallas_call x17, Pallas kernels, call(): pl.pallas_call(kernel, out_shape=out_shape, in_specs=[pl.BlockSpec(memory...  9.44 us
  transfers between devices with their start and end apart: 17, of which 12 were waited for; matrix products, arithmetic and copies ran while one was open for 0% of the time, Pallas kernels for 3%

profile of v3, /device:TPU:1, one launch (start us, length us, event | category | flops | bytes accessed | tf_op | source)
XLA Modules:
  0.0 162.2 jit_solution(14500365039980927771)
XLA Ops:
  0.0 2.2 %shard_map.109 = (bf16[6784,256]{1,0:T(8,128)(2,1)S(1)}, bf16[64,256]{1,0:T(8,128)(2,1)S(1)}, bf16[64,64]{1,0:T(8,128)(2,1)S(1)}, bf16[1,64]{1,0:T(2,128)(2,1)S(1)}, bf16[1,128]{1,0:T(2,128)(2,1)S(1)}) custom-call(bf16[2048,256]{1,0:T(8,128)(2,1)} %bitcast.24, bf16[2048,256]{1,0:T(8,128)(2,1)} %bitcast.25, bf16[256,2048]{1,0:T(8,128)(2,1)} %bitcast.26, ...), custom_call_target="tpu_custom_call" | custom-call | flops 889192448 | bytes 1736704 | tf_op jit(solution)/shard_map/pallas_call | solution.py:33
  2.2 8.7 %collective-permute-start.1 = (bf16[6784,256]{1,0:T(8,128)(2,1)S(1)}, bf16[6784,256]{1,0:T(8,128)(2,1)S(1)}, u32[]{:S(2)}, u32[]{:S(2)}) collective-permute-start(bf16[6784,256]{1,0:T(8,128)(2,1)S(1)} %get-tuple-element.36.own_ref), channel_id=1, source_target_pairs={{0,1},{1,0},{2,3},{3,2},{4,5},{5,4},{6,7},{7,6},{8,9},{9,8},{10,11... | collective-permute-start | bytes 10420232 | tf_op jit(solution)/shard_map/ppermute | solution.py:266
  13.6 16.6 %all-gather = bf16[1280,256]{1,0:T(8,128)(2,1)S(1)} all-gather(bf16[80,256]{1,0:T(8,128)(2,1)S(1)} %shard_map.110), channel_id=2, replica_groups=mesh['sp'=32,'tp'=16] {'tp'}, dimensions={0}, use_global_device_ids=true | all-gather | bytes 696320 | tf_op jit(solution)/shard_map/all_gather | solution.py:296
  31.0 25.9 %all_to_all.10 = bf16[32,16,256]{2,1,0:T(8,128)(2,1)S(1)} all-to-all(bf16[32,16,256]{2,1,0:T(8,128)(2,1)S(1)} %bitcast.19), channel_id=1, replica_groups=mesh['sp'=32,'tp'=16] {'sp'}, dimensions={0} | all-to-all | bytes 524288 | tf_op jit(solution)/shard_map/all_to_all | solution.py:308
  57.0 2.4 %collective-permute-start.2 = (bf16[512,256]{1,0:T(8,128)(2,1)S(1)}, bf16[512,256]{1,0:T(8,128)(2,1)S(1)}, u32[]{:S(2)}, u32[]{:S(2)}) collective-permute-start(bf16[512,256]{1,0:T(8,128)(2,1)S(1)} %bitcast.15), channel_id=1, source_target_pairs={{0,2},{1,15},{2,4},{3,1},{4,6},{5,3},{6,8},{7,5},{8,10},{9,7},{10,... | collective-permute-start | bytes 786440 | tf_op jit(solution)/shard_map/ppermute | solution.py:263
  59.4 2.8 %collective-permute-start.6 = (bf16[512,256]{1,0:T(8,128)(2,1)S(1)}, bf16[512,256]{1,0:T(8,128)(2,1)S(1)}, u32[]{:S(2)}, u32[]{:S(2)}) collective-permute-start(bf16[512,256]{1,0:T(8,128)(2,1)S(1)} %bitcast.16), channel_id=1, source_target_pairs={{0,14},{1,3},{2,0},{3,5},{4,2},{5,7},{6,4},{7,9},{8,6},{9,11},{10,... | collective-permute-start | bytes 786440 | tf_op jit(solution)/shard_map/ppermute | solution.py:263
  62.2 1.8 %collective-permute-done.2.p_ref = bf16[512,256]{1,0:T(8,128)(2,1)S(1)} collective-permute-done((bf16[512,256]{1,0:T(8,128)(2,1)S(1)}, bf16[512,256]{1,0:T(8,128)(2,1)S(1)}, u32[]{:S(2)}, u32[]{:S(2)}) %collective-permute-start.2) | collective-permute-done | bytes 262176 | tf_op jit(solution)/shard_map/ppermute | solution.py:263
  64.1 3.6 %collective-permute-start.3 = (bf16[512,256]{1,0:T(8,128)(2,1)S(1)}, bf16[512,256]{1,0:T(8,128)(2,1)S(1)}, u32[]{:S(2)}, u32[]{:S(2)}) collective-permute-start(bf16[512,256]{1,0:T(8,128)(2,1)S(1)} %collective-permute-done.2.p_ref), channel_id=1, source_target_pairs={{0,2},{1,15},{2,4},{3,1},{4,6},{5,3},{6,8},{7,5},{8,10},{9,7},{10,... | collective-permute-start | bytes 786440 | tf_op jit(solution)/shard_map/ppermute | solution.py:263
  67.7 2.8 %collective-permute-done.6.m_ref = bf16[512,256]{1,0:T(8,128)(2,1)S(1)} collective-permute-done((bf16[512,256]{1,0:T(8,128)(2,1)S(1)}, bf16[512,256]{1,0:T(8,128)(2,1)S(1)}, u32[]{:S(2)}, u32[]{:S(2)}) %collective-permute-start.6) | collective-permute-done | bytes 262176 | tf_op jit(solution)/shard_map/ppermute | solution.py:263
  70.5 1.9 %collective-permute-start.7 = (bf16[512,256]{1,0:T(8,128)(2,1)S(1)}, bf16[512,256]{1,0:T(8,128)(2,1)S(1)}, u32[]{:S(2)}, u32[]{:S(2)}) collective-permute-start(bf16[512,256]{1,0:T(8,128)(2,1)S(1)} %collective-permute-done.6.m_ref), channel_id=1, source_target_pairs={{0,14},{1,3},{2,0},{3,5},{4,2},{5,7},{6,4},{7,9},{8,6},{9,11},{10,... | collective-permute-start | bytes 786440 | tf_op jit(solution)/shard_map/ppermute | solution.py:263
  72.6 5.0 %collective-permute-start.4 = (bf16[512,256]{1,0:T(8,128)(2,1)S(1)}, bf16[512,256]{1,0:T(8,128)(2,1)S(1)}, u32[]{:S(2)}, u32[]{:S(2)}) collective-permute-start(bf16[512,256]{1,0:T(8,128)(2,1)S(1)} %collective-permute-done.3.p_ref), channel_id=1, source_target_pairs={{0,2},{1,15},{2,4},{3,1},{4,6},{5,3},{6,8},{7,5},{8,10},{9,7},{10,... | collective-permute-start | bytes 786440 | tf_op jit(solution)/shard_map/ppermute | solution.py:263
  77.7 3.0 %collective-permute-done.7.m_ref = bf16[512,256]{1,0:T(8,128)(2,1)S(1)} collective-permute-done((bf16[512,256]{1,0:T(8,128)(2,1)S(1)}, bf16[512,256]{1,0:T(8,128)(2,1)S(1)}, u32[]{:S(2)}, u32[]{:S(2)}) %collective-permute-start.7) | collective-permute-done | bytes 262176 | tf_op jit(solution)/shard_map/ppermute | solution.py:263
  80.7 1.9 %collective-permute-start.8 = (bf16[512,256]{1,0:T(8,128)(2,1)S(1)}, bf16[512,256]{1,0:T(8,128)(2,1)S(1)}, u32[]{:S(2)}, u32[]{:S(2)}) collective-permute-start(bf16[512,256]{1,0:T(8,128)(2,1)S(1)} %collective-permute-done.7.m_ref), channel_id=1, source_target_pairs={{0,14},{1,3},{2,0},{3,5},{4,2},{5,7},{6,4},{7,9},{8,6},{9,11},{10,... | collective-permute-start | bytes 786440 | tf_op jit(solution)/shard_map/ppermute | solution.py:263
  83.0 5.3 %collective-permute-start.5 = (bf16[512,256]{1,0:T(8,128)(2,1)S(1)}, bf16[512,256]{1,0:T(8,128)(2,1)S(1)}, u32[]{:S(2)}, u32[]{:S(2)}) collective-permute-start(bf16[512,256]{1,0:T(8,128)(2,1)S(1)} %collective-permute-done.4.p_ref), channel_id=1, source_target_pairs={{0,2},{1,15},{2,4},{3,1},{4,6},{5,3},{6,8},{7,5},{8,10},{9,7},{10,... | collective-permute-start | bytes 786440 | tf_op jit(solution)/shard_map/ppermute | solution.py:263
  93.7 5.3 %collective-permute-start.9 = (bf16[512,256]{1,0:T(8,128)(2,1)S(1)}, bf16[512,256]{1,0:T(8,128)(2,1)S(1)}, u32[]{:S(2)}, u32[]{:S(2)}) collective-permute-start(bf16[512,256]{1,0:T(8,128)(2,1)S(1)} %get-tuple-element.53), channel_id=1, source_target_pairs={{0,2},{1,15},{2,4},{3,1},{4,6},{5,3},{6,8},{7,5},{8,10},{9,7},{10,... | collective-permute-start | bytes 786440 | tf_op jit(solution)/shard_map/ppermute | solution.py:263
  99.0 1.9 %collective-permute-start.13 = (bf16[512,256]{1,0:T(8,128)(2,1)S(1)}, bf16[512,256]{1,0:T(8,128)(2,1)S(1)}, u32[]{:S(2)}, u32[]{:S(2)}) collective-permute-start(bf16[512,256]{1,0:T(8,128)(2,1)S(1)} %get-tuple-element.56), channel_id=1, source_target_pairs={{0,14},{1,3},{2,0},{3,5},{4,2},{5,7},{6,4},{7,9},{8,6},{9,11},{10,... | collective-permute-start | bytes 786440 | tf_op jit(solution)/shard_map/ppermute | solution.py:263
  102.4 5.0 %collective-permute-start.10 = (bf16[512,256]{1,0:T(8,128)(2,1)S(1)}, bf16[512,256]{1,0:T(8,128)(2,1)S(1)}, u32[]{:S(2)}, u32[]{:S(2)}) collective-permute-start(bf16[512,256]{1,0:T(8,128)(2,1)S(1)} %shard_map.118), channel_id=1, source_target_pairs={{0,2},{1,15},{2,4},{3,1},{4,6},{5,3},{6,8},{7,5},{8,10},{9,7},{10,... | collective-permute-start | bytes 786440 | tf_op jit(solution)/shard_map/ppermute | solution.py:263
  107.5 1.9 %collective-permute-start.14 = (bf16[512,256]{1,0:T(8,128)(2,1)S(1)}, bf16[512,256]{1,0:T(8,128)(2,1)S(1)}, u32[]{:S(2)}, u32[]{:S(2)}) collective-permute-start(bf16[512,256]{1,0:T(8,128)(2,1)S(1)} %shard_map.121), channel_id=1, source_target_pairs={{0,14},{1,3},{2,0},{3,5},{4,2},{5,7},{6,4},{7,9},{8,6},{9,11},{10,... | collective-permute-start | bytes 786440 | tf_op jit(solution)/shard_map/ppermute | solution.py:263
  110.8 5.4 %collective-permute-start.11 = (bf16[512,256]{1,0:T(8,128)(2,1)S(1)}, bf16[512,256]{1,0:T(8,128)(2,1)S(1)}, u32[]{:S(2)}, u32[]{:S(2)}) collective-permute-start(bf16[512,256]{1,0:T(8,128)(2,1)S(1)} %shard_map.119), channel_id=1, source_target_pairs={{0,2},{1,15},{2,4},{3,1},{4,6},{5,3},{6,8},{7,5},{8,10},{9,7},{10,... | collective-permute-start | bytes 786440 | tf_op jit(solution)/shard_map/ppermute | solution.py:263
  116.2 1.9 %collective-permute-start.15 = (bf16[512,256]{1,0:T(8,128)(2,1)S(1)}, bf16[512,256]{1,0:T(8,128)(2,1)S(1)}, u32[]{:S(2)}, u32[]{:S(2)}) collective-permute-start(bf16[512,256]{1,0:T(8,128)(2,1)S(1)} %shard_map.122), channel_id=1, source_target_pairs={{0,14},{1,3},{2,0},{3,5},{4,2},{5,7},{6,4},{7,9},{8,6},{9,11},{10,... | collective-permute-start | bytes 786440 | tf_op jit(solution)/shard_map/ppermute | solution.py:263
  119.5 5.0 %collective-permute-start.12 = (bf16[512,256]{1,0:T(8,128)(2,1)S(1)}, bf16[512,256]{1,0:T(8,128)(2,1)S(1)}, u32[]{:S(2)}, u32[]{:S(2)}) collective-permute-start(bf16[512,256]{1,0:T(8,128)(2,1)S(1)} %shard_map.120), channel_id=1, source_target_pairs={{0,2},{1,15},{2,4},{3,1},{4,6},{5,3},{6,8},{7,5},{8,10},{9,7},{10,... | collective-permute-start | bytes 786440 | tf_op jit(solution)/shard_map/ppermute | solution.py:263
  124.5 3.3 %collective-permute-done.12.p_ref = bf16[512,256]{1,0:T(8,128)(2,1)S(1)} collective-permute-done((bf16[512,256]{1,0:T(8,128)(2,1)S(1)}, bf16[512,256]{1,0:T(8,128)(2,1)S(1)}, u32[]{:S(2)}, u32[]{:S(2)}) %collective-permute-start.12) | collective-permute-done | bytes 262176 | tf_op jit(solution)/shard_map/ppermute | solution.py:263
  127.9 15.9 %all_to_all.11 = bf16[32,16,256]{2,1,0:T(8,128)(2,1)S(1)} all-to-all(bf16[32,16,256]{2,1,0:T(8,128)(2,1)S(1)} %bitcast.18), channel_id=1, replica_groups=mesh['sp'=32,'tp'=16] {'sp'}, dimensions={0} | all-to-all | bytes 524288 | tf_op jit(solution)/shard_map/all_to_all | solution.py:359
  144.3 16.3 %collective-permute-start.16 = (f32[256,128]{1,0:T(8,128)S(1)}, f32[256,128]{1,0:T(8,128)S(1)}, u32[]{:S(2)}, u32[]{:S(2)}) collective-permute-start(f32[256,128]{1,0:T(8,128)S(1)} %get-tuple-element.58), channel_id=1, source_target_pairs={{0,1},{1,0},{2,3},{3,2},{4,5},{5,4},{6,7},{7,6},{8,9},{9,8},{10,11... | collective-permute-start | bytes 393224 | tf_op jit(solution)/shard_map/ppermute | solution.py:266
  (36 shorter events, 15.9 us)
Async XLA Ops:
  0.0 11.0 %copy-start.2 = (bf16[256,64]{0,1:T(8,128)(2,1)S(1)}, bf16[256,64]{0,1:T(8,128)(2,1)}, u32[]{:S(2)}) copy-start(bf16[256,64]{0,1:T(8,128)(2,1)} %param.11) | copy-start | bytes 98308
  0.0 30.2 %copy-start = (s32[256,2]{0,1:T(2,128)S(1)}, s32[256,2]{0,1:T(2,128)}, u32[]{:S(2)}) copy-start(s32[256,2]{0,1:T(2,128)} %param.17) | copy-start | bytes 6148
  2.2 28.0 %collective-permute-start.1 = (bf16[6784,256]{1,0:T(8,128)(2,1)S(1)}, bf16[6784,256]{1,0:T(8,128)(2,1)S(1)}, u32[]{:S(2)}, u32[]{:S(2)}) collective-permute-start(bf16[6784,256]{1,0:T(8,128)(2,1)S(1)} %get-tuple-element.36.own_ref), channel_id=1, source_target_pairs={{0,1},{1,0},{2,3},{3,2},{4,5},{5,4},{6,7},{7,6},{8,9},{9,8},{10,11... | collective-permute-start | bytes 10420232 | tf_op jit(solution)/shard_map/ppermute | solution.py:266
  11.0 2.3 %collective-permute-start = (bf16[64,256]{1,0:T(8,128)(2,1)S(1)}, bf16[64,256]{1,0:T(8,128)(2,1)S(1)}, u32[]{:S(2)}, u32[]{:S(2)}) collective-permute-start(bf16[64,256]{1,0:T(8,128)(2,1)S(1)} %bitcast.28), channel_id=1, source_target_pairs={{0,16},{16,32},{32,48},{48,64},{64,80},{80,96},{96,112},{112,128},... | collective-permute-start | bytes 98312 | tf_op jit(solution)/shard_map/ppermute | solution.py:271
  57.0 7.1 %collective-permute-start.2 = (bf16[512,256]{1,0:T(8,128)(2,1)S(1)}, bf16[512,256]{1,0:T(8,128)(2,1)S(1)}, u32[]{:S(2)}, u32[]{:S(2)}) collective-permute-start(bf16[512,256]{1,0:T(8,128)(2,1)S(1)} %bitcast.15), channel_id=1, source_target_pairs={{0,2},{1,15},{2,4},{3,1},{4,6},{5,3},{6,8},{7,5},{8,10},{9,7},{10,... | collective-permute-start | bytes 786440 | tf_op jit(solution)/shard_map/ppermute | solution.py:263
  59.4 11.1 %collective-permute-start.6 = (bf16[512,256]{1,0:T(8,128)(2,1)S(1)}, bf16[512,256]{1,0:T(8,128)(2,1)S(1)}, u32[]{:S(2)}, u32[]{:S(2)}) collective-permute-start(bf16[512,256]{1,0:T(8,128)(2,1)S(1)} %bitcast.16), channel_id=1, source_target_pairs={{0,14},{1,3},{2,0},{3,5},{4,2},{5,7},{6,4},{7,9},{8,6},{9,11},{10,... | collective-permute-start | bytes 786440 | tf_op jit(solution)/shard_map/ppermute | solution.py:263
  64.1 8.6 %collective-permute-start.3 = (bf16[512,256]{1,0:T(8,128)(2,1)S(1)}, bf16[512,256]{1,0:T(8,128)(2,1)S(1)}, u32[]{:S(2)}, u32[]{:S(2)}) collective-permute-start(bf16[512,256]{1,0:T(8,128)(2,1)S(1)} %collective-permute-done.2.p_ref), channel_id=1, source_target_pairs={{0,2},{1,15},{2,4},{3,1},{4,6},{5,3},{6,8},{7,5},{8,10},{9,7},{10,... | collective-permute-start | bytes 786440 | tf_op jit(solution)/shard_map/ppermute | solution.py:263
  70.5 10.2 %collective-permute-start.7 = (bf16[512,256]{1,0:T(8,128)(2,1)S(1)}, bf16[512,256]{1,0:T(8,128)(2,1)S(1)}, u32[]{:S(2)}, u32[]{:S(2)}) collective-permute-start(bf16[512,256]{1,0:T(8,128)(2,1)S(1)} %collective-permute-done.6.m_ref), channel_id=1, source_target_pairs={{0,14},{1,3},{2,0},{3,5},{4,2},{5,7},{6,4},{7,9},{8,6},{9,11},{10,... | collective-permute-start | bytes 786440 | tf_op jit(solution)/shard_map/ppermute | solution.py:263
  72.6 10.3 %collective-permute-start.4 = (bf16[512,256]{1,0:T(8,128)(2,1)S(1)}, bf16[512,256]{1,0:T(8,128)(2,1)S(1)}, u32[]{:S(2)}, u32[]{:S(2)}) collective-permute-start(bf16[512,256]{1,0:T(8,128)(2,1)S(1)} %collective-permute-done.3.p_ref), channel_id=1, source_target_pairs={{0,2},{1,15},{2,4},{3,1},{4,6},{5,3},{6,8},{7,5},{8,10},{9,7},{10,... | collective-permute-start | bytes 786440 | tf_op jit(solution)/shard_map/ppermute | solution.py:263
  80.7 9.6 %collective-permute-start.8 = (bf16[512,256]{1,0:T(8,128)(2,1)S(1)}, bf16[512,256]{1,0:T(8,128)(2,1)S(1)}, u32[]{:S(2)}, u32[]{:S(2)}) collective-permute-start(bf16[512,256]{1,0:T(8,128)(2,1)S(1)} %collective-permute-done.7.m_ref), channel_id=1, source_target_pairs={{0,14},{1,3},{2,0},{3,5},{4,2},{5,7},{6,4},{7,9},{8,6},{9,11},{10,... | collective-permute-start | bytes 786440 | tf_op jit(solution)/shard_map/ppermute | solution.py:263
  83.0 9.8 %collective-permute-start.5 = (bf16[512,256]{1,0:T(8,128)(2,1)S(1)}, bf16[512,256]{1,0:T(8,128)(2,1)S(1)}, u32[]{:S(2)}, u32[]{:S(2)}) collective-permute-start(bf16[512,256]{1,0:T(8,128)(2,1)S(1)} %collective-permute-done.4.p_ref), channel_id=1, source_target_pairs={{0,2},{1,15},{2,4},{3,1},{4,6},{5,3},{6,8},{7,5},{8,10},{9,7},{10,... | collective-permute-start | bytes 786440 | tf_op jit(solution)/shard_map/ppermute | solution.py:263
  93.7 8.6 %collective-permute-start.9 = (bf16[512,256]{1,0:T(8,128)(2,1)S(1)}, bf16[512,256]{1,0:T(8,128)(2,1)S(1)}, u32[]{:S(2)}, u32[]{:S(2)}) collective-permute-start(bf16[512,256]{1,0:T(8,128)(2,1)S(1)} %get-tuple-element.53), channel_id=1, source_target_pairs={{0,2},{1,15},{2,4},{3,1},{4,6},{5,3},{6,8},{7,5},{8,10},{9,7},{10,... | collective-permute-start | bytes 786440 | tf_op jit(solution)/shard_map/ppermute | solution.py:263
  99.0 8.4 %collective-permute-start.13 = (bf16[512,256]{1,0:T(8,128)(2,1)S(1)}, bf16[512,256]{1,0:T(8,128)(2,1)S(1)}, u32[]{:S(2)}, u32[]{:S(2)}) collective-permute-start(bf16[512,256]{1,0:T(8,128)(2,1)S(1)} %get-tuple-element.56), channel_id=1, source_target_pairs={{0,14},{1,3},{2,0},{3,5},{4,2},{5,7},{6,4},{7,9},{8,6},{9,11},{10,... | collective-permute-start | bytes 786440 | tf_op jit(solution)/shard_map/ppermute | solution.py:263
  102.4 8.3 %collective-permute-start.10 = (bf16[512,256]{1,0:T(8,128)(2,1)S(1)}, bf16[512,256]{1,0:T(8,128)(2,1)S(1)}, u32[]{:S(2)}, u32[]{:S(2)}) collective-permute-start(bf16[512,256]{1,0:T(8,128)(2,1)S(1)} %shard_map.118), channel_id=1, source_target_pairs={{0,2},{1,15},{2,4},{3,1},{4,6},{5,3},{6,8},{7,5},{8,10},{9,7},{10,... | collective-permute-start | bytes 786440 | tf_op jit(solution)/shard_map/ppermute | solution.py:263
  107.5 8.7 %collective-permute-start.14 = (bf16[512,256]{1,0:T(8,128)(2,1)S(1)}, bf16[512,256]{1,0:T(8,128)(2,1)S(1)}, u32[]{:S(2)}, u32[]{:S(2)}) collective-permute-start(bf16[512,256]{1,0:T(8,128)(2,1)S(1)} %shard_map.121), channel_id=1, source_target_pairs={{0,14},{1,3},{2,0},{3,5},{4,2},{5,7},{6,4},{7,9},{8,6},{9,11},{10,... | collective-permute-start | bytes 786440 | tf_op jit(solution)/shard_map/ppermute | solution.py:263
  110.8 33.0 %copy-start.1 = (f32[256,2]{0,1:T(2,128)S(1)}, f32[256,2]{0,1:T(2,128)}, u32[]{:S(2)}) copy-start(f32[256,2]{0,1:T(2,128)} %param.18) | copy-start | bytes 6148
  110.8 8.7 %collective-permute-start.11 = (bf16[512,256]{1,0:T(8,128)(2,1)S(1)}, bf16[512,256]{1,0:T(8,128)(2,1)S(1)}, u32[]{:S(2)}, u32[]{:S(2)}) collective-permute-start(bf16[512,256]{1,0:T(8,128)(2,1)S(1)} %shard_map.119), channel_id=1, source_target_pairs={{0,2},{1,15},{2,4},{3,1},{4,6},{5,3},{6,8},{7,5},{8,10},{9,7},{10,... | collective-permute-start | bytes 786440 | tf_op jit(solution)/shard_map/ppermute | solution.py:263
  116.2 8.3 %collective-permute-start.15 = (bf16[512,256]{1,0:T(8,128)(2,1)S(1)}, bf16[512,256]{1,0:T(8,128)(2,1)S(1)}, u32[]{:S(2)}, u32[]{:S(2)}) collective-permute-start(bf16[512,256]{1,0:T(8,128)(2,1)S(1)} %shard_map.122), channel_id=1, source_target_pairs={{0,14},{1,3},{2,0},{3,5},{4,2},{5,7},{6,4},{7,9},{8,6},{9,11},{10,... | collective-permute-start | bytes 786440 | tf_op jit(solution)/shard_map/ppermute | solution.py:263
  119.5 8.3 %collective-permute-start.12 = (bf16[512,256]{1,0:T(8,128)(2,1)S(1)}, bf16[512,256]{1,0:T(8,128)(2,1)S(1)}, u32[]{:S(2)}, u32[]{:S(2)}) collective-permute-start(bf16[512,256]{1,0:T(8,128)(2,1)S(1)} %shard_map.120), channel_id=1, source_target_pairs={{0,2},{1,15},{2,4},{3,1},{4,6},{5,3},{6,8},{7,5},{8,10},{9,7},{10,... | collective-permute-start | bytes 786440 | tf_op jit(solution)/shard_map/ppermute | solution.py:263
  144.3 17.2 %collective-permute-start.16 = (f32[256,128]{1,0:T(8,128)S(1)}, f32[256,128]{1,0:T(8,128)S(1)}, u32[]{:S(2)}, u32[]{:S(2)}) collective-permute-start(f32[256,128]{1,0:T(8,128)S(1)} %get-tuple-element.58), channel_id=1, source_target_pairs={{0,1},{1,0},{2,3},{3,2},{4,5},{5,4},{6,7},{7,6},{8,9},{9,8},{10,11... | collective-permute-start | bytes 393224 | tf_op jit(solution)/shard_map/ppermute | solution.py:266

commit v4 on v3

--- a/solution.py
+++ b/solution.py
@@ -161,8 +161,13 @@
 
 
 def chip_at(chips, step):
-    here, core = lax.div(lax.axis_index("tp"), CORES), lax.rem(lax.axis_index("tp"), CORES)
-    return lax.rem(here + step * (1 - 2 * core) + chips, chips)
+    here = lax.div(lax.axis_index("tp"), CORES)
+    return lax.rem(here + step + chips, chips)
+
+
+def chip_across(chips, step):
+    core = lax.rem(lax.axis_index("tp"), CORES)
+    return chip_at(chips, step * (1 - 2 * core))
 
 
 def first_kernel(pack, chips, x_ref, gain_ref, own_ref, other_ref, acc_ref, square_ref):
@@ -194,12 +199,12 @@
     up = jnp.clip(acc_ref[:, units:] * scale, -GATE_LIMIT, GATE_LIMIT)
     hidden_ref[...] = ((up + 1.0) * gate * jax.nn.sigmoid(GATE_ALPHA * gate)).astype(BF16)
     up_ref[...] = partial(pack, hidden_ref, packs, far).astype(BF16)
-    low_ref[...] = partial(pack, hidden_ref, packs, chip_at(chips, 1 - chips // 2)).astype(BF16)
+    low_ref[...] = partial(pack, hidden_ref, packs, chip_across(chips, 1 - chips // 2)).astype(BF16)
 
 
 def down_kernel(pack, chips, steps, hidden_ref, own_ref, other_ref, *outs):
     for step, out_ref in zip(steps, outs):
-        out_ref[...] = partial(pack, hidden_ref, (own_ref, other_ref), chip_at(chips, step))
+        out_ref[...] = partial(pack, hidden_ref, (own_ref, other_ref), chip_across(chips, step))
 
 
 def add_kernel(part_ref, came_ref, out_ref):
@@ -256,10 +261,9 @@
     total = features * members
     held = blocks * half
 
-    def along(value, step):
-        pairs = [
-            (y * CORES + c, (y + step * (1 - 2 * c)) % chips * CORES + c) for y in range(chips) for c in range(CORES)
-        ]
+    def along(value, step, other=1):
+        pairs = [(y * CORES, (y + step) % chips * CORES) for y in range(chips)]
+        pairs += [(y * CORES + 1, (y + step * other) % chips * CORES + 1) for y in range(chips)]
         return lax.ppermute(value, "tp", pairs)
 
     def across(value):
@@ -350,9 +354,9 @@
     )
     part = dict(zip(steps, parts))
     for step in range(last - 1, -1, -1):
-        ahead = along(ahead, 1)
+        ahead = along(ahead, 1, -1)
         if step:
-            back = along(back, -1)
+            back = along(back, -1, -1)
             ahead = joined(part[step], ahead)
             back = joined(part[1 - step], back) if step > 1 else back
     result = call(own_kernel, pltpu.VMEM((held, width), BF16), (part[0], ahead, back), held * width, 8)

time: 163 us -> 158 us (0.969)
  starting transfers between devices: 75.8 us -> 62.8 us
  blocking collectives: 58.4 us -> 65.2 us
    ppermute x14, starting transfers between devices: 49.5 us -> 41.9 us  [along(): return lax.ppermute(value, 'tp', pairs)]
    all_to_all x1, blocking collectives: 15.9 us -> 22.7 us  [on_device(): lax.all_to_all(result.reshape(blocks, half, width), 'sp', split_axis=0, c...]
    ppermute x2, starting transfers between devices: 25 us -> 19.7 us  [across(): return lax.ppermute(value, 'tp', [(t, t ^ 1) for t in range(members)])]
  transfers between devices with their start and end apart: 17 -> 17, of which waited for: 12 -> 11; matrix products, arithmetic and copies ran while one was open for 0% -> 0% of each run, Pallas kernels for 3% -> 3%
where the time goes in v4:
time: 158 us; the launch traced here: 157 us
  blocking collectives  65.2 us (41%)
  starting transfers between devices  62.8 us (40%)
  waiting for transfers between devices  19.6 us (12%)
  Pallas kernels  9.43 us (6%)
    ppermute x14, starting transfers between devices, along(): return lax.ppermute(value, 'tp', pairs)  41.9 us
    all_to_all x1, blocking collectives, on_device(): lax.all_to_all(sent.reshape(experts, half, width), 'sp', split_axis=0, co...  25.9 us
    all_to_all x1, blocking collectives, on_device(): lax.all_to_all(result.reshape(blocks, half, width), 'sp', split_axis=0, c...  22.7 us
    ppermute x2, starting transfers between devices, across(): return lax.ppermute(value, 'tp', [(t, t ^ 1) for t in range(members)])  19.7 us
    ppermute x14, waiting for transfers between devices, along(): return lax.ppermute(value, 'tp', pairs)  17.6 us
    all_gather x1, blocking collectives, on_device(): mixed = lax.all_gather(pooled, 'tp', axis=0, tiled=False)  16.6 us
    pallas_call x17, Pallas kernels, call(): pl.pallas_call(kernel, out_shape=out_shape, in_specs=[pl.BlockSpec(memory...  9.43 us
  transfers between devices with their start and end apart: 17, of which 11 were waited for; matrix products, arithmetic and copies ran while one was open for 0% of the time, Pallas kernels for 3%

profile of v4, /device:TPU:1, one launch (start us, length us, event | category | flops | bytes accessed | tf_op | source)
XLA Modules:
  0.0 157.4 jit_solution(8672268710960083684)
XLA Ops:
  0.0 2.2 %shard_map.109 = (bf16[6784,256]{1,0:T(8,128)(2,1)S(1)}, bf16[64,256]{1,0:T(8,128)(2,1)S(1)}, bf16[64,64]{1,0:T(8,128)(2,1)S(1)}, bf16[1,64]{1,0:T(2,128)(2,1)S(1)}, bf16[1,128]{1,0:T(2,128)(2,1)S(1)}) custom-call(bf16[2048,256]{1,0:T(8,128)(2,1)} %bitcast.24, bf16[2048,256]{1,0:T(8,128)(2,1)} %bitcast.25, bf16[256,2048]{1,0:T(8,128)(2,1)} %bitcast.26, ...), custom_call_target="tpu_custom_call" | custom-call | flops 889192448 | bytes 1736704 | tf_op jit(solution)/shard_map/pallas_call | solution.py:33
  2.2 8.7 %collective-permute-start.1 = (bf16[6784,256]{1,0:T(8,128)(2,1)S(1)}, bf16[6784,256]{1,0:T(8,128)(2,1)S(1)}, u32[]{:S(2)}, u32[]{:S(2)}) collective-permute-start(bf16[6784,256]{1,0:T(8,128)(2,1)S(1)} %get-tuple-element.36.own_ref), channel_id=1, source_target_pairs={{0,1},{1,0},{2,3},{3,2},{4,5},{5,4},{6,7},{7,6},{8,9},{9,8},{10,11... | collective-permute-start | bytes 10420232 | tf_op jit(solution)/shard_map/ppermute | solution.py:270
  13.6 16.6 %all-gather = bf16[1280,256]{1,0:T(8,128)(2,1)S(1)} all-gather(bf16[80,256]{1,0:T(8,128)(2,1)S(1)} %shard_map.110), channel_id=2, replica_groups=mesh['sp'=32,'tp'=16] {'tp'}, dimensions={0}, use_global_device_ids=true | all-gather | bytes 696320 | tf_op jit(solution)/shard_map/all_gather | solution.py:300
  31.0 25.9 %all_to_all.10 = bf16[32,16,256]{2,1,0:T(8,128)(2,1)S(1)} all-to-all(bf16[32,16,256]{2,1,0:T(8,128)(2,1)S(1)} %bitcast.19), channel_id=1, replica_groups=mesh['sp'=32,'tp'=16] {'sp'}, dimensions={0} | all-to-all | bytes 524288 | tf_op jit(solution)/shard_map/all_to_all | solution.py:312
  57.0 1.9 %collective-permute-start.2 = (bf16[512,256]{1,0:T(8,128)(2,1)S(1)}, bf16[512,256]{1,0:T(8,128)(2,1)S(1)}, u32[]{:S(2)}, u32[]{:S(2)}) collective-permute-start(bf16[512,256]{1,0:T(8,128)(2,1)S(1)} %bitcast.15), channel_id=1, source_target_pairs={{0,2},{2,4},{4,6},{6,8},{8,10},{10,12},{12,14},{14,0},{1,3},{3,5},... | collective-permute-start | bytes 786440 | tf_op jit(solution)/shard_map/ppermute | solution.py:267
  58.9 4.6 %collective-permute-start.6 = (bf16[512,256]{1,0:T(8,128)(2,1)S(1)}, bf16[512,256]{1,0:T(8,128)(2,1)S(1)}, u32[]{:S(2)}, u32[]{:S(2)}) collective-permute-start(bf16[512,256]{1,0:T(8,128)(2,1)S(1)} %bitcast.16), channel_id=1, source_target_pairs={{0,14},{2,0},{4,2},{6,4},{8,6},{10,8},{12,10},{14,12},{1,15},{3,1}... | collective-permute-start | bytes 786440 | tf_op jit(solution)/shard_map/ppermute | solution.py:267
  63.4 1.8 %collective-permute-done.2.p_ref = bf16[512,256]{1,0:T(8,128)(2,1)S(1)} collective-permute-done((bf16[512,256]{1,0:T(8,128)(2,1)S(1)}, bf16[512,256]{1,0:T(8,128)(2,1)S(1)}, u32[]{:S(2)}, u32[]{:S(2)}) %collective-permute-start.2) | collective-permute-done | bytes 262176 | tf_op jit(solution)/shard_map/ppermute | solution.py:267
  65.3 1.9 %collective-permute-start.3 = (bf16[512,256]{1,0:T(8,128)(2,1)S(1)}, bf16[512,256]{1,0:T(8,128)(2,1)S(1)}, u32[]{:S(2)}, u32[]{:S(2)}) collective-permute-start(bf16[512,256]{1,0:T(8,128)(2,1)S(1)} %collective-permute-done.2.p_ref), channel_id=1, source_target_pairs={{0,2},{2,4},{4,6},{6,8},{8,10},{10,12},{12,14},{14,0},{1,3},{3,5},... | collective-permute-start | bytes 786440 | tf_op jit(solution)/shard_map/ppermute | solution.py:267
  67.2 4.6 %collective-permute-start.7 = (bf16[512,256]{1,0:T(8,128)(2,1)S(1)}, bf16[512,256]{1,0:T(8,128)(2,1)S(1)}, u32[]{:S(2)}, u32[]{:S(2)}) collective-permute-start(bf16[512,256]{1,0:T(8,128)(2,1)S(1)} %collective-permute-done.6.m_ref), channel_id=1, source_target_pairs={{0,14},{2,0},{4,2},{6,4},{8,6},{10,8},{12,10},{14,12},{1,15},{3,1}... | collective-permute-start | bytes 786440 | tf_op jit(solution)/shard_map/ppermute | solution.py:267
  73.6 1.9 %collective-permute-start.4 = (bf16[512,256]{1,0:T(8,128)(2,1)S(1)}, bf16[512,256]{1,0:T(8,128)(2,1)S(1)}, u32[]{:S(2)}, u32[]{:S(2)}) collective-permute-start(bf16[512,256]{1,0:T(8,128)(2,1)S(1)} %collective-permute-done.3.p_ref), channel_id=1, source_target_pairs={{0,2},{2,4},{4,6},{6,8},{8,10},{10,12},{12,14},{14,0},{1,3},{3,5},... | collective-permute-start | bytes 786440 | tf_op jit(solution)/shard_map/ppermute | solution.py:267
  75.5 4.6 %collective-permute-start.8 = (bf16[512,256]{1,0:T(8,128)(2,1)S(1)}, bf16[512,256]{1,0:T(8,128)(2,1)S(1)}, u32[]{:S(2)}, u32[]{:S(2)}) collective-permute-start(bf16[512,256]{1,0:T(8,128)(2,1)S(1)} %collective-permute-done.7.m_ref), channel_id=1, source_target_pairs={{0,14},{2,0},{4,2},{6,4},{8,6},{10,8},{12,10},{14,12},{1,15},{3,1}... | collective-permute-start | bytes 786440 | tf_op jit(solution)/shard_map/ppermute | solution.py:267
  81.9 1.9 %collective-permute-start.5 = (bf16[512,256]{1,0:T(8,128)(2,1)S(1)}, bf16[512,256]{1,0:T(8,128)(2,1)S(1)}, u32[]{:S(2)}, u32[]{:S(2)}) collective-permute-start(bf16[512,256]{1,0:T(8,128)(2,1)S(1)} %collective-permute-done.4.p_ref), channel_id=1, source_target_pairs={{0,2},{2,4},{4,6},{6,8},{8,10},{10,12},{12,14},{14,0},{1,3},{3,5},... | collective-permute-start | bytes 786440 | tf_op jit(solution)/shard_map/ppermute | solution.py:267
  86.5 3.7 %collective-permute-done.5.p_ref = bf16[512,256]{1,0:T(8,128)(2,1)S(1)} collective-permute-done((bf16[512,256]{1,0:T(8,128)(2,1)S(1)}, bf16[512,256]{1,0:T(8,128)(2,1)S(1)}, u32[]{:S(2)}, u32[]{:S(2)}) %collective-permute-start.5) | collective-permute-done | bytes 262176 | tf_op jit(solution)/shard_map/ppermute | solution.py:267
  91.2 1.9 %collective-permute-start.9 = (bf16[512,256]{1,0:T(8,128)(2,1)S(1)}, bf16[512,256]{1,0:T(8,128)(2,1)S(1)}, u32[]{:S(2)}, u32[]{:S(2)}) collective-permute-start(bf16[512,256]{1,0:T(8,128)(2,1)S(1)} %get-tuple-element.53), channel_id=1, source_target_pairs={{0,2},{2,4},{4,6},{6,8},{8,10},{10,12},{12,14},{14,0},{1,15},{3,1}... | collective-permute-start | bytes 786440 | tf_op jit(solution)/shard_map/ppermute | solution.py:267
  93.1 3.4 %collective-permute-start.13 = (bf16[512,256]{1,0:T(8,128)(2,1)S(1)}, bf16[512,256]{1,0:T(8,128)(2,1)S(1)}, u32[]{:S(2)}, u32[]{:S(2)}) collective-permute-start(bf16[512,256]{1,0:T(8,128)(2,1)S(1)} %get-tuple-element.56), channel_id=1, source_target_pairs={{0,14},{2,0},{4,2},{6,4},{8,6},{10,8},{12,10},{14,12},{1,3},{3,5},... | collective-permute-start | bytes 786440 | tf_op jit(solution)/shard_map/ppermute | solution.py:267
  98.4 3.1 %collective-permute-start.10 = (bf16[512,256]{1,0:T(8,128)(2,1)S(1)}, bf16[512,256]{1,0:T(8,128)(2,1)S(1)}, u32[]{:S(2)}, u32[]{:S(2)}) collective-permute-start(bf16[512,256]{1,0:T(8,128)(2,1)S(1)} %shard_map.118), channel_id=1, source_target_pairs={{0,2},{2,4},{4,6},{6,8},{8,10},{10,12},{12,14},{14,0},{1,15},{3,1}... | collective-permute-start | bytes 786440 | tf_op jit(solution)/shard_map/ppermute | solution.py:267
  101.6 2.2 %collective-permute-start.14 = (bf16[512,256]{1,0:T(8,128)(2,1)S(1)}, bf16[512,256]{1,0:T(8,128)(2,1)S(1)}, u32[]{:S(2)}, u32[]{:S(2)}) collective-permute-start(bf16[512,256]{1,0:T(8,128)(2,1)S(1)} %shard_map.121), channel_id=1, source_target_pairs={{0,14},{2,0},{4,2},{6,4},{8,6},{10,8},{12,10},{14,12},{1,3},{3,5},... | collective-permute-start | bytes 786440 | tf_op jit(solution)/shard_map/ppermute | solution.py:267
  103.7 2.7 %collective-permute-done.10.came_ref = bf16[512,256]{1,0:T(8,128)(2,1)S(1)} collective-permute-done((bf16[512,256]{1,0:T(8,128)(2,1)S(1)}, bf16[512,256]{1,0:T(8,128)(2,1)S(1)}, u32[]{:S(2)}, u32[]{:S(2)}) %collective-permute-start.10) | collective-permute-done | bytes 262176 | tf_op jit(solution)/shard_map/ppermute | solution.py:267
  106.5 3.4 %collective-permute-start.11 = (bf16[512,256]{1,0:T(8,128)(2,1)S(1)}, bf16[512,256]{1,0:T(8,128)(2,1)S(1)}, u32[]{:S(2)}, u32[]{:S(2)}) collective-permute-start(bf16[512,256]{1,0:T(8,128)(2,1)S(1)} %shard_map.119), channel_id=1, source_target_pairs={{0,2},{2,4},{4,6},{6,8},{8,10},{10,12},{12,14},{14,0},{1,15},{3,1}... | collective-permute-start | bytes 786440 | tf_op jit(solution)/shard_map/ppermute | solution.py:267
  110.0 1.9 %collective-permute-start.15 = (bf16[512,256]{1,0:T(8,128)(2,1)S(1)}, bf16[512,256]{1,0:T(8,128)(2,1)S(1)}, u32[]{:S(2)}, u32[]{:S(2)}) collective-permute-start(bf16[512,256]{1,0:T(8,128)(2,1)S(1)} %shard_map.122), channel_id=1, source_target_pairs={{0,14},{2,0},{4,2},{6,4},{8,6},{10,8},{12,10},{14,12},{1,3},{3,5},... | collective-permute-start | bytes 786440 | tf_op jit(solution)/shard_map/ppermute | solution.py:267
  113.6 4.6 %collective-permute-start.12 = (bf16[512,256]{1,0:T(8,128)(2,1)S(1)}, bf16[512,256]{1,0:T(8,128)(2,1)S(1)}, u32[]{:S(2)}, u32[]{:S(2)}) collective-permute-start(bf16[512,256]{1,0:T(8,128)(2,1)S(1)} %shard_map.120), channel_id=1, source_target_pairs={{0,2},{2,4},{4,6},{6,8},{8,10},{10,12},{12,14},{14,0},{1,15},{3,1}... | collective-permute-start | bytes 786440 | tf_op jit(solution)/shard_map/ppermute | solution.py:267
  119.3 2.3 %collective-permute-done.12.p_ref = bf16[512,256]{1,0:T(8,128)(2,1)S(1)} collective-permute-done((bf16[512,256]{1,0:T(8,128)(2,1)S(1)}, bf16[512,256]{1,0:T(8,128)(2,1)S(1)}, u32[]{:S(2)}, u32[]{:S(2)}) %collective-permute-start.12) | collective-permute-done | bytes 262176 | tf_op jit(solution)/shard_map/ppermute | solution.py:267
  121.6 22.7 %all_to_all.11 = bf16[32,16,256]{2,1,0:T(8,128)(2,1)S(1)} all-to-all(bf16[32,16,256]{2,1,0:T(8,128)(2,1)S(1)} %bitcast.18), channel_id=1, replica_groups=mesh['sp'=32,'tp'=16] {'sp'}, dimensions={0} | all-to-all | bytes 524288 | tf_op jit(solution)/shard_map/all_to_all | solution.py:363
  144.8 10.9 %collective-permute-start.16 = (f32[256,128]{1,0:T(8,128)S(1)}, f32[256,128]{1,0:T(8,128)S(1)}, u32[]{:S(2)}, u32[]{:S(2)}) collective-permute-start(f32[256,128]{1,0:T(8,128)S(1)} %get-tuple-element.58), channel_id=1, source_target_pairs={{0,1},{1,0},{2,3},{3,2},{4,5},{5,4},{6,7},{7,6},{8,9},{9,8},{10,11... | collective-permute-start | bytes 393224 | tf_op jit(solution)/shard_map/ppermute | solution.py:270
  (36 shorter events, 17.6 us)
Async XLA Ops:
  0.0 11.0 %copy-start.2 = (bf16[256,64]{0,1:T(8,128)(2,1)S(1)}, bf16[256,64]{0,1:T(8,128)(2,1)}, u32[]{:S(2)}) copy-start(bf16[256,64]{0,1:T(8,128)(2,1)} %param.11) | copy-start | bytes 98308
  0.0 30.2 %copy-start = (s32[256,2]{0,1:T(2,128)S(1)}, s32[256,2]{0,1:T(2,128)}, u32[]{:S(2)}) copy-start(s32[256,2]{0,1:T(2,128)} %param.17) | copy-start | bytes 6148
  2.2 28.0 %collective-permute-start.1 = (bf16[6784,256]{1,0:T(8,128)(2,1)S(1)}, bf16[6784,256]{1,0:T(8,128)(2,1)S(1)}, u32[]{:S(2)}, u32[]{:S(2)}) collective-permute-start(bf16[6784,256]{1,0:T(8,128)(2,1)S(1)} %get-tuple-element.36.own_ref), channel_id=1, source_target_pairs={{0,1},{1,0},{2,3},{3,2},{4,5},{5,4},{6,7},{7,6},{8,9},{9,8},{10,11... | collective-permute-start | bytes 10420232 | tf_op jit(solution)/shard_map/ppermute | solution.py:270
  11.0 2.3 %collective-permute-start = (bf16[64,256]{1,0:T(8,128)(2,1)S(1)}, bf16[64,256]{1,0:T(8,128)(2,1)S(1)}, u32[]{:S(2)}, u32[]{:S(2)}) collective-permute-start(bf16[64,256]{1,0:T(8,128)(2,1)S(1)} %bitcast.28), channel_id=1, source_target_pairs={{0,16},{16,32},{32,48},{48,64},{64,80},{80,96},{96,112},{112,128},... | collective-permute-start | bytes 98312 | tf_op jit(solution)/shard_map/ppermute | solution.py:275
  57.0 8.3 %collective-permute-start.2 = (bf16[512,256]{1,0:T(8,128)(2,1)S(1)}, bf16[512,256]{1,0:T(8,128)(2,1)S(1)}, u32[]{:S(2)}, u32[]{:S(2)}) collective-permute-start(bf16[512,256]{1,0:T(8,128)(2,1)S(1)} %bitcast.15), channel_id=1, source_target_pairs={{0,2},{2,4},{4,6},{6,8},{8,10},{10,12},{12,14},{14,0},{1,3},{3,5},... | collective-permute-start | bytes 786440 | tf_op jit(solution)/shard_map/ppermute | solution.py:267
  58.9 8.3 %collective-permute-start.6 = (bf16[512,256]{1,0:T(8,128)(2,1)S(1)}, bf16[512,256]{1,0:T(8,128)(2,1)S(1)}, u32[]{:S(2)}, u32[]{:S(2)}) collective-permute-start(bf16[512,256]{1,0:T(8,128)(2,1)S(1)} %bitcast.16), channel_id=1, source_target_pairs={{0,14},{2,0},{4,2},{6,4},{8,6},{10,8},{12,10},{14,12},{1,15},{3,1}... | collective-permute-start | bytes 786440 | tf_op jit(solution)/shard_map/ppermute | solution.py:267
  65.3 8.3 %collective-permute-start.3 = (bf16[512,256]{1,0:T(8,128)(2,1)S(1)}, bf16[512,256]{1,0:T(8,128)(2,1)S(1)}, u32[]{:S(2)}, u32[]{:S(2)}) collective-permute-start(bf16[512,256]{1,0:T(8,128)(2,1)S(1)} %collective-permute-done.2.p_ref), channel_id=1, source_target_pairs={{0,2},{2,4},{4,6},{6,8},{8,10},{10,12},{12,14},{14,0},{1,3},{3,5},... | collective-permute-start | bytes 786440 | tf_op jit(solution)/shard_map/ppermute | solution.py:267
  67.2 8.3 %collective-permute-start.7 = (bf16[512,256]{1,0:T(8,128)(2,1)S(1)}, bf16[512,256]{1,0:T(8,128)(2,1)S(1)}, u32[]{:S(2)}, u32[]{:S(2)}) collective-permute-start(bf16[512,256]{1,0:T(8,128)(2,1)S(1)} %collective-permute-done.6.m_ref), channel_id=1, source_target_pairs={{0,14},{2,0},{4,2},{6,4},{8,6},{10,8},{12,10},{14,12},{1,15},{3,1}... | collective-permute-start | bytes 786440 | tf_op jit(solution)/shard_map/ppermute | solution.py:267
  73.6 8.3 %collective-permute-start.4 = (bf16[512,256]{1,0:T(8,128)(2,1)S(1)}, bf16[512,256]{1,0:T(8,128)(2,1)S(1)}, u32[]{:S(2)}, u32[]{:S(2)}) collective-permute-start(bf16[512,256]{1,0:T(8,128)(2,1)S(1)} %collective-permute-done.3.p_ref), channel_id=1, source_target_pairs={{0,2},{2,4},{4,6},{6,8},{8,10},{10,12},{12,14},{14,0},{1,3},{3,5},... | collective-permute-start | bytes 786440 | tf_op jit(solution)/shard_map/ppermute | solution.py:267
  75.5 10.2 %collective-permute-start.8 = (bf16[512,256]{1,0:T(8,128)(2,1)S(1)}, bf16[512,256]{1,0:T(8,128)(2,1)S(1)}, u32[]{:S(2)}, u32[]{:S(2)}) collective-permute-start(bf16[512,256]{1,0:T(8,128)(2,1)S(1)} %collective-permute-done.7.m_ref), channel_id=1, source_target_pairs={{0,14},{2,0},{4,2},{6,4},{8,6},{10,8},{12,10},{14,12},{1,15},{3,1}... | collective-permute-start | bytes 786440 | tf_op jit(solution)/shard_map/ppermute | solution.py:267
  81.9 8.3 %collective-permute-start.5 = (bf16[512,256]{1,0:T(8,128)(2,1)S(1)}, bf16[512,256]{1,0:T(8,128)(2,1)S(1)}, u32[]{:S(2)}, u32[]{:S(2)}) collective-permute-start(bf16[512,256]{1,0:T(8,128)(2,1)S(1)} %collective-permute-done.4.p_ref), channel_id=1, source_target_pairs={{0,2},{2,4},{4,6},{6,8},{8,10},{10,12},{12,14},{14,0},{1,3},{3,5},... | collective-permute-start | bytes 786440 | tf_op jit(solution)/shard_map/ppermute | solution.py:267
  91.2 7.1 %collective-permute-start.9 = (bf16[512,256]{1,0:T(8,128)(2,1)S(1)}, bf16[512,256]{1,0:T(8,128)(2,1)S(1)}, u32[]{:S(2)}, u32[]{:S(2)}) collective-permute-start(bf16[512,256]{1,0:T(8,128)(2,1)S(1)} %get-tuple-element.53), channel_id=1, source_target_pairs={{0,2},{2,4},{4,6},{6,8},{8,10},{10,12},{12,14},{14,0},{1,15},{3,1}... | collective-permute-start | bytes 786440 | tf_op jit(solution)/shard_map/ppermute | solution.py:267
  93.1 8.4 %collective-permute-start.13 = (bf16[512,256]{1,0:T(8,128)(2,1)S(1)}, bf16[512,256]{1,0:T(8,128)(2,1)S(1)}, u32[]{:S(2)}, u32[]{:S(2)}) collective-permute-start(bf16[512,256]{1,0:T(8,128)(2,1)S(1)} %get-tuple-element.56), channel_id=1, source_target_pairs={{0,14},{2,0},{4,2},{6,4},{8,6},{10,8},{12,10},{14,12},{1,3},{3,5},... | collective-permute-start | bytes 786440 | tf_op jit(solution)/shard_map/ppermute | solution.py:267
  98.4 8.0 %collective-permute-start.10 = (bf16[512,256]{1,0:T(8,128)(2,1)S(1)}, bf16[512,256]{1,0:T(8,128)(2,1)S(1)}, u32[]{:S(2)}, u32[]{:S(2)}) collective-permute-start(bf16[512,256]{1,0:T(8,128)(2,1)S(1)} %shard_map.118), channel_id=1, source_target_pairs={{0,2},{2,4},{4,6},{6,8},{8,10},{10,12},{12,14},{14,0},{1,15},{3,1}... | collective-permute-start | bytes 786440 | tf_op jit(solution)/shard_map/ppermute | solution.py:267
  101.6 8.3 %collective-permute-start.14 = (bf16[512,256]{1,0:T(8,128)(2,1)S(1)}, bf16[512,256]{1,0:T(8,128)(2,1)S(1)}, u32[]{:S(2)}, u32[]{:S(2)}) collective-permute-start(bf16[512,256]{1,0:T(8,128)(2,1)S(1)} %shard_map.121), channel_id=1, source_target_pairs={{0,14},{2,0},{4,2},{6,4},{8,6},{10,8},{12,10},{14,12},{1,3},{3,5},... | collective-permute-start | bytes 786440 | tf_op jit(solution)/shard_map/ppermute | solution.py:267
  106.5 37.8 %copy-start.1 = (f32[256,2]{0,1:T(2,128)S(1)}, f32[256,2]{0,1:T(2,128)}, u32[]{:S(2)}) copy-start(f32[256,2]{0,1:T(2,128)} %param.18) | copy-start | bytes 6148
  106.5 7.1 %collective-permute-start.11 = (bf16[512,256]{1,0:T(8,128)(2,1)S(1)}, bf16[512,256]{1,0:T(8,128)(2,1)S(1)}, u32[]{:S(2)}, u32[]{:S(2)}) collective-permute-start(bf16[512,256]{1,0:T(8,128)(2,1)S(1)} %shard_map.119), channel_id=1, source_target_pairs={{0,2},{2,4},{4,6},{6,8},{8,10},{10,12},{12,14},{14,0},{1,15},{3,1}... | collective-permute-start | bytes 786440 | tf_op jit(solution)/shard_map/ppermute | solution.py:267
  110.0 9.3 %collective-permute-start.15 = (bf16[512,256]{1,0:T(8,128)(2,1)S(1)}, bf16[512,256]{1,0:T(8,128)(2,1)S(1)}, u32[]{:S(2)}, u32[]{:S(2)}) collective-permute-start(bf16[512,256]{1,0:T(8,128)(2,1)S(1)} %shard_map.122), channel_id=1, source_target_pairs={{0,14},{2,0},{4,2},{6,4},{8,6},{10,8},{12,10},{14,12},{1,3},{3,5},... | collective-permute-start | bytes 786440 | tf_op jit(solution)/shard_map/ppermute | solution.py:267
  113.6 7.9 %collective-permute-start.12 = (bf16[512,256]{1,0:T(8,128)(2,1)S(1)}, bf16[512,256]{1,0:T(8,128)(2,1)S(1)}, u32[]{:S(2)}, u32[]{:S(2)}) collective-permute-start(bf16[512,256]{1,0:T(8,128)(2,1)S(1)} %shard_map.120), channel_id=1, source_target_pairs={{0,2},{2,4},{4,6},{6,8},{8,10},{10,12},{12,14},{14,0},{1,15},{3,1}... | collective-permute-start | bytes 786440 | tf_op jit(solution)/shard_map/ppermute | solution.py:267
  144.8 11.9 %collective-permute-start.16 = (f32[256,128]{1,0:T(8,128)S(1)}, f32[256,128]{1,0:T(8,128)S(1)}, u32[]{:S(2)}, u32[]{:S(2)}) collective-permute-start(f32[256,128]{1,0:T(8,128)S(1)} %get-tuple-element.58), channel_id=1, source_target_pairs={{0,1},{1,0},{2,3},{3,2},{4,5},{5,4},{6,7},{7,6},{8,9},{9,8},{10,11... | collective-permute-start | bytes 393224 | tf_op jit(solution)/shard_map/ppermute | solution.py:270

commit v5 on v4

--- a/solution.py
+++ b/solution.py
@@ -33,7 +33,7 @@
     return pl.pallas_call(
         kernel,
         out_shape=out_shape,
-        in_specs=[pl.BlockSpec(memory_space=space)] * len(args),
+        in_specs=[pl.BlockSpec(memory_space=s) for s in (space if isinstance(space, tuple) else (space,) * len(args))],
         scratch_shapes=scratch,
         out_specs=jax.tree.map(lambda _: pl.BlockSpec(memory_space=pltpu.VMEM), out_shape),
         compiler_params=pltpu.CompilerParams(vmem_limit_bytes=mib * MIB),
@@ -57,11 +57,14 @@
     pooled = (total / count - x.astype(F32)).astype(BF16)
     eye = iota((width, width), 0) == iota((width, width), 1)
     gain = jnp.sum(jnp.where(eye, gain_ref[...].astype(F32), 0.0), axis=1, keepdims=True)
-    out_ref[:width, :] = (mm(w_ref[...], pooled, 0, 0) * gain).astype(BF16)
+    mixed = (mm(w_ref[...], pooled, 0, 0) * gain).astype(BF16)
     features = norm_ref.shape[1]
-    tail = out_ref.shape[0] - width
-    out_ref[width:, :features] = jnp.broadcast_to(norm_ref[...].astype(F32), (tail, features)).astype(BF16)
-    out_ref[width:, features:] = jnp.zeros((tail, out_ref.shape[1] - features), BF16)
+    tail = out_ref.shape[1] - width
+    norm = jnp.broadcast_to(norm_ref[...].astype(F32), (tail, features)).astype(BF16)
+    for i in range(out_ref.shape[0]):
+        out_ref[i, :width, :] = mixed
+        out_ref[i, width:, :features] = norm
+        out_ref[i, width:, features:] = jnp.zeros((tail, rows - features), BF16)
 
 
 def row_slots(routes_ref, experts, capacity):
@@ -92,55 +95,86 @@
         self.width = width
 
 
-def prep_kernel(pack, gate, up, down, project, resid, x, w, gain, norm, out, x_out, w_out, gain_out, norm_out, sems):
+def copy_all(pairs, sems):
+    copies = [pltpu.make_async_copy(a, b, sems.at[i]) for i, (a, b) in enumerate(pairs)]
+    for copy in copies:
+        copy.start()
+    for copy in copies:
+        copy.wait()
+
+
+def fetch_kernel(source, out, sem):
+    copy = pltpu.make_async_copy(source.at[: out.shape[0], :], out, sem)
+    copy.start()
+    copy.wait()
+
+
+def load_kernel(count, *refs):
+    copy_all(list(zip(refs[:count], refs[count : 2 * count])), refs[2 * count])
+
+
+def prep_kernel(pack, gate, up, down, project, resid, out, sems):
     width, features = pack.width, project.shape[1]
     units = down.shape[0]
-    pairs = [(x, x_out), (w, w_out), (gain, gain_out), (norm, norm_out)]
-    for base, source in ((pack.project, project), (pack.resid, resid)):
-        half = source.shape[0] // 2
-        for i in range(2):
-            pairs.append(
-                (source.at[i * half : (i + 1) * half, :],
-                 out.at[base : base + half, i * features : (i + 1) * features])
-            )
+    pairs = []
+    for t in range(project.shape[0] // GSIZE):
+        base, c = pack.project + t // CORES * GSIZE, t % CORES
+        pairs.append(
+            (project.at[t * GSIZE : (t + 1) * GSIZE, :],
+             out.at[base : base + GSIZE, c * features : (c + 1) * features])
+        )
+    half = resid.shape[0] // 2
+    for i in range(2):
+        pairs.append(
+            (resid.at[i * half : (i + 1) * half, :],
+             out.at[pack.resid : pack.rows, i * features : (i + 1) * features])
+        )
     pairs.append((gate, out.at[pack.gate : pack.up, :]))
     pairs.append((up, out.at[pack.up : pack.down, :]))
     for i in range(down.shape[1] // width):
         pairs.append(
             (down.at[:, i * width : (i + 1) * width], out.at[pack.down + i * units : pack.down + (i + 1) * units, :])
         )
-    copies = [pltpu.make_async_copy(a, b, sems.at[i]) for i, (a, b) in enumerate(pairs)]
-    for copy in copies:
-        copy.start()
-    for copy in copies:
-        copy.wait()
-
-
-def dispatch_kernel(pack, experts, capacity, mixed_ref, own_ref, other_ref, routes_ref, stream_ref, gain_ref, out_ref):
+    copy_all(pairs, sems)
+
+
+def dispatch_kernel(
+    pack, experts, capacity, near_ref, far_ref, own_ref, other_ref, routes_ref, stream_ref, gain_ref, out_ref,
+    fetched_ref, sem,
+):
+    fetch = pltpu.make_async_copy(other_ref.at[pack.project : pack.rows, :], fetched_ref, sem)
+    fetch.start()
     core = lax.rem(lax.axis_index("tp"), CORES)
-    members, _, rows = mixed_ref.shape
+    chips, _, rows = near_ref.shape
     features = stream_ref.shape[1]
-    mixed = mixed_ref[:, :GSIZE, :].reshape(members * GSIZE, rows)
-    deep = members * GSIZE // 2
-    streams = []
-    for ref in (own_ref, other_ref):
-        halves = [ref[pack.project : pack.resid, i * features : (i + 1) * features] for i in range(2)]
-        projected = mm(mixed[:deep], halves[0], 0, 0) + mm(mixed[deep:], halves[1], 0, 0)
-        resid = jnp.concatenate(
-            [ref[pack.resid : pack.rows, i * features : (i + 1) * features] for i in range(2)], axis=0
-        )
-        streams.append((resid.astype(F32) + projected).astype(BF16))
-    own, other = streams
+
+    def by_core(mine, others):
+        return jnp.where(core == 0, mine, others), jnp.where(core == 0, others, mine)
+
+    near = near_ref[:, :GSIZE, :].reshape(chips * GSIZE, rows)
+    far = far_ref[:, :GSIZE, :].reshape(chips * GSIZE, rows)
+
+    def stream_of(ref, base):
+        deep, end = base + pack.resid - pack.project, base + pack.rows - pack.project
+        halves = [(ref[base:deep, lanes], ref[deep:end, lanes]) for lanes in (slice(0, features), slice(features, None))]
+        mine, others = by_core(halves[0][0], halves[1][0])
+        projected = mm(near, mine, 0, 0) + mm(far, others, 0, 0)
+        resid = jnp.concatenate([halves[0][1], halves[1][1]], axis=0)
+        return (resid.astype(F32) + projected).astype(BF16)
+
+    own = stream_of(own_ref, pack.project)
     stream_ref[...] = own
-    for t in range(members):
-        y, c = divmod(t, CORES)
-        gain_ref[y, :, c * features : (c + 1) * features] = mixed_ref[t, GSIZE : GSIZE + 8, :features].astype(F32)
+    for y in range(chips):
+        gains = (ref[y, GSIZE : GSIZE + 8, :features].astype(F32) for ref in (near_ref, far_ref))
+        gain_ref[y, :, :features], gain_ref[y, :, features:] = by_core(*gains)
     slots = row_slots(routes_ref, experts, capacity)
     ids = slot_ids((out_ref.shape[0], rows), 0, capacity, core)
     hit = (slots[0] == ids) | (slots[1] == ids)
     chosen = jnp.where(hit, 1.0, 0.0).astype(BF16)
-    out_ref[:, :features] = mm(chosen, jnp.where(core == 0, own, other)).astype(BF16)
-    out_ref[:, features:] = mm(chosen, jnp.where(core == 0, other, own)).astype(BF16)
+    fetch.wait()
+    left, right = by_core(own, stream_of(fetched_ref, 0))
+    out_ref[:, :features] = mm(chosen, left).astype(BF16)
+    out_ref[:, features:] = mm(chosen, right).astype(BF16)
 
 
 def add_chunk(pack, x, chip, gain_ref, packs, acc_ref, square_ref, first=False):
@@ -275,29 +309,42 @@
     before = lax.ppermute(
         pool_input.T, "sp", [(s, s + 1) for s in range(blocks - 1)]
     )
+
+    def in_hbm(*values):
+        return tuple(pltpu.with_memory_space_constraint(v, pltpu.HBM) for v in values)
+
     small = (pool_input.T, pool_weight[0], pool_gain.reshape(1, channels), norm_gain.reshape(1, features))
-    own, *small = call(
-        functools.partial(prep_kernel, pack),
-        (pltpu.VMEM((pack.rows, width), BF16), *(pltpu.VMEM(v.shape, v.dtype) for v in small)),
-        tuple(
-            pltpu.with_memory_space_constraint(v, pltpu.HBM)
-            for v in (expert_gate[0], expert_up[0], expert_down[0], out_weight, resid, *small)
-        ),
-        pack.rows * width * 512,
+    small = call(
+        functools.partial(load_kernel, len(small)),
+        tuple(pltpu.VMEM(v.shape, v.dtype) for v in small),
+        in_hbm(*small),
+        tok_rows * 512,
         8,
-        space=pltpu.HBM,
-        scratch=[pltpu.SemaphoreType.DMA((10 + chips,))],
-    )
-    other = across(own)
-    packs = (own, other)
+        space=pl.ANY,
+        scratch=[pltpu.SemaphoreType.DMA((len(small),))],
+    )
     pooled = call(
         pool_kernel,
-        shape((GSIZE + 16, tok_rows), BF16),
+        shape((chips, GSIZE + 16, tok_rows), BF16),
         (before, *small),
         tok_rows * tok_rows * channels * 2,
         8,
     )
-    mixed = lax.all_gather(pooled, "tp", axis=0, tiled=False)
+    near = lax.all_to_all(
+        pooled, "tp", split_axis=0, concat_axis=0, tiled=True,
+        axis_index_groups=[[y * CORES + c for y in range(chips)] for c in range(CORES)],
+    )
+    (own,) = call(
+        functools.partial(prep_kernel, pack),
+        (pltpu.VMEM((pack.rows, width), BF16),),
+        in_hbm(expert_gate[0], expert_up[0], expert_down[0], out_weight, resid),
+        pack.rows * width * 512,
+        8,
+        space=pl.ANY,
+        scratch=[pltpu.SemaphoreType.DMA((4 + members + chips,))],
+    )
+    other = across(own)
+    far = across(near)
     stored, gains, sent = call(
         functools.partial(dispatch_kernel, pack, experts, capacity),
         (
@@ -305,14 +352,26 @@
             shape((chips, 8, width), F32),
             shape((experts * half, width), BF16),
         ),
-        (mixed, *packs, routes.T),
+        (near, far, own, *in_hbm(other), routes.T),
         2 * experts * half * width * tok_rows,
         16,
+        space=(pltpu.VMEM, pltpu.VMEM, pltpu.VMEM, pl.ANY, pltpu.VMEM),
+        scratch=[pltpu.VMEM((pack.rows - pack.project, width), BF16), pltpu.SemaphoreType.DMA(())],
     )
     x = lax.all_to_all(
         sent.reshape(experts, half, width), "sp", split_axis=0, concat_axis=0, tiled=True
     ).reshape(held, width)
 
+    (fetched,) = call(
+        fetch_kernel,
+        (pltpu.VMEM((pack.project, width), BF16),),
+        in_hbm(other),
+        pack.rows * width * 512,
+        8,
+        space=pl.ANY,
+        scratch=[pltpu.SemaphoreType.DMA(())],
+    )
+    packs = (own, fetched)
     acc_shape = (shape((held, 4 * units), F32), shape((held, 128), F32))
     chunk_flops = 2 * held * width * 4 * units
     acc, square = call(

time: 158 us -> 167 us (1.057)
  starting transfers between devices: 62.8 us -> 74 us
  blocking collectives: 65.2 us -> 59.9 us
  Pallas kernels: 9.43 us -> 13.3 us
  waiting for transfers between devices: 19.6 us -> 16.8 us
  local copies, waits for them, and re-layouts: 0.01 us -> 1.74 us
    all_gather x1 -> x0, blocking collectives: 16.6 us -> none  [on_device(): mixed = lax.all_gather(pooled, 'tp', axis=0, tiled=False)]
    all_to_all x0 -> x1, blocking collectives: none -> 14.8 us  [on_device(): lax.all_to_all(pooled, 'tp', split_axis=0, concat_axis=0, tiled=True, axi...]
    ppermute x2 -> x3, starting transfers between devices: 19.7 us -> 28.3 us  [across(): return lax.ppermute(value, 'tp', [(t, t ^ 1) for t in range(members)])]
    pallas_call x17 -> x19, Pallas kernels: 9.43 us -> 13.3 us  [call(): pl.pallas_call(kernel, out_shape=out_shape, in_specs=[pl.BlockSpec(memory...]
    ppermute x14, waiting for transfers between devices: 17.6 us -> 14.4 us  [along(): return lax.ppermute(value, 'tp', pairs)]
    all_to_all x1, blocking collectives: 22.7 us -> 19.5 us  [on_device(): lax.all_to_all(result.reshape(blocks, half, width), 'sp', split_axis=0, c...]
    ppermute x14, starting transfers between devices: 41.9 us -> 44.5 us  [along(): return lax.ppermute(value, 'tp', pairs)]
    unnamed x6 -> x8, local copies, waits for them, and re-layouts: 0.01 us -> 1.74 us
  transfers between devices with their start and end apart: 17 -> 18, of which waited for: 11 -> 14; matrix products, arithmetic and copies ran while one was open for 0% -> 0% of each run, Pallas kernels for 3% -> 4%
where the time goes in v5:
time: 167 us; the launch traced here: 166 us
  starting transfers between devices  74 us (44%)
  blocking collectives  59.9 us (36%)
  waiting for transfers between devices  16.8 us (10%)
  Pallas kernels  13.3 us (8%)
  local copies, waits for them, and re-layouts  1.74 us (1%)
    ppermute x14, starting transfers between devices, along(): return lax.ppermute(value, 'tp', pairs)  44.5 us
    ppermute x3, starting transfers between devices, across(): return lax.ppermute(value, 'tp', [(t, t ^ 1) for t in range(members)])  28.3 us
    all_to_all x1, blocking collectives, on_device(): lax.all_to_all(sent.reshape(experts, half, width), 'sp', split_axis=0, co...  25.6 us
    all_to_all x1, blocking collectives, on_device(): lax.all_to_all(result.reshape(blocks, half, width), 'sp', split_axis=0, c...  19.5 us
    all_to_all x1, blocking collectives, on_device(): lax.all_to_all(pooled, 'tp', split_axis=0, concat_axis=0, tiled=True, axi...  14.8 us
    ppermute x14, waiting for transfers between devices, along(): return lax.ppermute(value, 'tp', pairs)  14.4 us
    pallas_call x19, Pallas kernels, call(): pl.pallas_call(kernel, out_shape=out_shape, in_specs=[pl.BlockSpec(memory...  13.3 us
  transfers between devices with their start and end apart: 18, of which 14 were waited for; matrix products, arithmetic and copies ran while one was open for 0% of the time, Pallas kernels for 4%

profile of v5, /device:TPU:1, one launch (start us, length us, event | category | flops | bytes accessed | tf_op | source)
XLA Modules:
  0.0 166.0 jit_solution(15751701155674541203)
XLA Ops:
  0.0 2.3 %shard_map.111.own_ref = bf16[6784,256]{1,0:T(8,128)(2,1)S(1)} custom-call(bf16[2048,256]{1,0:T(8,128)(2,1)} %bitcast.22, bf16[2048,256]{1,0:T(8,128)(2,1)} %bitcast.23, bf16[256,2048]{1,0:T(8,128)(2,1)} %bitcast.24, bf16[1024,128]{1,0:T(8,128)(2,1)} %project.1, bf16[256,128]{1,0:T(8,128)(2,1)} %resid.1), custom_call_target="tpu_custom_call" | custom-call | flops 889192448 | bytes 1736704 | tf_op jit(solution)/shard_map/pallas_call | solution.py:33
  2.3 8.7 %collective-permute-start.2 = (bf16[6784,256]{1,0:T(8,128)(2,1)S(1)}, bf16[6784,256]{1,0:T(8,128)(2,1)S(1)}, u32[]{:S(2)}, u32[]{:S(2)}) collective-permute-start(bf16[6784,256]{1,0:T(8,128)(2,1)S(1)} %shard_map.111.own_ref), channel_id=1, source_target_pairs={{0,1},{1,0},{2,3},{3,2},{4,5},{5,4},{6,7},{7,6},{8,9},{9,8},{10,11... | collective-permute-start | bytes 10420232 | tf_op jit(solution)/shard_map/ppermute | solution.py:304
  13.7 14.8 %all_to_all.15.near_ref = bf16[8,80,256]{2,1,0:T(8,128)(2,1)S(1)} all-to-all(bf16[8,80,256]{2,1,0:T(8,128)(2,1)S(1)} %shard_map.110), channel_id=1, replica_groups={{0,2,4,6,8,10,12,14},{1,3,5,7,9,11,13,15},{16,18,20,22,24,26,28,30},{17..., dimensions={0} | all-to-all | bytes 655360 | tf_op jit(solution)/shard_map/all_to_all | solution.py:333
  28.4 4.5 %collective-permute-start.1 = (bf16[8,80,256]{2,1,0:T(8,128)(2,1)S(1)}, bf16[8,80,256]{2,1,0:T(8,128)(2,1)S(1)}, u32[]{:S(2)}, u32[]{:S(2)}) collective-permute-start(bf16[8,80,256]{2,1,0:T(8,128)(2,1)S(1)} %all_to_all.15.near_ref), channel_id=1, source_target_pairs={{0,1},{1,0},{2,3},{3,2},{4,5},{5,4},{6,7},{7,6},{8,9},{9,8},{10,11... | collective-permute-start | bytes 983048 | tf_op jit(solution)/shard_map/ppermute | solution.py:304
  35.9 1.9 %shard_map.112 = (bf16[256,128]{1,0:T(8,128)(2,1)S(1)}, f32[8,8,256]{2,1,0:T(8,128)S(1)}, bf16[512,256]{1,0:T(8,128)(2,1)S(1)}) custom-call(bf16[8,80,256]{2,1,0:T(8,128)(2,1)S(1)} %all_to_all.15.near_ref, bf16[8,80,256]{2,1,0:T(8,128)(2,1)S(1)} %collective-permute-done.1.far_ref, bf16[6784,256]{1,0:T(8,128)(2,1)S(1)} %shard_map.111.own_ref, ...), custom_call_target="tpu_custom_call" | custom-call | flops 67108864 | bytes 131072 | tf_op jit(solution)/shard_map/pallas_call | solution.py:33
  37.8 25.6 %all_to_all.16 = bf16[32,16,256]{2,1,0:T(8,128)(2,1)S(1)} all-to-all(bf16[32,16,256]{2,1,0:T(8,128)(2,1)S(1)} %bitcast.17), channel_id=1, replica_groups=mesh['sp'=32,'tp'=16] {'sp'}, dimensions={0} | all-to-all | bytes 524288 | tf_op jit(solution)/shard_map/all_to_all | solution.py:361
  63.5 2.2 %collective-permute-start.3 = (bf16[512,256]{1,0:T(8,128)(2,1)S(1)}, bf16[512,256]{1,0:T(8,128)(2,1)S(1)}, u32[]{:S(2)}, u32[]{:S(2)}) collective-permute-start(bf16[512,256]{1,0:T(8,128)(2,1)S(1)} %bitcast.14), channel_id=1, source_target_pairs={{0,2},{2,4},{4,6},{6,8},{8,10},{10,12},{12,14},{14,0},{1,3},{3,5},... | collective-permute-start | bytes 786440 | tf_op jit(solution)/shard_map/ppermute | solution.py:301
  65.6 4.3 %collective-permute-start.7 = (bf16[512,256]{1,0:T(8,128)(2,1)S(1)}, bf16[512,256]{1,0:T(8,128)(2,1)S(1)}, u32[]{:S(2)}, u32[]{:S(2)}) collective-permute-start(bf16[512,256]{1,0:T(8,128)(2,1)S(1)} %bitcast.15), channel_id=1, source_target_pairs={{0,14},{2,0},{4,2},{6,4},{8,6},{10,8},{12,10},{14,12},{1,15},{3,1}... | collective-permute-start | bytes 786440 | tf_op jit(solution)/shard_map/ppermute | solution.py:301
  70.0 2.2 %collective-permute-done.3.p_ref = bf16[512,256]{1,0:T(8,128)(2,1)S(1)} collective-permute-done((bf16[512,256]{1,0:T(8,128)(2,1)S(1)}, bf16[512,256]{1,0:T(8,128)(2,1)S(1)}, u32[]{:S(2)}, u32[]{:S(2)}) %collective-permute-start.3) | collective-permute-done | bytes 262176 | tf_op jit(solution)/shard_map/ppermute | solution.py:301
  72.1 1.9 %collective-permute-start.4 = (bf16[512,256]{1,0:T(8,128)(2,1)S(1)}, bf16[512,256]{1,0:T(8,128)(2,1)S(1)}, u32[]{:S(2)}, u32[]{:S(2)}) collective-permute-start(bf16[512,256]{1,0:T(8,128)(2,1)S(1)} %collective-permute-done.3.p_ref), channel_id=1, source_target_pairs={{0,2},{2,4},{4,6},{6,8},{8,10},{10,12},{12,14},{14,0},{1,3},{3,5},... | collective-permute-start | bytes 786440 | tf_op jit(solution)/shard_map/ppermute | solution.py:301
  74.0 4.6 %collective-permute-start.8 = (bf16[512,256]{1,0:T(8,128)(2,1)S(1)}, bf16[512,256]{1,0:T(8,128)(2,1)S(1)}, u32[]{:S(2)}, u32[]{:S(2)}) collective-permute-start(bf16[512,256]{1,0:T(8,128)(2,1)S(1)} %collective-permute-done.7.m_ref), channel_id=1, source_target_pairs={{0,14},{2,0},{4,2},{6,4},{8,6},{10,8},{12,10},{14,12},{1,15},{3,1}... | collective-permute-start | bytes 786440 | tf_op jit(solution)/shard_map/ppermute | solution.py:301
  80.4 1.9 %collective-permute-start.5 = (bf16[512,256]{1,0:T(8,128)(2,1)S(1)}, bf16[512,256]{1,0:T(8,128)(2,1)S(1)}, u32[]{:S(2)}, u32[]{:S(2)}) collective-permute-start(bf16[512,256]{1,0:T(8,128)(2,1)S(1)} %collective-permute-done.4.p_ref), channel_id=1, source_target_pairs={{0,2},{2,4},{4,6},{6,8},{8,10},{10,12},{12,14},{14,0},{1,3},{3,5},... | collective-permute-start | bytes 786440 | tf_op jit(solution)/shard_map/ppermute | solution.py:301
  82.4 4.6 %collective-permute-start.9 = (bf16[512,256]{1,0:T(8,128)(2,1)S(1)}, bf16[512,256]{1,0:T(8,128)(2,1)S(1)}, u32[]{:S(2)}, u32[]{:S(2)}) collective-permute-start(bf16[512,256]{1,0:T(8,128)(2,1)S(1)} %collective-permute-done.8.m_ref), channel_id=1, source_target_pairs={{0,14},{2,0},{4,2},{6,4},{8,6},{10,8},{12,10},{14,12},{1,15},{3,1}... | collective-permute-start | bytes 786440 | tf_op jit(solution)/shard_map/ppermute | solution.py:301
  88.7 1.9 %collective-permute-start.6 = (bf16[512,256]{1,0:T(8,128)(2,1)S(1)}, bf16[512,256]{1,0:T(8,128)(2,1)S(1)}, u32[]{:S(2)}, u32[]{:S(2)}) collective-permute-start(bf16[512,256]{1,0:T(8,128)(2,1)S(1)} %collective-permute-done.5.p_ref), channel_id=1, source_target_pairs={{0,2},{2,4},{4,6},{6,8},{8,10},{10,12},{12,14},{14,0},{1,3},{3,5},... | collective-permute-start | bytes 786440 | tf_op jit(solution)/shard_map/ppermute | solution.py:301
  98.0 2.8 %collective-permute-start.10 = (bf16[512,256]{1,0:T(8,128)(2,1)S(1)}, bf16[512,256]{1,0:T(8,128)(2,1)S(1)}, u32[]{:S(2)}, u32[]{:S(2)}) collective-permute-start(bf16[512,256]{1,0:T(8,128)(2,1)S(1)} %get-tuple-element.51), channel_id=1, source_target_pairs={{0,2},{2,4},{4,6},{6,8},{8,10},{10,12},{12,14},{14,0},{1,15},{3,1}... | collective-permute-start | bytes 786440 | tf_op jit(solution)/shard_map/ppermute | solution.py:301
  101.8 2.5 %collective-permute-start.14 = (bf16[512,256]{1,0:T(8,128)(2,1)S(1)}, bf16[512,256]{1,0:T(8,128)(2,1)S(1)}, u32[]{:S(2)}, u32[]{:S(2)}) collective-permute-start(bf16[512,256]{1,0:T(8,128)(2,1)S(1)} %get-tuple-element.54), channel_id=1, source_target_pairs={{0,14},{2,0},{4,2},{6,4},{8,6},{10,8},{12,10},{14,12},{1,3},{3,5},... | collective-permute-start | bytes 786440 | tf_op jit(solution)/shard_map/ppermute | solution.py:301
  105.2 4.0 %collective-permute-start.11 = (bf16[512,256]{1,0:T(8,128)(2,1)S(1)}, bf16[512,256]{1,0:T(8,128)(2,1)S(1)}, u32[]{:S(2)}, u32[]{:S(2)}) collective-permute-start(bf16[512,256]{1,0:T(8,128)(2,1)S(1)} %shard_map.120), channel_id=1, source_target_pairs={{0,2},{2,4},{4,6},{6,8},{8,10},{10,12},{12,14},{14,0},{1,15},{3,1}... | collective-permute-start | bytes 786440 | tf_op jit(solution)/shard_map/ppermute | solution.py:301
  110.2 2.0 %collective-permute-start.15 = (bf16[512,256]{1,0:T(8,128)(2,1)S(1)}, bf16[512,256]{1,0:T(8,128)(2,1)S(1)}, u32[]{:S(2)}, u32[]{:S(2)}) collective-permute-start(bf16[512,256]{1,0:T(8,128)(2,1)S(1)} %shard_map.123), channel_id=1, source_target_pairs={{0,14},{2,0},{4,2},{6,4},{8,6},{10,8},{12,10},{14,12},{1,3},{3,5},... | collective-permute-start | bytes 786440 | tf_op jit(solution)/shard_map/ppermute | solution.py:301
  112.7 4.9 %collective-permute-start.12 = (bf16[512,256]{1,0:T(8,128)(2,1)S(1)}, bf16[512,256]{1,0:T(8,128)(2,1)S(1)}, u32[]{:S(2)}, u32[]{:S(2)}) collective-permute-start(bf16[512,256]{1,0:T(8,128)(2,1)S(1)} %shard_map.121), channel_id=1, source_target_pairs={{0,2},{2,4},{4,6},{6,8},{8,10},{10,12},{12,14},{14,0},{1,15},{3,1}... | collective-permute-start | bytes 786440 | tf_op jit(solution)/shard_map/ppermute | solution.py:301
  118.6 1.9 %collective-permute-start.16 = (bf16[512,256]{1,0:T(8,128)(2,1)S(1)}, bf16[512,256]{1,0:T(8,128)(2,1)S(1)}, u32[]{:S(2)}, u32[]{:S(2)}) collective-permute-start(bf16[512,256]{1,0:T(8,128)(2,1)S(1)} %shard_map.124), channel_id=1, source_target_pairs={{0,14},{2,0},{4,2},{6,4},{8,6},{10,8},{12,10},{14,12},{1,3},{3,5},... | collective-permute-start | bytes 786440 | tf_op jit(solution)/shard_map/ppermute | solution.py:301
  120.9 5.0 %collective-permute-start.13 = (bf16[512,256]{1,0:T(8,128)(2,1)S(1)}, bf16[512,256]{1,0:T(8,128)(2,1)S(1)}, u32[]{:S(2)}, u32[]{:S(2)}) collective-permute-start(bf16[512,256]{1,0:T(8,128)(2,1)S(1)} %shard_map.122), channel_id=1, source_target_pairs={{0,2},{2,4},{4,6},{6,8},{8,10},{10,12},{12,14},{14,0},{1,15},{3,1}... | collective-permute-start | bytes 786440 | tf_op jit(solution)/shard_map/ppermute | solution.py:301
  126.9 2.3 %collective-permute-done.13.p_ref = bf16[512,256]{1,0:T(8,128)(2,1)S(1)} collective-permute-done((bf16[512,256]{1,0:T(8,128)(2,1)S(1)}, bf16[512,256]{1,0:T(8,128)(2,1)S(1)}, u32[]{:S(2)}, u32[]{:S(2)}) %collective-permute-start.13) | collective-permute-done | bytes 262176 | tf_op jit(solution)/shard_map/ppermute | solution.py:301
  129.3 19.5 %all_to_all.17 = bf16[32,16,256]{2,1,0:T(8,128)(2,1)S(1)} all-to-all(bf16[32,16,256]{2,1,0:T(8,128)(2,1)S(1)} %bitcast.13), channel_id=1, replica_groups=mesh['sp'=32,'tp'=16] {'sp'}, dimensions={0} | all-to-all | bytes 524288 | tf_op jit(solution)/shard_map/all_to_all | solution.py:422
  149.3 15.1 %collective-permute-start.17 = (f32[256,128]{1,0:T(8,128)S(1)}, f32[256,128]{1,0:T(8,128)S(1)}, u32[]{:S(2)}, u32[]{:S(2)}) collective-permute-start(f32[256,128]{1,0:T(8,128)S(1)} %get-tuple-element.56), channel_id=1, source_target_pairs={{0,1},{1,0},{2,3},{3,2},{4,5},{5,4},{6,7},{7,6},{8,9},{9,8},{10,11... | collective-permute-start | bytes 393224 | tf_op jit(solution)/shard_map/ppermute | solution.py:304
  (42 shorter events, 24.4 us)
Async XLA Ops:
  0.0 11.0 %copy-start.3 = (bf16[256,64]{0,1:T(8,128)(2,1)S(1)}, bf16[256,64]{0,1:T(8,128)(2,1)}, u32[]{:S(2)}) copy-start(bf16[256,64]{0,1:T(8,128)(2,1)} %param.11) | copy-start | bytes 98308
  0.0 35.9 %copy-start = (s32[256,2]{0,1:T(2,128)S(1)}, s32[256,2]{0,1:T(2,128)}, u32[]{:S(2)}) copy-start(s32[256,2]{0,1:T(2,128)} %param.17) | copy-start | bytes 6148
  2.3 31.9 %collective-permute-start.2 = (bf16[6784,256]{1,0:T(8,128)(2,1)S(1)}, bf16[6784,256]{1,0:T(8,128)(2,1)S(1)}, u32[]{:S(2)}, u32[]{:S(2)}) collective-permute-start(bf16[6784,256]{1,0:T(8,128)(2,1)S(1)} %shard_map.111.own_ref), channel_id=1, source_target_pairs={{0,1},{1,0},{2,3},{3,2},{4,5},{5,4},{6,7},{7,6},{8,9},{9,8},{10,11... | collective-permute-start | bytes 10420232 | tf_op jit(solution)/shard_map/ppermute | solution.py:304
  11.0 2.3 %collective-permute-start = (bf16[64,256]{1,0:T(8,128)(2,1)S(1)}, bf16[64,256]{1,0:T(8,128)(2,1)S(1)}, u32[]{:S(2)}, u32[]{:S(2)}) collective-permute-start(bf16[64,256]{1,0:T(8,128)(2,1)S(1)} %bitcast.26), channel_id=1, source_target_pairs={{0,16},{16,32},{32,48},{48,64},{64,80},{80,96},{96,112},{112,128},... | collective-permute-start | bytes 98312 | tf_op jit(solution)/shard_map/ppermute | solution.py:309
  28.4 5.7 %collective-permute-start.1 = (bf16[8,80,256]{2,1,0:T(8,128)(2,1)S(1)}, bf16[8,80,256]{2,1,0:T(8,128)(2,1)S(1)}, u32[]{:S(2)}, u32[]{:S(2)}) collective-permute-start(bf16[8,80,256]{2,1,0:T(8,128)(2,1)S(1)} %all_to_all.15.near_ref), channel_id=1, source_target_pairs={{0,1},{1,0},{2,3},{3,2},{4,5},{5,4},{6,7},{7,6},{8,9},{9,8},{10,11... | collective-permute-start | bytes 983048 | tf_op jit(solution)/shard_map/ppermute | solution.py:304
  34.2 1.7 %copy-start.2 = (bf16[6784,256]{1,0:T(8,128)(2,1)}, bf16[6784,256]{1,0:T(8,128)(2,1)S(1)}, u32[]{:S(2)}) copy-start(bf16[6784,256]{1,0:T(8,128)(2,1)S(1)} %collective-permute-done.2.other_ref.source) | copy-start | bytes 10420228
  63.5 8.6 %collective-permute-start.3 = (bf16[512,256]{1,0:T(8,128)(2,1)S(1)}, bf16[512,256]{1,0:T(8,128)(2,1)S(1)}, u32[]{:S(2)}, u32[]{:S(2)}) collective-permute-start(bf16[512,256]{1,0:T(8,128)(2,1)S(1)} %bitcast.14), channel_id=1, source_target_pairs={{0,2},{2,4},{4,6},{6,8},{8,10},{10,12},{12,14},{14,0},{1,3},{3,5},... | collective-permute-start | bytes 786440 | tf_op jit(solution)/shard_map/ppermute | solution.py:301
  65.6 8.4 %collective-permute-start.7 = (bf16[512,256]{1,0:T(8,128)(2,1)S(1)}, bf16[512,256]{1,0:T(8,128)(2,1)S(1)}, u32[]{:S(2)}, u32[]{:S(2)}) collective-permute-start(bf16[512,256]{1,0:T(8,128)(2,1)S(1)} %bitcast.15), channel_id=1, source_target_pairs={{0,14},{2,0},{4,2},{6,4},{8,6},{10,8},{12,10},{14,12},{1,15},{3,1}... | collective-permute-start | bytes 786440 | tf_op jit(solution)/shard_map/ppermute | solution.py:301
  72.1 8.3 %collective-permute-start.4 = (bf16[512,256]{1,0:T(8,128)(2,1)S(1)}, bf16[512,256]{1,0:T(8,128)(2,1)S(1)}, u32[]{:S(2)}, u32[]{:S(2)}) collective-permute-start(bf16[512,256]{1,0:T(8,128)(2,1)S(1)} %collective-permute-done.3.p_ref), channel_id=1, source_target_pairs={{0,2},{2,4},{4,6},{6,8},{8,10},{10,12},{12,14},{14,0},{1,3},{3,5},... | collective-permute-start | bytes 786440 | tf_op jit(solution)/shard_map/ppermute | solution.py:301
  74.0 8.3 %collective-permute-start.8 = (bf16[512,256]{1,0:T(8,128)(2,1)S(1)}, bf16[512,256]{1,0:T(8,128)(2,1)S(1)}, u32[]{:S(2)}, u32[]{:S(2)}) collective-permute-start(bf16[512,256]{1,0:T(8,128)(2,1)S(1)} %collective-permute-done.7.m_ref), channel_id=1, source_target_pairs={{0,14},{2,0},{4,2},{6,4},{8,6},{10,8},{12,10},{14,12},{1,15},{3,1}... | collective-permute-start | bytes 786440 | tf_op jit(solution)/shard_map/ppermute | solution.py:301
  80.4 8.3 %collective-permute-start.5 = (bf16[512,256]{1,0:T(8,128)(2,1)S(1)}, bf16[512,256]{1,0:T(8,128)(2,1)S(1)}, u32[]{:S(2)}, u32[]{:S(2)}) collective-permute-start(bf16[512,256]{1,0:T(8,128)(2,1)S(1)} %collective-permute-done.4.p_ref), channel_id=1, source_target_pairs={{0,2},{2,4},{4,6},{6,8},{8,10},{10,12},{12,14},{14,0},{1,3},{3,5},... | collective-permute-start | bytes 786440 | tf_op jit(solution)/shard_map/ppermute | solution.py:301
  82.4 12.1 %collective-permute-start.9 = (bf16[512,256]{1,0:T(8,128)(2,1)S(1)}, bf16[512,256]{1,0:T(8,128)(2,1)S(1)}, u32[]{:S(2)}, u32[]{:S(2)}) collective-permute-start(bf16[512,256]{1,0:T(8,128)(2,1)S(1)} %collective-permute-done.8.m_ref), channel_id=1, source_target_pairs={{0,14},{2,0},{4,2},{6,4},{8,6},{10,8},{12,10},{14,12},{1,15},{3,1}... | collective-permute-start | bytes 786440 | tf_op jit(solution)/shard_map/ppermute | solution.py:301
  88.7 8.3 %collective-permute-start.6 = (bf16[512,256]{1,0:T(8,128)(2,1)S(1)}, bf16[512,256]{1,0:T(8,128)(2,1)S(1)}, u32[]{:S(2)}, u32[]{:S(2)}) collective-permute-start(bf16[512,256]{1,0:T(8,128)(2,1)S(1)} %collective-permute-done.5.p_ref), channel_id=1, source_target_pairs={{0,2},{2,4},{4,6},{6,8},{8,10},{10,12},{12,14},{14,0},{1,3},{3,5},... | collective-permute-start | bytes 786440 | tf_op jit(solution)/shard_map/ppermute | solution.py:301
  98.0 7.1 %collective-permute-start.10 = (bf16[512,256]{1,0:T(8,128)(2,1)S(1)}, bf16[512,256]{1,0:T(8,128)(2,1)S(1)}, u32[]{:S(2)}, u32[]{:S(2)}) collective-permute-start(bf16[512,256]{1,0:T(8,128)(2,1)S(1)} %get-tuple-element.51), channel_id=1, source_target_pairs={{0,2},{2,4},{4,6},{6,8},{8,10},{10,12},{12,14},{14,0},{1,15},{3,1}... | collective-permute-start | bytes 786440 | tf_op jit(solution)/shard_map/ppermute | solution.py:301
  101.8 8.3 %collective-permute-start.14 = (bf16[512,256]{1,0:T(8,128)(2,1)S(1)}, bf16[512,256]{1,0:T(8,128)(2,1)S(1)}, u32[]{:S(2)}, u32[]{:S(2)}) collective-permute-start(bf16[512,256]{1,0:T(8,128)(2,1)S(1)} %get-tuple-element.54), channel_id=1, source_target_pairs={{0,14},{2,0},{4,2},{6,4},{8,6},{10,8},{12,10},{14,12},{1,3},{3,5},... | collective-permute-start | bytes 786440 | tf_op jit(solution)/shard_map/ppermute | solution.py:301
  105.2 7.4 %collective-permute-start.11 = (bf16[512,256]{1,0:T(8,128)(2,1)S(1)}, bf16[512,256]{1,0:T(8,128)(2,1)S(1)}, u32[]{:S(2)}, u32[]{:S(2)}) collective-permute-start(bf16[512,256]{1,0:T(8,128)(2,1)S(1)} %shard_map.120), channel_id=1, source_target_pairs={{0,2},{2,4},{4,6},{6,8},{8,10},{10,12},{12,14},{14,0},{1,15},{3,1}... | collective-permute-start | bytes 786440 | tf_op jit(solution)/shard_map/ppermute | solution.py:301
  110.2 8.3 %collective-permute-start.15 = (bf16[512,256]{1,0:T(8,128)(2,1)S(1)}, bf16[512,256]{1,0:T(8,128)(2,1)S(1)}, u32[]{:S(2)}, u32[]{:S(2)}) collective-permute-start(bf16[512,256]{1,0:T(8,128)(2,1)S(1)} %shard_map.123), channel_id=1, source_target_pairs={{0,14},{2,0},{4,2},{6,4},{8,6},{10,8},{12,10},{14,12},{1,3},{3,5},... | collective-permute-start | bytes 786440 | tf_op jit(solution)/shard_map/ppermute | solution.py:301
  112.7 36.2 %copy-start.1 = (f32[256,2]{0,1:T(2,128)S(1)}, f32[256,2]{0,1:T(2,128)}, u32[]{:S(2)}) copy-start(f32[256,2]{0,1:T(2,128)} %param.18) | copy-start | bytes 6148
  112.7 8.2 %collective-permute-start.12 = (bf16[512,256]{1,0:T(8,128)(2,1)S(1)}, bf16[512,256]{1,0:T(8,128)(2,1)S(1)}, u32[]{:S(2)}, u32[]{:S(2)}) collective-permute-start(bf16[512,256]{1,0:T(8,128)(2,1)S(1)} %shard_map.121), channel_id=1, source_target_pairs={{0,2},{2,4},{4,6},{6,8},{8,10},{10,12},{12,14},{14,0},{1,15},{3,1}... | collective-permute-start | bytes 786440 | tf_op jit(solution)/shard_map/ppermute | solution.py:301
  118.6 8.3 %collective-permute-start.16 = (bf16[512,256]{1,0:T(8,128)(2,1)S(1)}, bf16[512,256]{1,0:T(8,128)(2,1)S(1)}, u32[]{:S(2)}, u32[]{:S(2)}) collective-permute-start(bf16[512,256]{1,0:T(8,128)(2,1)S(1)} %shard_map.124), channel_id=1, source_target_pairs={{0,14},{2,0},{4,2},{6,4},{8,6},{10,8},{12,10},{14,12},{1,3},{3,5},... | collective-permute-start | bytes 786440 | tf_op jit(solution)/shard_map/ppermute | solution.py:301
  120.9 8.3 %collective-permute-start.13 = (bf16[512,256]{1,0:T(8,128)(2,1)S(1)}, bf16[512,256]{1,0:T(8,128)(2,1)S(1)}, u32[]{:S(2)}, u32[]{:S(2)}) collective-permute-start(bf16[512,256]{1,0:T(8,128)(2,1)S(1)} %shard_map.122), channel_id=1, source_target_pairs={{0,2},{2,4},{4,6},{6,8},{8,10},{10,12},{12,14},{14,0},{1,15},{3,1}... | collective-permute-start | bytes 786440 | tf_op jit(solution)/shard_map/ppermute | solution.py:301
  149.3 16.0 %collective-permute-start.17 = (f32[256,128]{1,0:T(8,128)S(1)}, f32[256,128]{1,0:T(8,128)S(1)}, u32[]{:S(2)}, u32[]{:S(2)}) collective-permute-start(f32[256,128]{1,0:T(8,128)S(1)} %get-tuple-element.56), channel_id=1, source_target_pairs={{0,1},{1,0},{2,3},{3,2},{4,5},{5,4},{6,7},{7,6},{8,9},{9,8},{10,11... | collective-permute-start | bytes 393224 | tf_op jit(solution)/shard_map/ppermute | solution.py:304

commit v6 on v4

--- a/solution.py
+++ b/solution.py
@@ -187,11 +187,12 @@
 
 
 def last_kernel(
-    pack, chips, total, p_ref, gain_ref, own_ref, other_ref, acc_in, square_in, acc_ref, square_ref, hidden_ref, up_ref, low_ref
+    pack, chips, total, p_ref, m_ref, gain_ref, own_ref, other_ref, acc_in, square_in, acc_ref, square_ref, hidden_ref, up_ref, low_ref
 ):
     packs = (own_ref, other_ref)
     far = chip_at(chips, chips // 2)
-    add_chunk(pack, p_ref[...], far, gain_ref, packs, acc_ref, square_ref)
+    came = jnp.where(lax.rem(lax.axis_index("tp"), CORES) == 0, p_ref[...], m_ref[...])
+    add_chunk(pack, came, far, gain_ref, packs, acc_ref, square_ref)
     mean = jnp.sum(square_ref[...], axis=1, keepdims=True) / total
     scale = lax.rsqrt(mean + NORM_EPS)
     units = hidden_ref.shape[1]
@@ -261,9 +262,9 @@
     total = features * members
     held = blocks * half
 
-    def along(value, step, other=1):
-        pairs = [(y * CORES, (y + step) % chips * CORES) for y in range(chips)]
-        pairs += [(y * CORES + 1, (y + step * other) % chips * CORES + 1) for y in range(chips)]
+    def along(value, step, other=1, cores=range(CORES)):
+        steps = (step, step * other)
+        pairs = [(y * CORES + c, (y + steps[c]) % chips * CORES + c) for y in range(chips) for c in cores]
         return lax.ppermute(value, "tp", pairs)
 
     def across(value):
@@ -331,14 +332,15 @@
             16,
             {5: 0, 6: 1},
         )
-    ahead = along(ahead, 1)
+    ahead = along(ahead, 1, cores=(0,))
+    back = along(back, -1, cores=(1,))
     _, _, hidden, ahead, back = call(
         functools.partial(last_kernel, pack, chips, float(total)),
         (*acc_shape, shape((held, CORES * units), BF16), *(shape((held, width), BF16),) * 2),
-        (ahead, gains, *packs, acc, square),
+        (ahead, back, gains, *packs, acc, square),
         2 * chunk_flops,
         24,
-        {4: 0, 5: 1},
+        {5: 0, 6: 1},
     )
 
     def joined(part, came):

time: 158 us -> 164 us (1.038)
  starting transfers between devices: 62.8 us -> 74 us
  blocking collectives: 65.2 us -> 58.5 us
    ppermute x14 -> x15, starting transfers between devices: 41.9 us -> 51.3 us  [along(): return lax.ppermute(value, 'tp', pairs)]
    all_to_all x1, blocking collectives: 22.7 us -> 15.9 us  [on_device(): lax.all_to_all(result.reshape(blocks, half, width), 'sp', split_axis=0, c...]
    ppermute x2, starting transfers between devices: 19.7 us -> 21.5 us  [across(): return lax.ppermute(value, 'tp', [(t, t ^ 1) for t in range(members)])]
    ppermute x14 -> x15, waiting for transfers between devices: 17.6 us -> 19.1 us  [along(): return lax.ppermute(value, 'tp', pairs)]
  transfers between devices with their start and end apart: 17 -> 18, of which waited for: 11 -> 13; matrix products, arithmetic and copies ran while one was open for 0% -> 0% of each run, Pallas kernels for 3% -> 3%
where the time goes in v6:
time: 164 us; the launch traced here: 163 us
  starting transfers between devices  74 us (45%)
  blocking collectives  58.5 us (36%)
  waiting for transfers between devices  21.1 us (13%)
  Pallas kernels  9.42 us (6%)
    ppermute x15, starting transfers between devices, along(): return lax.ppermute(value, 'tp', pairs)  51.3 us
    all_to_all x1, blocking collectives, on_device(): lax.all_to_all(sent.reshape(experts, half, width), 'sp', split_axis=0, co...  25.9 us
    ppermute x2, starting transfers between devices, across(): return lax.ppermute(value, 'tp', [(t, t ^ 1) for t in range(members)])  21.5 us
    ppermute x15, waiting for transfers between devices, along(): return lax.ppermute(value, 'tp', pairs)  19.1 us
    all_gather x1, blocking collectives, on_device(): mixed = lax.all_gather(pooled, 'tp', axis=0, tiled=False)  16.6 us
    all_to_all x1, blocking collectives, on_device(): lax.all_to_all(result.reshape(blocks, half, width), 'sp', split_axis=0, c...  15.9 us
    pallas_call x17, Pallas kernels, call(): pl.pallas_call(kernel, out_shape=out_shape, in_specs=[pl.BlockSpec(memory...  9.42 us
  transfers between devices with their start and end apart: 18, of which 13 were waited for; matrix products, arithmetic and copies ran while one was open for 0% of the time, Pallas kernels for 3%

profile of v6, /device:TPU:1, one launch (start us, length us, event | category | flops | bytes accessed | tf_op | source)
XLA Modules:
  0.0 163.3 jit_solution(1603765871934734972)
XLA Ops:
  0.0 2.2 %shard_map.109 = (bf16[6784,256]{1,0:T(8,128)(2,1)S(1)}, bf16[64,256]{1,0:T(8,128)(2,1)S(1)}, bf16[64,64]{1,0:T(8,128)(2,1)S(1)}, bf16[1,64]{1,0:T(2,128)(2,1)S(1)}, bf16[1,128]{1,0:T(2,128)(2,1)S(1)}) custom-call(bf16[2048,256]{1,0:T(8,128)(2,1)} %bitcast.24, bf16[2048,256]{1,0:T(8,128)(2,1)} %bitcast.25, bf16[256,2048]{1,0:T(8,128)(2,1)} %bitcast.26, ...), custom_call_target="tpu_custom_call" | custom-call | flops 889192448 | bytes 1736704 | tf_op jit(solution)/shard_map/pallas_call | solution.py:33
  2.2 8.7 %collective-permute-start.1 = (bf16[6784,256]{1,0:T(8,128)(2,1)S(1)}, bf16[6784,256]{1,0:T(8,128)(2,1)S(1)}, u32[]{:S(2)}, u32[]{:S(2)}) collective-permute-start(bf16[6784,256]{1,0:T(8,128)(2,1)S(1)} %get-tuple-element.36.own_ref), channel_id=1, source_target_pairs={{0,1},{1,0},{2,3},{3,2},{4,5},{5,4},{6,7},{7,6},{8,9},{9,8},{10,11... | collective-permute-start | bytes 10420232 | tf_op jit(solution)/shard_map/ppermute | solution.py:271
  13.6 16.6 %all-gather = bf16[1280,256]{1,0:T(8,128)(2,1)S(1)} all-gather(bf16[80,256]{1,0:T(8,128)(2,1)S(1)} %shard_map.110), channel_id=2, replica_groups=mesh['sp'=32,'tp'=16] {'tp'}, dimensions={0}, use_global_device_ids=true | all-gather | bytes 696320 | tf_op jit(solution)/shard_map/all_gather | solution.py:301
  31.0 25.9 %all_to_all.10 = bf16[32,16,256]{2,1,0:T(8,128)(2,1)S(1)} all-to-all(bf16[32,16,256]{2,1,0:T(8,128)(2,1)S(1)} %bitcast.19), channel_id=1, replica_groups=mesh['sp'=32,'tp'=16] {'sp'}, dimensions={0} | all-to-all | bytes 524288 | tf_op jit(solution)/shard_map/all_to_all | solution.py:313
  57.0 1.9 %collective-permute-start.2 = (bf16[512,256]{1,0:T(8,128)(2,1)S(1)}, bf16[512,256]{1,0:T(8,128)(2,1)S(1)}, u32[]{:S(2)}, u32[]{:S(2)}) collective-permute-start(bf16[512,256]{1,0:T(8,128)(2,1)S(1)} %bitcast.15), channel_id=1, source_target_pairs={{0,2},{1,3},{2,4},{3,5},{4,6},{5,7},{6,8},{7,9},{8,10},{9,11},{10,... | collective-permute-start | bytes 786440 | tf_op jit(solution)/shard_map/ppermute | solution.py:268
  58.9 4.6 %collective-permute-start.6 = (bf16[512,256]{1,0:T(8,128)(2,1)S(1)}, bf16[512,256]{1,0:T(8,128)(2,1)S(1)}, u32[]{:S(2)}, u32[]{:S(2)}) collective-permute-start(bf16[512,256]{1,0:T(8,128)(2,1)S(1)} %bitcast.16), channel_id=1, source_target_pairs={{0,14},{1,15},{2,0},{3,1},{4,2},{5,3},{6,4},{7,5},{8,6},{9,7},{10,... | collective-permute-start | bytes 786440 | tf_op jit(solution)/shard_map/ppermute | solution.py:268
  63.4 1.8 %collective-permute-done.2.p_ref = bf16[512,256]{1,0:T(8,128)(2,1)S(1)} collective-permute-done((bf16[512,256]{1,0:T(8,128)(2,1)S(1)}, bf16[512,256]{1,0:T(8,128)(2,1)S(1)}, u32[]{:S(2)}, u32[]{:S(2)}) %collective-permute-start.2) | collective-permute-done | bytes 262176 | tf_op jit(solution)/shard_map/ppermute | solution.py:268
  65.3 1.9 %collective-permute-start.3 = (bf16[512,256]{1,0:T(8,128)(2,1)S(1)}, bf16[512,256]{1,0:T(8,128)(2,1)S(1)}, u32[]{:S(2)}, u32[]{:S(2)}) collective-permute-start(bf16[512,256]{1,0:T(8,128)(2,1)S(1)} %collective-permute-done.2.p_ref), channel_id=1, source_target_pairs={{0,2},{1,3},{2,4},{3,5},{4,6},{5,7},{6,8},{7,9},{8,10},{9,11},{10,... | collective-permute-start | bytes 786440 | tf_op jit(solution)/shard_map/ppermute | solution.py:268
  67.2 4.6 %collective-permute-start.7 = (bf16[512,256]{1,0:T(8,128)(2,1)S(1)}, bf16[512,256]{1,0:T(8,128)(2,1)S(1)}, u32[]{:S(2)}, u32[]{:S(2)}) collective-permute-start(bf16[512,256]{1,0:T(8,128)(2,1)S(1)} %collective-permute-done.6.m_ref), channel_id=1, source_target_pairs={{0,14},{1,15},{2,0},{3,1},{4,2},{5,3},{6,4},{7,5},{8,6},{9,7},{10,... | collective-permute-start | bytes 786440 | tf_op jit(solution)/shard_map/ppermute | solution.py:268
  73.6 1.9 %collective-permute-start.4 = (bf16[512,256]{1,0:T(8,128)(2,1)S(1)}, bf16[512,256]{1,0:T(8,128)(2,1)S(1)}, u32[]{:S(2)}, u32[]{:S(2)}) collective-permute-start(bf16[512,256]{1,0:T(8,128)(2,1)S(1)} %collective-permute-done.3.p_ref), channel_id=1, source_target_pairs={{0,2},{1,3},{2,4},{3,5},{4,6},{5,7},{6,8},{7,9},{8,10},{9,11},{10,... | collective-permute-start | bytes 786440 | tf_op jit(solution)/shard_map/ppermute | solution.py:268
  75.5 4.6 %collective-permute-start.8 = (bf16[512,256]{1,0:T(8,128)(2,1)S(1)}, bf16[512,256]{1,0:T(8,128)(2,1)S(1)}, u32[]{:S(2)}, u32[]{:S(2)}) collective-permute-start(bf16[512,256]{1,0:T(8,128)(2,1)S(1)} %collective-permute-done.7.m_ref), channel_id=1, source_target_pairs={{0,14},{1,15},{2,0},{3,1},{4,2},{5,3},{6,4},{7,5},{8,6},{9,7},{10,... | collective-permute-start | bytes 786440 | tf_op jit(solution)/shard_map/ppermute | solution.py:268
  83.4 5.0 %collective-permute-start.9 = (bf16[512,256]{1,0:T(8,128)(2,1)S(1)}, bf16[512,256]{1,0:T(8,128)(2,1)S(1)}, u32[]{:S(2)}, u32[]{:S(2)}) collective-permute-start(bf16[512,256]{1,0:T(8,128)(2,1)S(1)} %collective-permute-done.8.m_ref), channel_id=1, source_target_pairs={{1,15},{3,1},{5,3},{7,5},{9,7},{11,9},{13,11},{15,13},{17,31},{19,... | collective-permute-start | bytes 786440 | tf_op jit(solution)/shard_map/ppermute | solution.py:268
  92.7 5.0 %collective-permute-start.10 = (bf16[512,256]{1,0:T(8,128)(2,1)S(1)}, bf16[512,256]{1,0:T(8,128)(2,1)S(1)}, u32[]{:S(2)}, u32[]{:S(2)}) collective-permute-start(bf16[512,256]{1,0:T(8,128)(2,1)S(1)} %get-tuple-element.53), channel_id=1, source_target_pairs={{0,2},{1,15},{2,4},{3,1},{4,6},{5,3},{6,8},{7,5},{8,10},{9,7},{10,... | collective-permute-start | bytes 786440 | tf_op jit(solution)/shard_map/ppermute | solution.py:268
  97.7 1.9 %collective-permute-start.14 = (bf16[512,256]{1,0:T(8,128)(2,1)S(1)}, bf16[512,256]{1,0:T(8,128)(2,1)S(1)}, u32[]{:S(2)}, u32[]{:S(2)}) collective-permute-start(bf16[512,256]{1,0:T(8,128)(2,1)S(1)} %get-tuple-element.56), channel_id=1, source_target_pairs={{0,14},{1,3},{2,0},{3,5},{4,2},{5,7},{6,4},{7,9},{8,6},{9,11},{10,... | collective-permute-start | bytes 786440 | tf_op jit(solution)/shard_map/ppermute | solution.py:268
  101.1 5.0 %collective-permute-start.11 = (bf16[512,256]{1,0:T(8,128)(2,1)S(1)}, bf16[512,256]{1,0:T(8,128)(2,1)S(1)}, u32[]{:S(2)}, u32[]{:S(2)}) collective-permute-start(bf16[512,256]{1,0:T(8,128)(2,1)S(1)} %shard_map.118), channel_id=1, source_target_pairs={{0,2},{1,15},{2,4},{3,1},{4,6},{5,3},{6,8},{7,5},{8,10},{9,7},{10,... | collective-permute-start | bytes 786440 | tf_op jit(solution)/shard_map/ppermute | solution.py:268
  106.1 2.2 %collective-permute-done.14.came_ref = bf16[512,256]{1,0:T(8,128)(2,1)S(1)} collective-permute-done((bf16[512,256]{1,0:T(8,128)(2,1)S(1)}, bf16[512,256]{1,0:T(8,128)(2,1)S(1)}, u32[]{:S(2)}, u32[]{:S(2)}) %collective-permute-start.14) | collective-permute-done | bytes 262176 | tf_op jit(solution)/shard_map/ppermute | solution.py:268
  108.3 1.9 %collective-permute-start.15 = (bf16[512,256]{1,0:T(8,128)(2,1)S(1)}, bf16[512,256]{1,0:T(8,128)(2,1)S(1)}, u32[]{:S(2)}, u32[]{:S(2)}) collective-permute-start(bf16[512,256]{1,0:T(8,128)(2,1)S(1)} %shard_map.121), channel_id=1, source_target_pairs={{0,14},{1,3},{2,0},{3,5},{4,2},{5,7},{6,4},{7,9},{8,6},{9,11},{10,... | collective-permute-start | bytes 786440 | tf_op jit(solution)/shard_map/ppermute | solution.py:268
  111.6 5.0 %collective-permute-start.12 = (bf16[512,256]{1,0:T(8,128)(2,1)S(1)}, bf16[512,256]{1,0:T(8,128)(2,1)S(1)}, u32[]{:S(2)}, u32[]{:S(2)}) collective-permute-start(bf16[512,256]{1,0:T(8,128)(2,1)S(1)} %shard_map.119), channel_id=1, source_target_pairs={{0,2},{1,15},{2,4},{3,1},{4,6},{5,3},{6,8},{7,5},{8,10},{9,7},{10,... | collective-permute-start | bytes 786440 | tf_op jit(solution)/shard_map/ppermute | solution.py:268
  118.0 1.9 %collective-permute-start.16 = (bf16[512,256]{1,0:T(8,128)(2,1)S(1)}, bf16[512,256]{1,0:T(8,128)(2,1)S(1)}, u32[]{:S(2)}, u32[]{:S(2)}) collective-permute-start(bf16[512,256]{1,0:T(8,128)(2,1)S(1)} %shard_map.122), channel_id=1, source_target_pairs={{0,14},{1,3},{2,0},{3,5},{4,2},{5,7},{6,4},{7,9},{8,6},{9,11},{10,... | collective-permute-start | bytes 786440 | tf_op jit(solution)/shard_map/ppermute | solution.py:268
  120.0 2.3 %collective-permute-done.12.came_ref = bf16[512,256]{1,0:T(8,128)(2,1)S(1)} collective-permute-done((bf16[512,256]{1,0:T(8,128)(2,1)S(1)}, bf16[512,256]{1,0:T(8,128)(2,1)S(1)}, u32[]{:S(2)}, u32[]{:S(2)}) %collective-permute-start.12) | collective-permute-done | bytes 262176 | tf_op jit(solution)/shard_map/ppermute | solution.py:268
  122.3 5.3 %collective-permute-start.13 = (bf16[512,256]{1,0:T(8,128)(2,1)S(1)}, bf16[512,256]{1,0:T(8,128)(2,1)S(1)}, u32[]{:S(2)}, u32[]{:S(2)}) collective-permute-start(bf16[512,256]{1,0:T(8,128)(2,1)S(1)} %shard_map.120), channel_id=1, source_target_pairs={{0,2},{1,15},{2,4},{3,1},{4,6},{5,3},{6,8},{7,5},{8,10},{9,7},{10,... | collective-permute-start | bytes 786440 | tf_op jit(solution)/shard_map/ppermute | solution.py:268
  127.6 4.8 %collective-permute-done.13.p_ref = bf16[512,256]{1,0:T(8,128)(2,1)S(1)} collective-permute-done((bf16[512,256]{1,0:T(8,128)(2,1)S(1)}, bf16[512,256]{1,0:T(8,128)(2,1)S(1)}, u32[]{:S(2)}, u32[]{:S(2)}) %collective-permute-start.13) | collective-permute-done | bytes 262176 | tf_op jit(solution)/shard_map/ppermute | solution.py:268
  132.5 15.9 %all_to_all.11 = bf16[32,16,256]{2,1,0:T(8,128)(2,1)S(1)} all-to-all(bf16[32,16,256]{2,1,0:T(8,128)(2,1)S(1)} %bitcast.18), channel_id=1, replica_groups=mesh['sp'=32,'tp'=16] {'sp'}, dimensions={0} | all-to-all | bytes 524288 | tf_op jit(solution)/shard_map/all_to_all | solution.py:365
  149.0 12.7 %collective-permute-start.17 = (f32[256,128]{1,0:T(8,128)S(1)}, f32[256,128]{1,0:T(8,128)S(1)}, u32[]{:S(2)}, u32[]{:S(2)}) collective-permute-start(f32[256,128]{1,0:T(8,128)S(1)} %get-tuple-element.58), channel_id=1, source_target_pairs={{0,1},{1,0},{2,3},{3,2},{4,5},{5,4},{6,7},{7,6},{8,9},{9,8},{10,11... | collective-permute-start | bytes 393224 | tf_op jit(solution)/shard_map/ppermute | solution.py:271
  (38 shorter events, 19.2 us)
Async XLA Ops:
  0.0 11.0 %copy-start.2 = (bf16[256,64]{0,1:T(8,128)(2,1)S(1)}, bf16[256,64]{0,1:T(8,128)(2,1)}, u32[]{:S(2)}) copy-start(bf16[256,64]{0,1:T(8,128)(2,1)} %param.11) | copy-start | bytes 98308
  0.0 30.2 %copy-start = (s32[256,2]{0,1:T(2,128)S(1)}, s32[256,2]{0,1:T(2,128)}, u32[]{:S(2)}) copy-start(s32[256,2]{0,1:T(2,128)} %param.17) | copy-start | bytes 6148
  2.2 28.0 %collective-permute-start.1 = (bf16[6784,256]{1,0:T(8,128)(2,1)S(1)}, bf16[6784,256]{1,0:T(8,128)(2,1)S(1)}, u32[]{:S(2)}, u32[]{:S(2)}) collective-permute-start(bf16[6784,256]{1,0:T(8,128)(2,1)S(1)} %get-tuple-element.36.own_ref), channel_id=1, source_target_pairs={{0,1},{1,0},{2,3},{3,2},{4,5},{5,4},{6,7},{7,6},{8,9},{9,8},{10,11... | collective-permute-start | bytes 10420232 | tf_op jit(solution)/shard_map/ppermute | solution.py:271
  11.0 2.3 %collective-permute-start = (bf16[64,256]{1,0:T(8,128)(2,1)S(1)}, bf16[64,256]{1,0:T(8,128)(2,1)S(1)}, u32[]{:S(2)}, u32[]{:S(2)}) collective-permute-start(bf16[64,256]{1,0:T(8,128)(2,1)S(1)} %bitcast.28), channel_id=1, source_target_pairs={{0,16},{16,32},{32,48},{48,64},{64,80},{80,96},{96,112},{112,128},... | collective-permute-start | bytes 98312 | tf_op jit(solution)/shard_map/ppermute | solution.py:276
  57.0 8.3 %collective-permute-start.2 = (bf16[512,256]{1,0:T(8,128)(2,1)S(1)}, bf16[512,256]{1,0:T(8,128)(2,1)S(1)}, u32[]{:S(2)}, u32[]{:S(2)}) collective-permute-start(bf16[512,256]{1,0:T(8,128)(2,1)S(1)} %bitcast.15), channel_id=1, source_target_pairs={{0,2},{1,3},{2,4},{3,5},{4,6},{5,7},{6,8},{7,9},{8,10},{9,11},{10,... | collective-permute-start | bytes 786440 | tf_op jit(solution)/shard_map/ppermute | solution.py:268
  58.9 8.3 %collective-permute-start.6 = (bf16[512,256]{1,0:T(8,128)(2,1)S(1)}, bf16[512,256]{1,0:T(8,128)(2,1)S(1)}, u32[]{:S(2)}, u32[]{:S(2)}) collective-permute-start(bf16[512,256]{1,0:T(8,128)(2,1)S(1)} %bitcast.16), channel_id=1, source_target_pairs={{0,14},{1,15},{2,0},{3,1},{4,2},{5,3},{6,4},{7,5},{8,6},{9,7},{10,... | collective-permute-start | bytes 786440 | tf_op jit(solution)/shard_map/ppermute | solution.py:268
  65.3 8.3 %collective-permute-start.3 = (bf16[512,256]{1,0:T(8,128)(2,1)S(1)}, bf16[512,256]{1,0:T(8,128)(2,1)S(1)}, u32[]{:S(2)}, u32[]{:S(2)}) collective-permute-start(bf16[512,256]{1,0:T(8,128)(2,1)S(1)} %collective-permute-done.2.p_ref), channel_id=1, source_target_pairs={{0,2},{1,3},{2,4},{3,5},{4,6},{5,7},{6,8},{7,9},{8,10},{9,11},{10,... | collective-permute-start | bytes 786440 | tf_op jit(solution)/shard_map/ppermute | solution.py:268
  67.2 8.3 %collective-permute-start.7 = (bf16[512,256]{1,0:T(8,128)(2,1)S(1)}, bf16[512,256]{1,0:T(8,128)(2,1)S(1)}, u32[]{:S(2)}, u32[]{:S(2)}) collective-permute-start(bf16[512,256]{1,0:T(8,128)(2,1)S(1)} %collective-permute-done.6.m_ref), channel_id=1, source_target_pairs={{0,14},{1,15},{2,0},{3,1},{4,2},{5,3},{6,4},{7,5},{8,6},{9,7},{10,... | collective-permute-start | bytes 786440 | tf_op jit(solution)/shard_map/ppermute | solution.py:268
  73.6 8.3 %collective-permute-start.4 = (bf16[512,256]{1,0:T(8,128)(2,1)S(1)}, bf16[512,256]{1,0:T(8,128)(2,1)S(1)}, u32[]{:S(2)}, u32[]{:S(2)}) collective-permute-start(bf16[512,256]{1,0:T(8,128)(2,1)S(1)} %collective-permute-done.3.p_ref), channel_id=1, source_target_pairs={{0,2},{1,3},{2,4},{3,5},{4,6},{5,7},{6,8},{7,9},{8,10},{9,11},{10,... | collective-permute-start | bytes 786440 | tf_op jit(solution)/shard_map/ppermute | solution.py:268
  75.5 7.9 %collective-permute-start.8 = (bf16[512,256]{1,0:T(8,128)(2,1)S(1)}, bf16[512,256]{1,0:T(8,128)(2,1)S(1)}, u32[]{:S(2)}, u32[]{:S(2)}) collective-permute-start(bf16[512,256]{1,0:T(8,128)(2,1)S(1)} %collective-permute-done.7.m_ref), channel_id=1, source_target_pairs={{0,14},{1,15},{2,0},{3,1},{4,2},{5,3},{6,4},{7,5},{8,6},{9,7},{10,... | collective-permute-start | bytes 786440 | tf_op jit(solution)/shard_map/ppermute | solution.py:268
  81.9 9.2 %collective-permute-start.5 = (bf16[512,256]{1,0:T(8,128)(2,1)S(1)}, bf16[512,256]{1,0:T(8,128)(2,1)S(1)}, u32[]{:S(2)}, u32[]{:S(2)}) collective-permute-start(bf16[512,256]{1,0:T(8,128)(2,1)S(1)} %collective-permute-done.4.p_ref), channel_id=1, source_target_pairs={{0,2},{2,4},{4,6},{6,8},{8,10},{10,12},{12,14},{14,0},{16,18},{18,... | collective-permute-start | bytes 786440 | tf_op jit(solution)/shard_map/ppermute | solution.py:268
  83.4 8.3 %collective-permute-start.9 = (bf16[512,256]{1,0:T(8,128)(2,1)S(1)}, bf16[512,256]{1,0:T(8,128)(2,1)S(1)}, u32[]{:S(2)}, u32[]{:S(2)}) collective-permute-start(bf16[512,256]{1,0:T(8,128)(2,1)S(1)} %collective-permute-done.8.m_ref), channel_id=1, source_target_pairs={{1,15},{3,1},{5,3},{7,5},{9,7},{11,9},{13,11},{15,13},{17,31},{19,... | collective-permute-start | bytes 786440 | tf_op jit(solution)/shard_map/ppermute | solution.py:268
  92.7 8.3 %collective-permute-start.10 = (bf16[512,256]{1,0:T(8,128)(2,1)S(1)}, bf16[512,256]{1,0:T(8,128)(2,1)S(1)}, u32[]{:S(2)}, u32[]{:S(2)}) collective-permute-start(bf16[512,256]{1,0:T(8,128)(2,1)S(1)} %get-tuple-element.53), channel_id=1, source_target_pairs={{0,2},{1,15},{2,4},{3,1},{4,6},{5,3},{6,8},{7,5},{8,10},{9,7},{10,... | collective-permute-start | bytes 786440 | tf_op jit(solution)/shard_map/ppermute | solution.py:268
  97.7 10.5 %collective-permute-start.14 = (bf16[512,256]{1,0:T(8,128)(2,1)S(1)}, bf16[512,256]{1,0:T(8,128)(2,1)S(1)}, u32[]{:S(2)}, u32[]{:S(2)}) collective-permute-start(bf16[512,256]{1,0:T(8,128)(2,1)S(1)} %get-tuple-element.56), channel_id=1, source_target_pairs={{0,14},{1,3},{2,0},{3,5},{4,2},{5,7},{6,4},{7,9},{8,6},{9,11},{10,... | collective-permute-start | bytes 786440 | tf_op jit(solution)/shard_map/ppermute | solution.py:268
  101.1 10.4 %collective-permute-start.11 = (bf16[512,256]{1,0:T(8,128)(2,1)S(1)}, bf16[512,256]{1,0:T(8,128)(2,1)S(1)}, u32[]{:S(2)}, u32[]{:S(2)}) collective-permute-start(bf16[512,256]{1,0:T(8,128)(2,1)S(1)} %shard_map.118), channel_id=1, source_target_pairs={{0,2},{1,15},{2,4},{3,1},{4,6},{5,3},{6,8},{7,5},{8,10},{9,7},{10,... | collective-permute-start | bytes 786440 | tf_op jit(solution)/shard_map/ppermute | solution.py:268
  108.3 9.7 %collective-permute-start.15 = (bf16[512,256]{1,0:T(8,128)(2,1)S(1)}, bf16[512,256]{1,0:T(8,128)(2,1)S(1)}, u32[]{:S(2)}, u32[]{:S(2)}) collective-permute-start(bf16[512,256]{1,0:T(8,128)(2,1)S(1)} %shard_map.121), channel_id=1, source_target_pairs={{0,14},{1,3},{2,0},{3,5},{4,2},{5,7},{6,4},{7,9},{8,6},{9,11},{10,... | collective-permute-start | bytes 786440 | tf_op jit(solution)/shard_map/ppermute | solution.py:268
  111.5 36.9 %copy-start.1 = (f32[256,2]{0,1:T(2,128)S(1)}, f32[256,2]{0,1:T(2,128)}, u32[]{:S(2)}) copy-start(f32[256,2]{0,1:T(2,128)} %param.18) | copy-start | bytes 6148
  111.6 10.7 %collective-permute-start.12 = (bf16[512,256]{1,0:T(8,128)(2,1)S(1)}, bf16[512,256]{1,0:T(8,128)(2,1)S(1)}, u32[]{:S(2)}, u32[]{:S(2)}) collective-permute-start(bf16[512,256]{1,0:T(8,128)(2,1)S(1)} %shard_map.119), channel_id=1, source_target_pairs={{0,2},{1,15},{2,4},{3,1},{4,6},{5,3},{6,8},{7,5},{8,10},{9,7},{10,... | collective-permute-start | bytes 786440 | tf_op jit(solution)/shard_map/ppermute | solution.py:268
  118.0 9.6 %collective-permute-start.16 = (bf16[512,256]{1,0:T(8,128)(2,1)S(1)}, bf16[512,256]{1,0:T(8,128)(2,1)S(1)}, u32[]{:S(2)}, u32[]{:S(2)}) collective-permute-start(bf16[512,256]{1,0:T(8,128)(2,1)S(1)} %shard_map.122), channel_id=1, source_target_pairs={{0,14},{1,3},{2,0},{3,5},{4,2},{5,7},{6,4},{7,9},{8,6},{9,11},{10,... | collective-permute-start | bytes 786440 | tf_op jit(solution)/shard_map/ppermute | solution.py:268
  122.3 10.1 %collective-permute-start.13 = (bf16[512,256]{1,0:T(8,128)(2,1)S(1)}, bf16[512,256]{1,0:T(8,128)(2,1)S(1)}, u32[]{:S(2)}, u32[]{:S(2)}) collective-permute-start(bf16[512,256]{1,0:T(8,128)(2,1)S(1)} %shard_map.120), channel_id=1, source_target_pairs={{0,2},{1,15},{2,4},{3,1},{4,6},{5,3},{6,8},{7,5},{8,10},{9,7},{10,... | collective-permute-start | bytes 786440 | tf_op jit(solution)/shard_map/ppermute | solution.py:268
  149.0 13.7 %collective-permute-start.17 = (f32[256,128]{1,0:T(8,128)S(1)}, f32[256,128]{1,0:T(8,128)S(1)}, u32[]{:S(2)}, u32[]{:S(2)}) collective-permute-start(f32[256,128]{1,0:T(8,128)S(1)} %get-tuple-element.58), channel_id=1, source_target_pairs={{0,1},{1,0},{2,3},{3,2},{4,5},{5,4},{6,7},{7,6},{8,9},{9,8},{10,11... | collective-permute-start | bytes 393224 | tf_op jit(solution)/shard_map/ppermute | solution.py:271

commit v7 on v4

--- a/solution.py
+++ b/solution.py
@@ -85,16 +85,21 @@
 
 class Pack:
     def __init__(self, deep, width, channels, rows):
-        self.gate, self.up, self.down = 0, deep, 2 * deep
-        self.project = 3 * deep
-        self.resid = self.project + channels // 2
-        self.rows = self.resid + rows // 2
+        self.gate, self.up, self.down, self.weights = 0, deep, 2 * deep, 3 * deep
+        self.project, self.resid, self.rows = 0, channels // 2, (channels + rows) // 2
         self.width = width
 
 
-def prep_kernel(pack, gate, up, down, project, resid, x, w, gain, norm, out, x_out, w_out, gain_out, norm_out, sems):
-    width, features = pack.width, project.shape[1]
-    units = down.shape[0]
+def copy_all(pairs, sems):
+    copies = [pltpu.make_async_copy(a, b, sems.at[i]) for i, (a, b) in enumerate(pairs)]
+    for copy in copies:
+        copy.start()
+    for copy in copies:
+        copy.wait()
+
+
+def prep_kernel(pack, project, resid, x, w, gain, norm, out, x_out, w_out, gain_out, norm_out, sems):
+    features = project.shape[1]
     pairs = [(x, x_out), (w, w_out), (gain, gain_out), (norm, norm_out)]
     for base, source in ((pack.project, project), (pack.resid, resid)):
         half = source.shape[0] // 2
@@ -103,17 +108,17 @@
                 (source.at[i * half : (i + 1) * half, :],
                  out.at[base : base + half, i * features : (i + 1) * features])
             )
-    pairs.append((gate, out.at[pack.gate : pack.up, :]))
-    pairs.append((up, out.at[pack.up : pack.down, :]))
+    copy_all(pairs, sems)
+
+
+def weights_kernel(pack, gate, up, down, out, sems):
+    width, units = pack.width, down.shape[0]
+    pairs = [(gate, out.at[pack.gate : pack.up, :]), (up, out.at[pack.up : pack.down, :])]
     for i in range(down.shape[1] // width):
         pairs.append(
             (down.at[:, i * width : (i + 1) * width], out.at[pack.down + i * units : pack.down + (i + 1) * units, :])
         )
-    copies = [pltpu.make_async_copy(a, b, sems.at[i]) for i, (a, b) in enumerate(pairs)]
-    for copy in copies:
-        copy.start()
-    for copy in copies:
-        copy.wait()
+    copy_all(pairs, sems)
 
 
 def dispatch_kernel(pack, experts, capacity, mixed_ref, own_ref, other_ref, routes_ref, stream_ref, gain_ref, out_ref):
@@ -272,6 +277,10 @@
     shape = jax.ShapeDtypeStruct
     deep, units = expert_gate.shape[1:]
     pack = Pack(deep, width, out_weight.shape[0], tok_rows)
+
+    def in_hbm(*values):
+        return tuple(pltpu.with_memory_space_constraint(v, pltpu.HBM) for v in values)
+
     before = lax.ppermute(
         pool_input.T, "sp", [(s, s + 1) for s in range(blocks - 1)]
     )
@@ -279,17 +288,13 @@
     own, *small = call(
         functools.partial(prep_kernel, pack),
         (pltpu.VMEM((pack.rows, width), BF16), *(pltpu.VMEM(v.shape, v.dtype) for v in small)),
-        tuple(
-            pltpu.with_memory_space_constraint(v, pltpu.HBM)
-            for v in (expert_gate[0], expert_up[0], expert_down[0], out_weight, resid, *small)
-        ),
+        in_hbm(out_weight, resid, *small),
         pack.rows * width * 512,
         8,
-        space=pltpu.HBM,
-        scratch=[pltpu.SemaphoreType.DMA((10 + chips,))],
+        space=pl.ANY,
+        scratch=[pltpu.SemaphoreType.DMA((8,))],
     )
     other = across(own)
-    packs = (own, other)
     pooled = call(
         pool_kernel,
         shape((GSIZE + 16, tok_rows), BF16),
@@ -305,7 +310,7 @@
             shape((chips, 8, width), F32),
             shape((experts * half, width), BF16),
         ),
-        (mixed, *packs, routes.T),
+        (mixed, own, other, routes.T),
         2 * experts * half * width * tok_rows,
         16,
     )
@@ -313,6 +318,16 @@
         sent.reshape(experts, half, width), "sp", split_axis=0, concat_axis=0, tiled=True
     ).reshape(held, width)
 
+    (own,) = call(
+        functools.partial(weights_kernel, pack),
+        (pltpu.VMEM((pack.weights, width), BF16),),
+        in_hbm(expert_gate[0], expert_up[0], expert_down[0]),
+        pack.weights * width * 512,
+        8,
+        space=pl.ANY,
+        scratch=[pltpu.SemaphoreType.DMA((2 + chips,))],
+    )
+    packs = (own, across(own))
     acc_shape = (shape((held, 4 * units), F32), shape((held, 128), F32))
     chunk_flops = 2 * held * width * 4 * units
     acc, square = call(

time: 158 us -> 158 us (level)
  blocking collectives: 65.2 us -> 63.1 us
  starting transfers between devices: 62.8 us -> 64.7 us
    all_to_all x1, blocking collectives: 25.9 us -> 24 us  [on_device(): lax.all_to_all(sent.reshape(experts, half, width), 'sp', split_axis=0, co...]
    ppermute x2 -> x3, starting transfers between devices: 19.7 us -> 21.6 us  [across(): return lax.ppermute(value, 'tp', [(t, t ^ 1) for t in range(members)])]
    pallas_call x17 -> x18, Pallas kernels: 9.43 us -> 10.2 us  [call(): pl.pallas_call(kernel, out_shape=out_shape, in_specs=[pl.BlockSpec(memory...]
  transfers between devices with their start and end apart: 17 -> 18, of which waited for: 11 -> 10; matrix products, arithmetic and copies ran while one was open for 0% -> 0% of each run, Pallas kernels for 3% -> 4%
where the time goes in v7:
time: 158 us; the launch traced here: 157 us
  starting transfers between devices  64.7 us (41%)
  blocking collectives  63.1 us (40%)
  waiting for transfers between devices  18.6 us (12%)
  Pallas kernels  10.2 us (6%)
    ppermute x14, starting transfers between devices, along(): return lax.ppermute(value, 'tp', pairs)  41.9 us
    all_to_all x1, blocking collectives, on_device(): lax.all_to_all(sent.reshape(experts, half, width), 'sp', split_axis=0, co...  24 us
    all_to_all x1, blocking collectives, on_device(): lax.all_to_all(result.reshape(blocks, half, width), 'sp', split_axis=0, c...  22.7 us
    ppermute x3, starting transfers between devices, across(): return lax.ppermute(value, 'tp', [(t, t ^ 1) for t in range(members)])  21.6 us
    ppermute x14, waiting for transfers between devices, along(): return lax.ppermute(value, 'tp', pairs)  17.6 us
    all_gather x1, blocking collectives, on_device(): mixed = lax.all_gather(pooled, 'tp', axis=0, tiled=False)  16.5 us
    pallas_call x18, Pallas kernels, call(): pl.pallas_call(kernel, out_shape=out_shape, in_specs=[pl.BlockSpec(memory...  10.2 us
  transfers between devices with their start and end apart: 18, of which 10 were waited for; matrix products, arithmetic and copies ran while one was open for 0% of the time, Pallas kernels for 4%

profile of v7, /device:TPU:1, one launch (start us, length us, event | category | flops | bytes accessed | tf_op | source)
XLA Modules:
  0.0 157.1 jit_solution(7099194304189383741)
XLA Ops:
  0.0 1.9 %shard_map.112.own_ref = bf16[6144,256]{1,0:T(8,128)(2,1)S(1)} custom-call(bf16[2048,256]{1,0:T(8,128)(2,1)} %bitcast.24, bf16[2048,256]{1,0:T(8,128)(2,1)} %bitcast.25, bf16[256,2048]{1,0:T(8,128)(2,1)} %bitcast.26), custom_call_target="tpu_custom_call" | custom-call | flops 805306368 | bytes 1572864 | tf_op jit(solution)/shard_map/pallas_call | solution.py:33
  1.9 8.7 %collective-permute-start.6 = (bf16[6144,256]{1,0:T(8,128)(2,1)S(1)}, bf16[6144,256]{1,0:T(8,128)(2,1)S(1)}, u32[]{:S(2)}, u32[]{:S(2)}) collective-permute-start(bf16[6144,256]{1,0:T(8,128)(2,1)S(1)} %shard_map.112.own_ref), channel_id=1, source_target_pairs={{0,1},{1,0},{2,3},{3,2},{4,5},{5,4},{6,7},{7,6},{8,9},{9,8},{10,11... | collective-permute-start | bytes 9437192 | tf_op jit(solution)/shard_map/ppermute | solution.py:275
  13.1 1.9 %collective-permute-start.1 = (bf16[640,256]{1,0:T(8,128)(2,1)S(1)}, bf16[640,256]{1,0:T(8,128)(2,1)S(1)}, u32[]{:S(2)}, u32[]{:S(2)}) collective-permute-start(bf16[640,256]{1,0:T(8,128)(2,1)S(1)} %get-tuple-element.36.own_ref), channel_id=1, source_target_pairs={{0,1},{1,0},{2,3},{3,2},{4,5},{5,4},{6,7},{7,6},{8,9},{9,8},{10,11... | collective-permute-start | bytes 983048 | tf_op jit(solution)/shard_map/ppermute | solution.py:275
  15.4 16.5 %all-gather = bf16[1280,256]{1,0:T(8,128)(2,1)S(1)} all-gather(bf16[80,256]{1,0:T(8,128)(2,1)S(1)} %shard_map.110), channel_id=2, replica_groups=mesh['sp'=32,'tp'=16] {'tp'}, dimensions={0}, use_global_device_ids=true | all-gather | bytes 696320 | tf_op jit(solution)/shard_map/all_gather | solution.py:305
  32.7 24.0 %all_to_all.10 = bf16[32,16,256]{2,1,0:T(8,128)(2,1)S(1)} all-to-all(bf16[32,16,256]{2,1,0:T(8,128)(2,1)S(1)} %bitcast.19), channel_id=1, replica_groups=mesh['sp'=32,'tp'=16] {'sp'}, dimensions={0} | all-to-all | bytes 524288 | tf_op jit(solution)/shard_map/all_to_all | solution.py:317
  56.7 1.9 %collective-permute-start.2 = (bf16[512,256]{1,0:T(8,128)(2,1)S(1)}, bf16[512,256]{1,0:T(8,128)(2,1)S(1)}, u32[]{:S(2)}, u32[]{:S(2)}) collective-permute-start(bf16[512,256]{1,0:T(8,128)(2,1)S(1)} %bitcast.15), channel_id=1, source_target_pairs={{0,2},{2,4},{4,6},{6,8},{8,10},{10,12},{12,14},{14,0},{1,3},{3,5},... | collective-permute-start | bytes 786440 | tf_op jit(solution)/shard_map/ppermute | solution.py:272
  58.6 4.6 %collective-permute-start.7 = (bf16[512,256]{1,0:T(8,128)(2,1)S(1)}, bf16[512,256]{1,0:T(8,128)(2,1)S(1)}, u32[]{:S(2)}, u32[]{:S(2)}) collective-permute-start(bf16[512,256]{1,0:T(8,128)(2,1)S(1)} %bitcast.16), channel_id=1, source_target_pairs={{0,14},{2,0},{4,2},{6,4},{8,6},{10,8},{12,10},{14,12},{1,15},{3,1}... | collective-permute-start | bytes 786440 | tf_op jit(solution)/shard_map/ppermute | solution.py:272
  65.0 1.9 %collective-permute-start.3 = (bf16[512,256]{1,0:T(8,128)(2,1)S(1)}, bf16[512,256]{1,0:T(8,128)(2,1)S(1)}, u32[]{:S(2)}, u32[]{:S(2)}) collective-permute-start(bf16[512,256]{1,0:T(8,128)(2,1)S(1)} %collective-permute-done.2.p_ref), channel_id=1, source_target_pairs={{0,2},{2,4},{4,6},{6,8},{8,10},{10,12},{12,14},{14,0},{1,3},{3,5},... | collective-permute-start | bytes 786440 | tf_op jit(solution)/shard_map/ppermute | solution.py:272
  66.9 4.6 %collective-permute-start.8 = (bf16[512,256]{1,0:T(8,128)(2,1)S(1)}, bf16[512,256]{1,0:T(8,128)(2,1)S(1)}, u32[]{:S(2)}, u32[]{:S(2)}) collective-permute-start(bf16[512,256]{1,0:T(8,128)(2,1)S(1)} %collective-permute-done.7.m_ref), channel_id=1, source_target_pairs={{0,14},{2,0},{4,2},{6,4},{8,6},{10,8},{12,10},{14,12},{1,15},{3,1}... | collective-permute-start | bytes 786440 | tf_op jit(solution)/shard_map/ppermute | solution.py:272
  73.3 1.9 %collective-permute-start.4 = (bf16[512,256]{1,0:T(8,128)(2,1)S(1)}, bf16[512,256]{1,0:T(8,128)(2,1)S(1)}, u32[]{:S(2)}, u32[]{:S(2)}) collective-permute-start(bf16[512,256]{1,0:T(8,128)(2,1)S(1)} %collective-permute-done.3.p_ref), channel_id=1, source_target_pairs={{0,2},{2,4},{4,6},{6,8},{8,10},{10,12},{12,14},{14,0},{1,3},{3,5},... | collective-permute-start | bytes 786440 | tf_op jit(solution)/shard_map/ppermute | solution.py:272
  75.2 4.6 %collective-permute-start.9 = (bf16[512,256]{1,0:T(8,128)(2,1)S(1)}, bf16[512,256]{1,0:T(8,128)(2,1)S(1)}, u32[]{:S(2)}, u32[]{:S(2)}) collective-permute-start(bf16[512,256]{1,0:T(8,128)(2,1)S(1)} %collective-permute-done.8.m_ref), channel_id=1, source_target_pairs={{0,14},{2,0},{4,2},{6,4},{8,6},{10,8},{12,10},{14,12},{1,15},{3,1}... | collective-permute-start | bytes 786440 | tf_op jit(solution)/shard_map/ppermute | solution.py:272
  81.6 1.9 %collective-permute-start.5 = (bf16[512,256]{1,0:T(8,128)(2,1)S(1)}, bf16[512,256]{1,0:T(8,128)(2,1)S(1)}, u32[]{:S(2)}, u32[]{:S(2)}) collective-permute-start(bf16[512,256]{1,0:T(8,128)(2,1)S(1)} %collective-permute-done.4.p_ref), channel_id=1, source_target_pairs={{0,2},{2,4},{4,6},{6,8},{8,10},{10,12},{12,14},{14,0},{1,3},{3,5},... | collective-permute-start | bytes 786440 | tf_op jit(solution)/shard_map/ppermute | solution.py:272
  86.2 3.7 %collective-permute-done.5.p_ref = bf16[512,256]{1,0:T(8,128)(2,1)S(1)} collective-permute-done((bf16[512,256]{1,0:T(8,128)(2,1)S(1)}, bf16[512,256]{1,0:T(8,128)(2,1)S(1)}, u32[]{:S(2)}, u32[]{:S(2)}) %collective-permute-start.5) | collective-permute-done | bytes 262176 | tf_op jit(solution)/shard_map/ppermute | solution.py:272
  90.9 1.9 %collective-permute-start.10 = (bf16[512,256]{1,0:T(8,128)(2,1)S(1)}, bf16[512,256]{1,0:T(8,128)(2,1)S(1)}, u32[]{:S(2)}, u32[]{:S(2)}) collective-permute-start(bf16[512,256]{1,0:T(8,128)(2,1)S(1)} %get-tuple-element.53), channel_id=1, source_target_pairs={{0,2},{2,4},{4,6},{6,8},{8,10},{10,12},{12,14},{14,0},{1,15},{3,1}... | collective-permute-start | bytes 786440 | tf_op jit(solution)/shard_map/ppermute | solution.py:272
  92.8 3.4 %collective-permute-start.14 = (bf16[512,256]{1,0:T(8,128)(2,1)S(1)}, bf16[512,256]{1,0:T(8,128)(2,1)S(1)}, u32[]{:S(2)}, u32[]{:S(2)}) collective-permute-start(bf16[512,256]{1,0:T(8,128)(2,1)S(1)} %get-tuple-element.56), channel_id=1, source_target_pairs={{0,14},{2,0},{4,2},{6,4},{8,6},{10,8},{12,10},{14,12},{1,3},{3,5},... | collective-permute-start | bytes 786440 | tf_op jit(solution)/shard_map/ppermute | solution.py:272
  98.1 3.1 %collective-permute-start.11 = (bf16[512,256]{1,0:T(8,128)(2,1)S(1)}, bf16[512,256]{1,0:T(8,128)(2,1)S(1)}, u32[]{:S(2)}, u32[]{:S(2)}) collective-permute-start(bf16[512,256]{1,0:T(8,128)(2,1)S(1)} %shard_map.119), channel_id=1, source_target_pairs={{0,2},{2,4},{4,6},{6,8},{8,10},{10,12},{12,14},{14,0},{1,15},{3,1}... | collective-permute-start | bytes 786440 | tf_op jit(solution)/shard_map/ppermute | solution.py:272
  101.3 2.2 %collective-permute-start.15 = (bf16[512,256]{1,0:T(8,128)(2,1)S(1)}, bf16[512,256]{1,0:T(8,128)(2,1)S(1)}, u32[]{:S(2)}, u32[]{:S(2)}) collective-permute-start(bf16[512,256]{1,0:T(8,128)(2,1)S(1)} %shard_map.122), channel_id=1, source_target_pairs={{0,14},{2,0},{4,2},{6,4},{8,6},{10,8},{12,10},{14,12},{1,3},{3,5},... | collective-permute-start | bytes 786440 | tf_op jit(solution)/shard_map/ppermute | solution.py:272
  103.4 2.7 %collective-permute-done.11.came_ref = bf16[512,256]{1,0:T(8,128)(2,1)S(1)} collective-permute-done((bf16[512,256]{1,0:T(8,128)(2,1)S(1)}, bf16[512,256]{1,0:T(8,128)(2,1)S(1)}, u32[]{:S(2)}, u32[]{:S(2)}) %collective-permute-start.11) | collective-permute-done | bytes 262176 | tf_op jit(solution)/shard_map/ppermute | solution.py:272
  106.2 3.4 %collective-permute-start.12 = (bf16[512,256]{1,0:T(8,128)(2,1)S(1)}, bf16[512,256]{1,0:T(8,128)(2,1)S(1)}, u32[]{:S(2)}, u32[]{:S(2)}) collective-permute-start(bf16[512,256]{1,0:T(8,128)(2,1)S(1)} %shard_map.120), channel_id=1, source_target_pairs={{0,2},{2,4},{4,6},{6,8},{8,10},{10,12},{12,14},{14,0},{1,15},{3,1}... | collective-permute-start | bytes 786440 | tf_op jit(solution)/shard_map/ppermute | solution.py:272
  109.7 1.9 %collective-permute-start.16 = (bf16[512,256]{1,0:T(8,128)(2,1)S(1)}, bf16[512,256]{1,0:T(8,128)(2,1)S(1)}, u32[]{:S(2)}, u32[]{:S(2)}) collective-permute-start(bf16[512,256]{1,0:T(8,128)(2,1)S(1)} %shard_map.123), channel_id=1, source_target_pairs={{0,14},{2,0},{4,2},{6,4},{8,6},{10,8},{12,10},{14,12},{1,3},{3,5},... | collective-permute-start | bytes 786440 | tf_op jit(solution)/shard_map/ppermute | solution.py:272
  113.3 4.6 %collective-permute-start.13 = (bf16[512,256]{1,0:T(8,128)(2,1)S(1)}, bf16[512,256]{1,0:T(8,128)(2,1)S(1)}, u32[]{:S(2)}, u32[]{:S(2)}) collective-permute-start(bf16[512,256]{1,0:T(8,128)(2,1)S(1)} %shard_map.121), channel_id=1, source_target_pairs={{0,2},{2,4},{4,6},{6,8},{8,10},{10,12},{12,14},{14,0},{1,15},{3,1}... | collective-permute-start | bytes 786440 | tf_op jit(solution)/shard_map/ppermute | solution.py:272
  119.0 2.3 %collective-permute-done.13.p_ref = bf16[512,256]{1,0:T(8,128)(2,1)S(1)} collective-permute-done((bf16[512,256]{1,0:T(8,128)(2,1)S(1)}, bf16[512,256]{1,0:T(8,128)(2,1)S(1)}, u32[]{:S(2)}, u32[]{:S(2)}) %collective-permute-start.13) | collective-permute-done | bytes 262176 | tf_op jit(solution)/shard_map/ppermute | solution.py:272
  121.3 22.7 %all_to_all.11 = bf16[32,16,256]{2,1,0:T(8,128)(2,1)S(1)} all-to-all(bf16[32,16,256]{2,1,0:T(8,128)(2,1)S(1)} %bitcast.18), channel_id=1, replica_groups=mesh['sp'=32,'tp'=16] {'sp'}, dimensions={0} | all-to-all | bytes 524288 | tf_op jit(solution)/shard_map/all_to_all | solution.py:378
  144.5 10.9 %collective-permute-start.17 = (f32[256,128]{1,0:T(8,128)S(1)}, f32[256,128]{1,0:T(8,128)S(1)}, u32[]{:S(2)}, u32[]{:S(2)}) collective-permute-start(f32[256,128]{1,0:T(8,128)S(1)} %get-tuple-element.58), channel_id=1, source_target_pairs={{0,1},{1,0},{2,3},{3,2},{4,5},{5,4},{6,7},{7,6},{8,9},{9,8},{10,11... | collective-permute-start | bytes 393224 | tf_op jit(solution)/shard_map/ppermute | solution.py:275
  (39 shorter events, 19.6 us)
Async XLA Ops:
  0.0 10.7 %copy-start.2 = (bf16[256,64]{0,1:T(8,128)(2,1)S(1)}, bf16[256,64]{0,1:T(8,128)(2,1)}, u32[]{:S(2)}) copy-start(bf16[256,64]{0,1:T(8,128)(2,1)} %param.11) | copy-start | bytes 98308
  0.0 31.9 %copy-start = (s32[256,2]{0,1:T(2,128)S(1)}, s32[256,2]{0,1:T(2,128)}, u32[]{:S(2)}) copy-start(s32[256,2]{0,1:T(2,128)} %param.17) | copy-start | bytes 6148
  1.9 81.6 %collective-permute-start.6 = (bf16[6144,256]{1,0:T(8,128)(2,1)S(1)}, bf16[6144,256]{1,0:T(8,128)(2,1)S(1)}, u32[]{:S(2)}, u32[]{:S(2)}) collective-permute-start(bf16[6144,256]{1,0:T(8,128)(2,1)S(1)} %shard_map.112.own_ref), channel_id=1, source_target_pairs={{0,1},{1,0},{2,3},{3,2},{4,5},{5,4},{6,7},{7,6},{8,9},{9,8},{10,11... | collective-permute-start | bytes 9437192 | tf_op jit(solution)/shard_map/ppermute | solution.py:275
  10.7 4.4 %collective-permute-start = (bf16[64,256]{1,0:T(8,128)(2,1)S(1)}, bf16[64,256]{1,0:T(8,128)(2,1)S(1)}, u32[]{:S(2)}, u32[]{:S(2)}) collective-permute-start(bf16[64,256]{1,0:T(8,128)(2,1)S(1)} %bitcast.28), channel_id=1, source_target_pairs={{0,16},{16,32},{32,48},{48,64},{64,80},{80,96},{96,112},{112,128},... | collective-permute-start | bytes 98312 | tf_op jit(solution)/shard_map/ppermute | solution.py:284
  13.1 18.8 %collective-permute-start.1 = (bf16[640,256]{1,0:T(8,128)(2,1)S(1)}, bf16[640,256]{1,0:T(8,128)(2,1)S(1)}, u32[]{:S(2)}, u32[]{:S(2)}) collective-permute-start(bf16[640,256]{1,0:T(8,128)(2,1)S(1)} %get-tuple-element.36.own_ref), channel_id=1, source_target_pairs={{0,1},{1,0},{2,3},{3,2},{4,5},{5,4},{6,7},{7,6},{8,9},{9,8},{10,11... | collective-permute-start | bytes 983048 | tf_op jit(solution)/shard_map/ppermute | solution.py:275
  56.7 8.3 %collective-permute-start.2 = (bf16[512,256]{1,0:T(8,128)(2,1)S(1)}, bf16[512,256]{1,0:T(8,128)(2,1)S(1)}, u32[]{:S(2)}, u32[]{:S(2)}) collective-permute-start(bf16[512,256]{1,0:T(8,128)(2,1)S(1)} %bitcast.15), channel_id=1, source_target_pairs={{0,2},{2,4},{4,6},{6,8},{8,10},{10,12},{12,14},{14,0},{1,3},{3,5},... | collective-permute-start | bytes 786440 | tf_op jit(solution)/shard_map/ppermute | solution.py:272
  58.6 8.3 %collective-permute-start.7 = (bf16[512,256]{1,0:T(8,128)(2,1)S(1)}, bf16[512,256]{1,0:T(8,128)(2,1)S(1)}, u32[]{:S(2)}, u32[]{:S(2)}) collective-permute-start(bf16[512,256]{1,0:T(8,128)(2,1)S(1)} %bitcast.16), channel_id=1, source_target_pairs={{0,14},{2,0},{4,2},{6,4},{8,6},{10,8},{12,10},{14,12},{1,15},{3,1}... | collective-permute-start | bytes 786440 | tf_op jit(solution)/shard_map/ppermute | solution.py:272
  65.0 8.3 %collective-permute-start.3 = (bf16[512,256]{1,0:T(8,128)(2,1)S(1)}, bf16[512,256]{1,0:T(8,128)(2,1)S(1)}, u32[]{:S(2)}, u32[]{:S(2)}) collective-permute-start(bf16[512,256]{1,0:T(8,128)(2,1)S(1)} %collective-permute-done.2.p_ref), channel_id=1, source_target_pairs={{0,2},{2,4},{4,6},{6,8},{8,10},{10,12},{12,14},{14,0},{1,3},{3,5},... | collective-permute-start | bytes 786440 | tf_op jit(solution)/shard_map/ppermute | solution.py:272
  66.9 8.3 %collective-permute-start.8 = (bf16[512,256]{1,0:T(8,128)(2,1)S(1)}, bf16[512,256]{1,0:T(8,128)(2,1)S(1)}, u32[]{:S(2)}, u32[]{:S(2)}) collective-permute-start(bf16[512,256]{1,0:T(8,128)(2,1)S(1)} %collective-permute-done.7.m_ref), channel_id=1, source_target_pairs={{0,14},{2,0},{4,2},{6,4},{8,6},{10,8},{12,10},{14,12},{1,15},{3,1}... | collective-permute-start | bytes 786440 | tf_op jit(solution)/shard_map/ppermute | solution.py:272
  73.3 8.3 %collective-permute-start.4 = (bf16[512,256]{1,0:T(8,128)(2,1)S(1)}, bf16[512,256]{1,0:T(8,128)(2,1)S(1)}, u32[]{:S(2)}, u32[]{:S(2)}) collective-permute-start(bf16[512,256]{1,0:T(8,128)(2,1)S(1)} %collective-permute-done.3.p_ref), channel_id=1, source_target_pairs={{0,2},{2,4},{4,6},{6,8},{8,10},{10,12},{12,14},{14,0},{1,3},{3,5},... | collective-permute-start | bytes 786440 | tf_op jit(solution)/shard_map/ppermute | solution.py:272
  75.2 10.2 %collective-permute-start.9 = (bf16[512,256]{1,0:T(8,128)(2,1)S(1)}, bf16[512,256]{1,0:T(8,128)(2,1)S(1)}, u32[]{:S(2)}, u32[]{:S(2)}) collective-permute-start(bf16[512,256]{1,0:T(8,128)(2,1)S(1)} %collective-permute-done.8.m_ref), channel_id=1, source_target_pairs={{0,14},{2,0},{4,2},{6,4},{8,6},{10,8},{12,10},{14,12},{1,15},{3,1}... | collective-permute-start | bytes 786440 | tf_op jit(solution)/shard_map/ppermute | solution.py:272
  81.6 8.3 %collective-permute-start.5 = (bf16[512,256]{1,0:T(8,128)(2,1)S(1)}, bf16[512,256]{1,0:T(8,128)(2,1)S(1)}, u32[]{:S(2)}, u32[]{:S(2)}) collective-permute-start(bf16[512,256]{1,0:T(8,128)(2,1)S(1)} %collective-permute-done.4.p_ref), channel_id=1, source_target_pairs={{0,2},{2,4},{4,6},{6,8},{8,10},{10,12},{12,14},{14,0},{1,3},{3,5},... | collective-permute-start | bytes 786440 | tf_op jit(solution)/shard_map/ppermute | solution.py:272
  90.9 7.1 %collective-permute-start.10 = (bf16[512,256]{1,0:T(8,128)(2,1)S(1)}, bf16[512,256]{1,0:T(8,128)(2,1)S(1)}, u32[]{:S(2)}, u32[]{:S(2)}) collective-permute-start(bf16[512,256]{1,0:T(8,128)(2,1)S(1)} %get-tuple-element.53), channel_id=1, source_target_pairs={{0,2},{2,4},{4,6},{6,8},{8,10},{10,12},{12,14},{14,0},{1,15},{3,1}... | collective-permute-start | bytes 786440 | tf_op jit(solution)/shard_map/ppermute | solution.py:272
  92.8 8.4 %collective-permute-start.14 = (bf16[512,256]{1,0:T(8,128)(2,1)S(1)}, bf16[512,256]{1,0:T(8,128)(2,1)S(1)}, u32[]{:S(2)}, u32[]{:S(2)}) collective-permute-start(bf16[512,256]{1,0:T(8,128)(2,1)S(1)} %get-tuple-element.56), channel_id=1, source_target_pairs={{0,14},{2,0},{4,2},{6,4},{8,6},{10,8},{12,10},{14,12},{1,3},{3,5},... | collective-permute-start | bytes 786440 | tf_op jit(solution)/shard_map/ppermute | solution.py:272
  98.1 8.0 %collective-permute-start.11 = (bf16[512,256]{1,0:T(8,128)(2,1)S(1)}, bf16[512,256]{1,0:T(8,128)(2,1)S(1)}, u32[]{:S(2)}, u32[]{:S(2)}) collective-permute-start(bf16[512,256]{1,0:T(8,128)(2,1)S(1)} %shard_map.119), channel_id=1, source_target_pairs={{0,2},{2,4},{4,6},{6,8},{8,10},{10,12},{12,14},{14,0},{1,15},{3,1}... | collective-permute-start | bytes 786440 | tf_op jit(solution)/shard_map/ppermute | solution.py:272
  101.3 8.3 %collective-permute-start.15 = (bf16[512,256]{1,0:T(8,128)(2,1)S(1)}, bf16[512,256]{1,0:T(8,128)(2,1)S(1)}, u32[]{:S(2)}, u32[]{:S(2)}) collective-permute-start(bf16[512,256]{1,0:T(8,128)(2,1)S(1)} %shard_map.122), channel_id=1, source_target_pairs={{0,14},{2,0},{4,2},{6,4},{8,6},{10,8},{12,10},{14,12},{1,3},{3,5},... | collective-permute-start | bytes 786440 | tf_op jit(solution)/shard_map/ppermute | solution.py:272
  106.2 37.8 %copy-start.1 = (f32[256,2]{0,1:T(2,128)S(1)}, f32[256,2]{0,1:T(2,128)}, u32[]{:S(2)}) copy-start(f32[256,2]{0,1:T(2,128)} %param.18) | copy-start | bytes 6148
  106.2 7.1 %collective-permute-start.12 = (bf16[512,256]{1,0:T(8,128)(2,1)S(1)}, bf16[512,256]{1,0:T(8,128)(2,1)S(1)}, u32[]{:S(2)}, u32[]{:S(2)}) collective-permute-start(bf16[512,256]{1,0:T(8,128)(2,1)S(1)} %shard_map.120), channel_id=1, source_target_pairs={{0,2},{2,4},{4,6},{6,8},{8,10},{10,12},{12,14},{14,0},{1,15},{3,1}... | collective-permute-start | bytes 786440 | tf_op jit(solution)/shard_map/ppermute | solution.py:272
  109.7 9.3 %collective-permute-start.16 = (bf16[512,256]{1,0:T(8,128)(2,1)S(1)}, bf16[512,256]{1,0:T(8,128)(2,1)S(1)}, u32[]{:S(2)}, u32[]{:S(2)}) collective-permute-start(bf16[512,256]{1,0:T(8,128)(2,1)S(1)} %shard_map.123), channel_id=1, source_target_pairs={{0,14},{2,0},{4,2},{6,4},{8,6},{10,8},{12,10},{14,12},{1,3},{3,5},... | collective-permute-start | bytes 786440 | tf_op jit(solution)/shard_map/ppermute | solution.py:272
  113.3 7.9 %collective-permute-start.13 = (bf16[512,256]{1,0:T(8,128)(2,1)S(1)}, bf16[512,256]{1,0:T(8,128)(2,1)S(1)}, u32[]{:S(2)}, u32[]{:S(2)}) collective-permute-start(bf16[512,256]{1,0:T(8,128)(2,1)S(1)} %shard_map.121), channel_id=1, source_target_pairs={{0,2},{2,4},{4,6},{6,8},{8,10},{10,12},{12,14},{14,0},{1,15},{3,1}... | collective-permute-start | bytes 786440 | tf_op jit(solution)/shard_map/ppermute | solution.py:272
  144.5 11.9 %collective-permute-start.17 = (f32[256,128]{1,0:T(8,128)S(1)}, f32[256,128]{1,0:T(8,128)S(1)}, u32[]{:S(2)}, u32[]{:S(2)}) collective-permute-start(f32[256,128]{1,0:T(8,128)S(1)} %get-tuple-element.58), channel_id=1, source_target_pairs={{0,1},{1,0},{2,3},{3,2},{4,5},{5,4},{6,7},{7,6},{8,9},{9,8},{10,11... | collective-permute-start | bytes 393224 | tf_op jit(solution)/shard_map/ppermute | solution.py:275

commit v8 on v4

--- a/solution.py
+++ b/solution.py
@@ -167,7 +167,7 @@
 
 def chip_across(chips, step):
     core = lax.rem(lax.axis_index("tp"), CORES)
-    return chip_at(chips, step * (1 - 2 * core))
+    return chip_at(chips, step * (2 * core - 1))
 
 
 def first_kernel(pack, chips, x_ref, gain_ref, own_ref, other_ref, acc_ref, square_ref):
@@ -354,9 +354,9 @@
     )
     part = dict(zip(steps, parts))
     for step in range(last - 1, -1, -1):
-        ahead = along(ahead, 1, -1)
+        ahead = along(ahead, -1, -1)
         if step:
-            back = along(back, -1, -1)
+            back = along(back, 1, -1)
             ahead = joined(part[step], ahead)
             back = joined(part[1 - step], back) if step > 1 else back
     result = call(own_kernel, pltpu.VMEM((held, width), BF16), (part[0], ahead, back), held * width, 8)

time: 158 us -> 159 us (level)
  waiting for transfers between devices: 19.6 us -> 25.2 us
  blocking collectives: 65.2 us -> 61.7 us
    ppermute x14, waiting for transfers between devices: 17.6 us -> 23.3 us  [along(): return lax.ppermute(value, 'tp', pairs)]
    all_to_all x1, blocking collectives: 22.7 us -> 19.2 us  [on_device(): lax.all_to_all(result.reshape(blocks, half, width), 'sp', split_axis=0, c...]
    ppermute x2, starting transfers between devices: 19.7 us -> 17.5 us  [across(): return lax.ppermute(value, 'tp', [(t, t ^ 1) for t in range(members)])]
  transfers between devices with their start and end apart: 17 -> 17, of which waited for: 11 -> 10; matrix products, arithmetic and copies ran while one was open for 0% -> 0% of each run, Pallas kernels for 3% -> 3%
where the time goes in v8:
time: 159 us
  starting transfers between devices  62 us (39%)
  blocking collectives  61.7 us (39%)
  waiting for transfers between devices  25.2 us (16%)
  Pallas kernels  9.43 us (6%)
    ppermute x14, starting transfers between devices, along(): return lax.ppermute(value, 'tp', pairs)  43.2 us
    all_to_all x1, blocking collectives, on_device(): lax.all_to_all(sent.reshape(experts, half, width), 'sp', split_axis=0, co...  25.9 us
    ppermute x14, waiting for transfers between devices, along(): return lax.ppermute(value, 'tp', pairs)  23.3 us
    all_to_all x1, blocking collectives, on_device(): lax.all_to_all(result.reshape(blocks, half, width), 'sp', split_axis=0, c...  19.2 us
    ppermute x2, starting transfers between devices, across(): return lax.ppermute(value, 'tp', [(t, t ^ 1) for t in range(members)])  17.5 us
    all_gather x1, blocking collectives, on_device(): mixed = lax.all_gather(pooled, 'tp', axis=0, tiled=False)  16.6 us
    pallas_call x17, Pallas kernels, call(): pl.pallas_call(kernel, out_shape=out_shape, in_specs=[pl.BlockSpec(memory...  9.43 us
  transfers between devices with their start and end apart: 17, of which 10 were waited for; matrix products, arithmetic and copies ran while one was open for 0% of the time, Pallas kernels for 3%

profile of v8, /device:TPU:1, one launch (start us, length us, event | category | flops | bytes accessed | tf_op | source)
XLA Modules:
  0.0 158.7 jit_solution(2288313015092487701)
XLA Ops:
  0.0 2.2 %shard_map.109 = (bf16[6784,256]{1,0:T(8,128)(2,1)S(1)}, bf16[64,256]{1,0:T(8,128)(2,1)S(1)}, bf16[64,64]{1,0:T(8,128)(2,1)S(1)}, bf16[1,64]{1,0:T(2,128)(2,1)S(1)}, bf16[1,128]{1,0:T(2,128)(2,1)S(1)}) custom-call(bf16[2048,256]{1,0:T(8,128)(2,1)} %bitcast.24, bf16[2048,256]{1,0:T(8,128)(2,1)} %bitcast.25, bf16[256,2048]{1,0:T(8,128)(2,1)} %bitcast.26, ...), custom_call_target="tpu_custom_call" | custom-call | flops 889192448 | bytes 1736704 | tf_op jit(solution)/shard_map/pallas_call | solution.py:33
  2.2 8.7 %collective-permute-start.1 = (bf16[6784,256]{1,0:T(8,128)(2,1)S(1)}, bf16[6784,256]{1,0:T(8,128)(2,1)S(1)}, u32[]{:S(2)}, u32[]{:S(2)}) collective-permute-start(bf16[6784,256]{1,0:T(8,128)(2,1)S(1)} %get-tuple-element.36.own_ref), channel_id=1, source_target_pairs={{0,1},{1,0},{2,3},{3,2},{4,5},{5,4},{6,7},{7,6},{8,9},{9,8},{10,11... | collective-permute-start | bytes 10420232 | tf_op jit(solution)/shard_map/ppermute | solution.py:270
  13.6 16.6 %all-gather = bf16[1280,256]{1,0:T(8,128)(2,1)S(1)} all-gather(bf16[80,256]{1,0:T(8,128)(2,1)S(1)} %shard_map.110), channel_id=2, replica_groups=mesh['sp'=32,'tp'=16] {'tp'}, dimensions={0}, use_global_device_ids=true | all-gather | bytes 696320 | tf_op jit(solution)/shard_map/all_gather | solution.py:300
  31.0 25.9 %all_to_all.10 = bf16[32,16,256]{2,1,0:T(8,128)(2,1)S(1)} all-to-all(bf16[32,16,256]{2,1,0:T(8,128)(2,1)S(1)} %bitcast.19), channel_id=1, replica_groups=mesh['sp'=32,'tp'=16] {'sp'}, dimensions={0} | all-to-all | bytes 524288 | tf_op jit(solution)/shard_map/all_to_all | solution.py:312
  57.0 1.9 %collective-permute-start.2 = (bf16[512,256]{1,0:T(8,128)(2,1)S(1)}, bf16[512,256]{1,0:T(8,128)(2,1)S(1)}, u32[]{:S(2)}, u32[]{:S(2)}) collective-permute-start(bf16[512,256]{1,0:T(8,128)(2,1)S(1)} %bitcast.15), channel_id=1, source_target_pairs={{0,2},{2,4},{4,6},{6,8},{8,10},{10,12},{12,14},{14,0},{1,3},{3,5},... | collective-permute-start | bytes 786440 | tf_op jit(solution)/shard_map/ppermute | solution.py:267
  58.9 4.6 %collective-permute-start.6 = (bf16[512,256]{1,0:T(8,128)(2,1)S(1)}, bf16[512,256]{1,0:T(8,128)(2,1)S(1)}, u32[]{:S(2)}, u32[]{:S(2)}) collective-permute-start(bf16[512,256]{1,0:T(8,128)(2,1)S(1)} %bitcast.16), channel_id=1, source_target_pairs={{0,14},{2,0},{4,2},{6,4},{8,6},{10,8},{12,10},{14,12},{1,15},{3,1}... | collective-permute-start | bytes 786440 | tf_op jit(solution)/shard_map/ppermute | solution.py:267
  65.3 1.9 %collective-permute-start.3 = (bf16[512,256]{1,0:T(8,128)(2,1)S(1)}, bf16[512,256]{1,0:T(8,128)(2,1)S(1)}, u32[]{:S(2)}, u32[]{:S(2)}) collective-permute-start(bf16[512,256]{1,0:T(8,128)(2,1)S(1)} %collective-permute-done.2.p_ref), channel_id=1, source_target_pairs={{0,2},{2,4},{4,6},{6,8},{8,10},{10,12},{12,14},{14,0},{1,3},{3,5},... | collective-permute-start | bytes 786440 | tf_op jit(solution)/shard_map/ppermute | solution.py:267
  67.2 4.6 %collective-permute-start.7 = (bf16[512,256]{1,0:T(8,128)(2,1)S(1)}, bf16[512,256]{1,0:T(8,128)(2,1)S(1)}, u32[]{:S(2)}, u32[]{:S(2)}) collective-permute-start(bf16[512,256]{1,0:T(8,128)(2,1)S(1)} %collective-permute-done.6.m_ref), channel_id=1, source_target_pairs={{0,14},{2,0},{4,2},{6,4},{8,6},{10,8},{12,10},{14,12},{1,15},{3,1}... | collective-permute-start | bytes 786440 | tf_op jit(solution)/shard_map/ppermute | solution.py:267
  73.6 1.9 %collective-permute-start.4 = (bf16[512,256]{1,0:T(8,128)(2,1)S(1)}, bf16[512,256]{1,0:T(8,128)(2,1)S(1)}, u32[]{:S(2)}, u32[]{:S(2)}) collective-permute-start(bf16[512,256]{1,0:T(8,128)(2,1)S(1)} %collective-permute-done.3.p_ref), channel_id=1, source_target_pairs={{0,2},{2,4},{4,6},{6,8},{8,10},{10,12},{12,14},{14,0},{1,3},{3,5},... | collective-permute-start | bytes 786440 | tf_op jit(solution)/shard_map/ppermute | solution.py:267
  75.5 4.6 %collective-permute-start.8 = (bf16[512,256]{1,0:T(8,128)(2,1)S(1)}, bf16[512,256]{1,0:T(8,128)(2,1)S(1)}, u32[]{:S(2)}, u32[]{:S(2)}) collective-permute-start(bf16[512,256]{1,0:T(8,128)(2,1)S(1)} %collective-permute-done.7.m_ref), channel_id=1, source_target_pairs={{0,14},{2,0},{4,2},{6,4},{8,6},{10,8},{12,10},{14,12},{1,15},{3,1}... | collective-permute-start | bytes 786440 | tf_op jit(solution)/shard_map/ppermute | solution.py:267
  81.9 1.9 %collective-permute-start.5 = (bf16[512,256]{1,0:T(8,128)(2,1)S(1)}, bf16[512,256]{1,0:T(8,128)(2,1)S(1)}, u32[]{:S(2)}, u32[]{:S(2)}) collective-permute-start(bf16[512,256]{1,0:T(8,128)(2,1)S(1)} %collective-permute-done.4.p_ref), channel_id=1, source_target_pairs={{0,2},{2,4},{4,6},{6,8},{8,10},{10,12},{12,14},{14,0},{1,3},{3,5},... | collective-permute-start | bytes 786440 | tf_op jit(solution)/shard_map/ppermute | solution.py:267
  86.5 3.7 %collective-permute-done.5.p_ref = bf16[512,256]{1,0:T(8,128)(2,1)S(1)} collective-permute-done((bf16[512,256]{1,0:T(8,128)(2,1)S(1)}, bf16[512,256]{1,0:T(8,128)(2,1)S(1)}, u32[]{:S(2)}, u32[]{:S(2)}) %collective-permute-start.5) | collective-permute-done | bytes 262176 | tf_op jit(solution)/shard_map/ppermute | solution.py:267
  91.2 1.9 %collective-permute-start.9 = (bf16[512,256]{1,0:T(8,128)(2,1)S(1)}, bf16[512,256]{1,0:T(8,128)(2,1)S(1)}, u32[]{:S(2)}, u32[]{:S(2)}) collective-permute-start(bf16[512,256]{1,0:T(8,128)(2,1)S(1)} %get-tuple-element.53), channel_id=1, source_target_pairs={{0,14},{2,0},{4,2},{6,4},{8,6},{10,8},{12,10},{14,12},{1,3},{3,5},... | collective-permute-start | bytes 786440 | tf_op jit(solution)/shard_map/ppermute | solution.py:267
  93.1 4.6 %collective-permute-start.13 = (bf16[512,256]{1,0:T(8,128)(2,1)S(1)}, bf16[512,256]{1,0:T(8,128)(2,1)S(1)}, u32[]{:S(2)}, u32[]{:S(2)}) collective-permute-start(bf16[512,256]{1,0:T(8,128)(2,1)S(1)} %get-tuple-element.56), channel_id=1, source_target_pairs={{0,2},{2,4},{4,6},{6,8},{8,10},{10,12},{12,14},{14,0},{1,15},{3,1}... | collective-permute-start | bytes 786440 | tf_op jit(solution)/shard_map/ppermute | solution.py:267
  99.6 1.9 %collective-permute-start.10 = (bf16[512,256]{1,0:T(8,128)(2,1)S(1)}, bf16[512,256]{1,0:T(8,128)(2,1)S(1)}, u32[]{:S(2)}, u32[]{:S(2)}) collective-permute-start(bf16[512,256]{1,0:T(8,128)(2,1)S(1)} %shard_map.118), channel_id=1, source_target_pairs={{0,14},{2,0},{4,2},{6,4},{8,6},{10,8},{12,10},{14,12},{1,3},{3,5},... | collective-permute-start | bytes 786440 | tf_op jit(solution)/shard_map/ppermute | solution.py:267
  101.6 5.1 %collective-permute-start.14 = (bf16[512,256]{1,0:T(8,128)(2,1)S(1)}, bf16[512,256]{1,0:T(8,128)(2,1)S(1)}, u32[]{:S(2)}, u32[]{:S(2)}) collective-permute-start(bf16[512,256]{1,0:T(8,128)(2,1)S(1)} %shard_map.121), channel_id=1, source_target_pairs={{0,2},{2,4},{4,6},{6,8},{8,10},{10,12},{12,14},{14,0},{1,15},{3,1}... | collective-permute-start | bytes 786440 | tf_op jit(solution)/shard_map/ppermute | solution.py:267
  106.6 3.4 %collective-permute-done.10.came_ref = bf16[512,256]{1,0:T(8,128)(2,1)S(1)} collective-permute-done((bf16[512,256]{1,0:T(8,128)(2,1)S(1)}, bf16[512,256]{1,0:T(8,128)(2,1)S(1)}, u32[]{:S(2)}, u32[]{:S(2)}) %collective-permute-start.10) | collective-permute-done | bytes 262176 | tf_op jit(solution)/shard_map/ppermute | solution.py:267
  110.1 1.9 %collective-permute-start.11 = (bf16[512,256]{1,0:T(8,128)(2,1)S(1)}, bf16[512,256]{1,0:T(8,128)(2,1)S(1)}, u32[]{:S(2)}, u32[]{:S(2)}) collective-permute-start(bf16[512,256]{1,0:T(8,128)(2,1)S(1)} %shard_map.119), channel_id=1, source_target_pairs={{0,14},{2,0},{4,2},{6,4},{8,6},{10,8},{12,10},{14,12},{1,3},{3,5},... | collective-permute-start | bytes 786440 | tf_op jit(solution)/shard_map/ppermute | solution.py:267
  112.1 4.6 %collective-permute-start.15 = (bf16[512,256]{1,0:T(8,128)(2,1)S(1)}, bf16[512,256]{1,0:T(8,128)(2,1)S(1)}, u32[]{:S(2)}, u32[]{:S(2)}) collective-permute-start(bf16[512,256]{1,0:T(8,128)(2,1)S(1)} %shard_map.122), channel_id=1, source_target_pairs={{0,2},{2,4},{4,6},{6,8},{8,10},{10,12},{12,14},{14,0},{1,15},{3,1}... | collective-permute-start | bytes 786440 | tf_op jit(solution)/shard_map/ppermute | solution.py:267
  116.7 3.1 %collective-permute-done.11.came_ref = bf16[512,256]{1,0:T(8,128)(2,1)S(1)} collective-permute-done((bf16[512,256]{1,0:T(8,128)(2,1)S(1)}, bf16[512,256]{1,0:T(8,128)(2,1)S(1)}, u32[]{:S(2)}, u32[]{:S(2)}) %collective-permute-start.11) | collective-permute-done | bytes 262176 | tf_op jit(solution)/shard_map/ppermute | solution.py:267
  119.8 1.9 %collective-permute-start.12 = (bf16[512,256]{1,0:T(8,128)(2,1)S(1)}, bf16[512,256]{1,0:T(8,128)(2,1)S(1)}, u32[]{:S(2)}, u32[]{:S(2)}) collective-permute-start(bf16[512,256]{1,0:T(8,128)(2,1)S(1)} %shard_map.120), channel_id=1, source_target_pairs={{0,14},{2,0},{4,2},{6,4},{8,6},{10,8},{12,10},{14,12},{1,3},{3,5},... | collective-permute-start | bytes 786440 | tf_op jit(solution)/shard_map/ppermute | solution.py:267
  121.7 6.8 %collective-permute-done.12.p_ref = bf16[512,256]{1,0:T(8,128)(2,1)S(1)} collective-permute-done((bf16[512,256]{1,0:T(8,128)(2,1)S(1)}, bf16[512,256]{1,0:T(8,128)(2,1)S(1)}, u32[]{:S(2)}, u32[]{:S(2)}) %collective-permute-start.12) | collective-permute-done | bytes 262176 | tf_op jit(solution)/shard_map/ppermute | solution.py:267
  128.6 19.2 %all_to_all.11 = bf16[32,16,256]{2,1,0:T(8,128)(2,1)S(1)} all-to-all(bf16[32,16,256]{2,1,0:T(8,128)(2,1)S(1)} %bitcast.18), channel_id=1, replica_groups=mesh['sp'=32,'tp'=16] {'sp'}, dimensions={0} | all-to-all | bytes 524288 | tf_op jit(solution)/shard_map/all_to_all | solution.py:363
  148.4 8.8 %collective-permute-start.16 = (f32[256,128]{1,0:T(8,128)S(1)}, f32[256,128]{1,0:T(8,128)S(1)}, u32[]{:S(2)}, u32[]{:S(2)}) collective-permute-start(f32[256,128]{1,0:T(8,128)S(1)} %get-tuple-element.58), channel_id=1, source_target_pairs={{0,1},{1,0},{2,3},{3,2},{4,5},{5,4},{6,7},{7,6},{8,9},{9,8},{10,11... | collective-permute-start | bytes 393224 | tf_op jit(solution)/shard_map/ppermute | solution.py:270
  (36 shorter events, 16.8 us)
Async XLA Ops:
  0.0 11.0 %copy-start.2 = (bf16[256,64]{0,1:T(8,128)(2,1)S(1)}, bf16[256,64]{0,1:T(8,128)(2,1)}, u32[]{:S(2)}) copy-start(bf16[256,64]{0,1:T(8,128)(2,1)} %param.11) | copy-start | bytes 98308
  0.0 30.2 %copy-start = (s32[256,2]{0,1:T(2,128)S(1)}, s32[256,2]{0,1:T(2,128)}, u32[]{:S(2)}) copy-start(s32[256,2]{0,1:T(2,128)} %param.17) | copy-start | bytes 6148
  2.2 28.0 %collective-permute-start.1 = (bf16[6784,256]{1,0:T(8,128)(2,1)S(1)}, bf16[6784,256]{1,0:T(8,128)(2,1)S(1)}, u32[]{:S(2)}, u32[]{:S(2)}) collective-permute-start(bf16[6784,256]{1,0:T(8,128)(2,1)S(1)} %get-tuple-element.36.own_ref), channel_id=1, source_target_pairs={{0,1},{1,0},{2,3},{3,2},{4,5},{5,4},{6,7},{7,6},{8,9},{9,8},{10,11... | collective-permute-start | bytes 10420232 | tf_op jit(solution)/shard_map/ppermute | solution.py:270
  11.0 2.3 %collective-permute-start = (bf16[64,256]{1,0:T(8,128)(2,1)S(1)}, bf16[64,256]{1,0:T(8,128)(2,1)S(1)}, u32[]{:S(2)}, u32[]{:S(2)}) collective-permute-start(bf16[64,256]{1,0:T(8,128)(2,1)S(1)} %bitcast.28), channel_id=1, source_target_pairs={{0,16},{16,32},{32,48},{48,64},{64,80},{80,96},{96,112},{112,128},... | collective-permute-start | bytes 98312 | tf_op jit(solution)/shard_map/ppermute | solution.py:275
  57.0 8.3 %collective-permute-start.2 = (bf16[512,256]{1,0:T(8,128)(2,1)S(1)}, bf16[512,256]{1,0:T(8,128)(2,1)S(1)}, u32[]{:S(2)}, u32[]{:S(2)}) collective-permute-start(bf16[512,256]{1,0:T(8,128)(2,1)S(1)} %bitcast.15), channel_id=1, source_target_pairs={{0,2},{2,4},{4,6},{6,8},{8,10},{10,12},{12,14},{14,0},{1,3},{3,5},... | collective-permute-start | bytes 786440 | tf_op jit(solution)/shard_map/ppermute | solution.py:267
  58.9 8.3 %collective-permute-start.6 = (bf16[512,256]{1,0:T(8,128)(2,1)S(1)}, bf16[512,256]{1,0:T(8,128)(2,1)S(1)}, u32[]{:S(2)}, u32[]{:S(2)}) collective-permute-start(bf16[512,256]{1,0:T(8,128)(2,1)S(1)} %bitcast.16), channel_id=1, source_target_pairs={{0,14},{2,0},{4,2},{6,4},{8,6},{10,8},{12,10},{14,12},{1,15},{3,1}... | collective-permute-start | bytes 786440 | tf_op jit(solution)/shard_map/ppermute | solution.py:267
  65.3 8.3 %collective-permute-start.3 = (bf16[512,256]{1,0:T(8,128)(2,1)S(1)}, bf16[512,256]{1,0:T(8,128)(2,1)S(1)}, u32[]{:S(2)}, u32[]{:S(2)}) collective-permute-start(bf16[512,256]{1,0:T(8,128)(2,1)S(1)} %collective-permute-done.2.p_ref), channel_id=1, source_target_pairs={{0,2},{2,4},{4,6},{6,8},{8,10},{10,12},{12,14},{14,0},{1,3},{3,5},... | collective-permute-start | bytes 786440 | tf_op jit(solution)/shard_map/ppermute | solution.py:267
  67.2 8.3 %collective-permute-start.7 = (bf16[512,256]{1,0:T(8,128)(2,1)S(1)}, bf16[512,256]{1,0:T(8,128)(2,1)S(1)}, u32[]{:S(2)}, u32[]{:S(2)}) collective-permute-start(bf16[512,256]{1,0:T(8,128)(2,1)S(1)} %collective-permute-done.6.m_ref), channel_id=1, source_target_pairs={{0,14},{2,0},{4,2},{6,4},{8,6},{10,8},{12,10},{14,12},{1,15},{3,1}... | collective-permute-start | bytes 786440 | tf_op jit(solution)/shard_map/ppermute | solution.py:267
  73.6 8.3 %collective-permute-start.4 = (bf16[512,256]{1,0:T(8,128)(2,1)S(1)}, bf16[512,256]{1,0:T(8,128)(2,1)S(1)}, u32[]{:S(2)}, u32[]{:S(2)}) collective-permute-start(bf16[512,256]{1,0:T(8,128)(2,1)S(1)} %collective-permute-done.3.p_ref), channel_id=1, source_target_pairs={{0,2},{2,4},{4,6},{6,8},{8,10},{10,12},{12,14},{14,0},{1,3},{3,5},... | collective-permute-start | bytes 786440 | tf_op jit(solution)/shard_map/ppermute | solution.py:267
  75.5 10.2 %collective-permute-start.8 = (bf16[512,256]{1,0:T(8,128)(2,1)S(1)}, bf16[512,256]{1,0:T(8,128)(2,1)S(1)}, u32[]{:S(2)}, u32[]{:S(2)}) collective-permute-start(bf16[512,256]{1,0:T(8,128)(2,1)S(1)} %collective-permute-done.7.m_ref), channel_id=1, source_target_pairs={{0,14},{2,0},{4,2},{6,4},{8,6},{10,8},{12,10},{14,12},{1,15},{3,1}... | collective-permute-start | bytes 786440 | tf_op jit(solution)/shard_map/ppermute | solution.py:267
  81.9 8.3 %collective-permute-start.5 = (bf16[512,256]{1,0:T(8,128)(2,1)S(1)}, bf16[512,256]{1,0:T(8,128)(2,1)S(1)}, u32[]{:S(2)}, u32[]{:S(2)}) collective-permute-start(bf16[512,256]{1,0:T(8,128)(2,1)S(1)} %collective-permute-done.4.p_ref), channel_id=1, source_target_pairs={{0,2},{2,4},{4,6},{6,8},{8,10},{10,12},{12,14},{14,0},{1,3},{3,5},... | collective-permute-start | bytes 786440 | tf_op jit(solution)/shard_map/ppermute | solution.py:267
  91.2 8.3 %collective-permute-start.9 = (bf16[512,256]{1,0:T(8,128)(2,1)S(1)}, bf16[512,256]{1,0:T(8,128)(2,1)S(1)}, u32[]{:S(2)}, u32[]{:S(2)}) collective-permute-start(bf16[512,256]{1,0:T(8,128)(2,1)S(1)} %get-tuple-element.53), channel_id=1, source_target_pairs={{0,14},{2,0},{4,2},{6,4},{8,6},{10,8},{12,10},{14,12},{1,3},{3,5},... | collective-permute-start | bytes 786440 | tf_op jit(solution)/shard_map/ppermute | solution.py:267
  93.1 8.4 %collective-permute-start.13 = (bf16[512,256]{1,0:T(8,128)(2,1)S(1)}, bf16[512,256]{1,0:T(8,128)(2,1)S(1)}, u32[]{:S(2)}, u32[]{:S(2)}) collective-permute-start(bf16[512,256]{1,0:T(8,128)(2,1)S(1)} %get-tuple-element.56), channel_id=1, source_target_pairs={{0,2},{2,4},{4,6},{6,8},{8,10},{10,12},{12,14},{14,0},{1,15},{3,1}... | collective-permute-start | bytes 786440 | tf_op jit(solution)/shard_map/ppermute | solution.py:267
  99.6 10.5 %collective-permute-start.10 = (bf16[512,256]{1,0:T(8,128)(2,1)S(1)}, bf16[512,256]{1,0:T(8,128)(2,1)S(1)}, u32[]{:S(2)}, u32[]{:S(2)}) collective-permute-start(bf16[512,256]{1,0:T(8,128)(2,1)S(1)} %shard_map.118), channel_id=1, source_target_pairs={{0,14},{2,0},{4,2},{6,4},{8,6},{10,8},{12,10},{14,12},{1,3},{3,5},... | collective-permute-start | bytes 786440 | tf_op jit(solution)/shard_map/ppermute | solution.py:267
  101.6 10.5 %collective-permute-start.14 = (bf16[512,256]{1,0:T(8,128)(2,1)S(1)}, bf16[512,256]{1,0:T(8,128)(2,1)S(1)}, u32[]{:S(2)}, u32[]{:S(2)}) collective-permute-start(bf16[512,256]{1,0:T(8,128)(2,1)S(1)} %shard_map.121), channel_id=1, source_target_pairs={{0,2},{2,4},{4,6},{6,8},{8,10},{10,12},{12,14},{14,0},{1,15},{3,1}... | collective-permute-start | bytes 786440 | tf_op jit(solution)/shard_map/ppermute | solution.py:267
  110.1 37.7 %copy-start.1 = (f32[256,2]{0,1:T(2,128)S(1)}, f32[256,2]{0,1:T(2,128)}, u32[]{:S(2)}) copy-start(f32[256,2]{0,1:T(2,128)} %param.18) | copy-start | bytes 6148
  110.1 9.6 %collective-permute-start.11 = (bf16[512,256]{1,0:T(8,128)(2,1)S(1)}, bf16[512,256]{1,0:T(8,128)(2,1)S(1)}, u32[]{:S(2)}, u32[]{:S(2)}) collective-permute-start(bf16[512,256]{1,0:T(8,128)(2,1)S(1)} %shard_map.119), channel_id=1, source_target_pairs={{0,14},{2,0},{4,2},{6,4},{8,6},{10,8},{12,10},{14,12},{1,3},{3,5},... | collective-permute-start | bytes 786440 | tf_op jit(solution)/shard_map/ppermute | solution.py:267
  112.1 9.6 %collective-permute-start.15 = (bf16[512,256]{1,0:T(8,128)(2,1)S(1)}, bf16[512,256]{1,0:T(8,128)(2,1)S(1)}, u32[]{:S(2)}, u32[]{:S(2)}) collective-permute-start(bf16[512,256]{1,0:T(8,128)(2,1)S(1)} %shard_map.122), channel_id=1, source_target_pairs={{0,2},{2,4},{4,6},{6,8},{8,10},{10,12},{12,14},{14,0},{1,15},{3,1}... | collective-permute-start | bytes 786440 | tf_op jit(solution)/shard_map/ppermute | solution.py:267
  119.8 8.8 %collective-permute-start.12 = (bf16[512,256]{1,0:T(8,128)(2,1)S(1)}, bf16[512,256]{1,0:T(8,128)(2,1)S(1)}, u32[]{:S(2)}, u32[]{:S(2)}) collective-permute-start(bf16[512,256]{1,0:T(8,128)(2,1)S(1)} %shard_map.120), channel_id=1, source_target_pairs={{0,14},{2,0},{4,2},{6,4},{8,6},{10,8},{12,10},{14,12},{1,3},{3,5},... | collective-permute-start | bytes 786440 | tf_op jit(solution)/shard_map/ppermute | solution.py:267
  148.4 9.7 %collective-permute-start.16 = (f32[256,128]{1,0:T(8,128)S(1)}, f32[256,128]{1,0:T(8,128)S(1)}, u32[]{:S(2)}, u32[]{:S(2)}) collective-permute-start(f32[256,128]{1,0:T(8,128)S(1)} %get-tuple-element.58), channel_id=1, source_target_pairs={{0,1},{1,0},{2,3},{3,2},{4,5},{5,4},{6,7},{7,6},{8,9},{9,8},{10,11... | collective-permute-start | bytes 393224 | tf_op jit(solution)/shard_map/ppermute | solution.py:270
